TPU v7x, 32 devices: a whole 2x2x4 slice. The times are simulated.
32 devices in a mesh: sp: 8 (over z, y), tp: 4 (over x, core).
Axes of the slice: x: 2, y: 2, z: 4, core: 2. Of those that a mesh axis runs over, the one named last changes fastest.
Arguments:
- stream: bfloat16 [2048, 2048], P('sp'), may hold values from -6 to 6
- attn_gain: float32 [2, 2048], replicated, may hold values from 0.1 to 1.9
- w_query: bfloat16 [2, 2048, 2048], P(None, None, 'tp'), may hold values from -0.125 to 0.125
- w_key: bfloat16 [2, 2048, 512], P(None, None, 'tp'), may hold values from -0.125 to 0.125
- w_value: bfloat16 [2, 2048, 512], P(None, None, 'tp'), may hold values from -0.125 to 0.125
- w_out: bfloat16 [2, 2048, 2048], P(None, 'tp'), may hold values from -1 to 1
- query_gain: float32 [2, 64], replicated, may hold values from 0.1 to 1.9
- key_gain: float32 [2, 64], replicated, may hold values from 0.1 to 1.9
- rel_bias: float32 [2, 32, 257], P(None, 'tp'), may hold values from -6 to 300
Outputs:
- result: bfloat16 [2048, 2048], P('sp', 'tp')
All inputs are finite; a program needn't handle non-finite values.
Results may differ from a plain program's by a relative error of at most 0.02.
Values may be sent and summed in bfloat16 or wider, within the bound.
No kernel may reach another device: no remote copies, remote signals or barrier semaphores. Data moves between devices by JAX's collectives and lax.ppermute only.
A program may use at most 64 MiB of HBM per device.

v0:
```python
import jax
import jax.numpy as jnp
from jax import lax
from jax.sharding import PartitionSpec as P

HEAD_DIM = 64
SEG = 64
LEFT = 4
CLIP = 128
LAYERS = 2


norm_eps = 1e-06
masked_score = -1e30


def passed_along(value, axis, steps):
    count = lax.axis_size(axis)
    initial, last = (max(0, -steps), min(count, count - steps))
    return lax.ppermute(value, axis, [(source, source + steps) for source in range(initial, last)])


def rms_scale(values_in, gain):
    squared = jnp.mean(values_in * values_in, axis=-1, keepdims=True)
    return values_in * lax.rsqrt(squared + norm_eps) * gain


def segment_bias(bias_table, span):
    line_len = SEG + span - 1
    offset = jnp.arange(line_len, dtype=jnp.int32)
    distance = jnp.clip(LEFT * SEG + SEG - 1 - offset, -CLIP, CLIP) + CLIP
    table_cols = jnp.arange(bias_table.shape[1], dtype=jnp.int32)
    onehot = (table_cols[:, None] == distance[None, :]).astype(jnp.float32)
    line = jnp.dot(
        bias_table, onehot, precision=lax.Precision.HIGHEST, preferred_element_type=jnp.float32
    )
    rows = [line[:, SEG - 1 - q : SEG - 1 - q + span] for q in range(SEG)]
    return jnp.stack(rows, axis=1)


def project_pair(normed, key_weight, value_weight, key_gain_row):
    row_count = normed.shape[0]
    key_flat = jnp.dot(normed, key_weight, preferred_element_type=jnp.float32)
    keys_made = (
        rms_scale(key_flat.reshape(row_count, -1, HEAD_DIM), key_gain_row)
        .astype(jnp.bfloat16)
        .reshape(row_count, -1)
    )
    values_made = jnp.dot(normed, value_weight, preferred_element_type=jnp.float32).astype(
        jnp.bfloat16
    )
    return (keys_made, values_made)


def band_attention(queries, keys_all, values_all, bias_table, first_pos):
    key_reach = LEFT * SEG
    span = (LEFT + 1) * SEG
    row_count = queries.shape[0]
    kv_here = keys_all.shape[1] // HEAD_DIM
    heads_here = queries.shape[1] // HEAD_DIM
    group = heads_here // kv_here
    bias = segment_bias(bias_table, span).reshape(kv_here, group, 1, SEG, span)
    seg_index = jnp.arange(LEFT, dtype=jnp.int32)[:, None]
    key_index = jnp.arange(span, dtype=jnp.int32)[None, :]

    def one_block(block_index):
        start = block_index * key_reach
        query_rows = queries.reshape(LEFT, SEG, kv_here, group, HEAD_DIM)
        key_rows = keys_all.reshape(2 * key_reach, kv_here, HEAD_DIM)
        value_rows = values_all.reshape(2 * key_reach, kv_here, HEAD_DIM)
        key_windows = jnp.stack([key_rows[q * SEG : q * SEG + span] for q in range(LEFT)], axis=0)
        value_windows = jnp.stack(
            [value_rows[q * SEG : q * SEG + span] for q in range(LEFT)], axis=0
        )
        scores = (
            jnp.einsum(
                "nqkgd,njkd->kgnqj", query_rows, key_windows, preferred_element_type=jnp.float32
            )
            * HEAD_DIM ** (-0.5)
            + bias
        )
        inside = first_pos + start + (seg_index - LEFT) * SEG + key_index >= 0
        scores = jnp.where(inside[None, None, :, None, :], scores, masked_score)
        peak = jnp.max(scores, axis=-1, keepdims=True)
        expon = jnp.exp(scores - peak)
        weights = (expon / jnp.sum(expon, axis=-1, keepdims=True)).astype(jnp.bfloat16)
        mixed = jnp.einsum(
            "kgnqj,njkd->nqkgd", weights, value_windows, preferred_element_type=jnp.float32
        )
        return mixed.astype(jnp.bfloat16).reshape(key_reach, heads_here * HEAD_DIM)

    blocks = lax.map(one_block, jnp.arange(row_count // key_reach, dtype=jnp.int32))
    return blocks.reshape(row_count, heads_here * HEAD_DIM)


def local(stream, attn_gain, w_query, w_key, w_value, w_out, query_gain, key_gain, rel_bias):
    row_count = stream.shape[0]
    key_reach = LEFT * SEG
    first_pos = lax.axis_index("sp") * row_count
    current = stream
    for layer_index in range(LAYERS):
        normed = rms_scale(current.astype(jnp.float32), attn_gain[layer_index]).astype(jnp.bfloat16)
        query_flat = jnp.dot(normed, w_query[layer_index], preferred_element_type=jnp.float32)
        queries = (
            rms_scale(query_flat.reshape(row_count, -1, HEAD_DIM), query_gain[layer_index])
            .astype(jnp.bfloat16)
            .reshape(row_count, -1)
        )
        keys_now, values_now = project_pair(
            normed, w_key[layer_index], w_value[layer_index], key_gain[layer_index]
        )
        rows_prior = passed_along(normed, "sp", 1)
        keys_prior, values_prior = project_pair(
            rows_prior, w_key[layer_index], w_value[layer_index], key_gain[layer_index]
        )
        keys_all = jnp.concatenate([keys_prior, keys_now], axis=0)
        values_all = jnp.concatenate([values_prior, values_now], axis=0)
        mixed = band_attention(queries, keys_all, values_all, rel_bias[layer_index], first_pos)
        partial_value = jnp.dot(mixed, w_out[layer_index], preferred_element_type=jnp.float32)
        if layer_index < LAYERS - 1:
            summed = lax.psum(partial_value.astype(jnp.bfloat16), "tp").astype(jnp.float32)
            current = (current.astype(jnp.float32) + summed).astype(jnp.bfloat16)
        else:
            summed = lax.psum_scatter(
                partial_value.astype(jnp.bfloat16), "tp", scatter_dimension=1, tiled=True
            ).astype(jnp.float32)
            feature_cols = summed.shape[1]
            own_cols = lax.dynamic_slice_in_dim(
                current, lax.axis_index("tp") * feature_cols, feature_cols, 1
            )
            current = (own_cols.astype(jnp.float32) + summed).astype(jnp.bfloat16)
    return current


def solution(mesh):
    return jax.shard_map(
        local,
        mesh=mesh,
        in_specs=(
            P("sp", None),
            P(),
            P(None, None, "tp"),
            P(None, None, "tp"),
            P(None, None, "tp"),
            P(None, "tp", None),
            P(),
            P(),
            P(None, "tp", None),
        ),
        out_specs=P("sp", "tp"),
        check_vma=False,
    )
```

profile of v0, /device:TPU:0, one launch (start us, length us, event | category | flops | bytes accessed | tf_op | source)
XLA Modules:
  0.0 247.3 jit_solution(2282217195734289427)
XLA Ops:
  7.9 1.5 fusion.11
  9.5 2.5 %fusion.13 = bf16[256,2048]{1,0:T(8,128)(2,1)} fusion(bf16[256,2048]{1,0:T(8,128)(2,1)} %param.9, f32[2048]{0:T(1024)S(1)} %bitcast.209, f32[256]{0:T(256)S(1)} %add_rsqrt_fusion.7), kind=kLoop, calls=%fused_computation.24 | loop fusion | flops 2097152 | bytes 2106368 | tf_op jit(solution)/shard_map/convert_element_type | solution.py:102
  12.0 5.9 %collective-permute-start = (bf16[256,2048]{1,0:T(8,128)(2,1)}, bf16[256,2048]{1,0:T(8,128)(2,1)}, u32[]{:S(2)}, u32[]{:S(2)}) collective-permute-start(bf16[256,2048]{1,0:T(8,128)(2,1)} %fusion.13), channel_id=1, source_target_pairs={{0,4},{4,8},{8,12},{12,16},{16,20},{20,24},{24,28},{1,5},{5,9},{9,... | collective-permute-start | bytes 3145736 | tf_op jit(solution)/shard_map/ppermute | solution.py:20
  21.2 3.8 %slice_bitcast_fusion.1 = (bf16[512,2048]{0,1:T(8,128)(2,1)}, bf16[512,2048]{0,1:T(8,128)(2,1)S(1)}) fusion(bf16[2,2048,512]{2,1,0:T(8,128)(2,1)} %param.11), kind=kLoop, calls=%fused_computation.31 | loop fusion | bytes 8388608 | tf_op jit(solution)/shard_map/dot_general | solution.py:103
  25.1 4.0 %copy.159 = bf16[512,2048]{1,0:T(8,128)(2,1)} copy(bf16[512,2048]{0,1:T(8,128)(2,1)} %get-tuple-element.41) | data formatting | bytes 4194304 | tf_op jit(solution)/shard_map/dot_general | solution.py:103
  29.0 3.5 %multiply_reduce_fusion.1 = (f32[256,8]{0,1:T(8,128)S(1)}, f32[256,8,64]{0,2,1:T(8,128)}) fusion(bf16[8,64,2048]{2,1,0:T(8,128)(2,1)} %bitcast.185, bf16[256,2048]{1,0:T(8,128)(2,1)} %fusion.13), kind=kOutput, calls=%fused_computation.79 | convolution fusion | flops 537131008 | bytes 3678208 | tf_op jit(solution)/shard_map/dot_general | solution.py:103
  35.0 1.8 multiply_reduce_fusion.4
  96.6 7.7 %stack.544 = f32[2,4,1,64,320]{4,3,1,0,2:T(8,128)S(1)} concatenate(f32[2,4,1,1,320]{4,3,1,0,2:T(1,128)} %stack.620, f32[2,4,1,1,320]{4,3,1,0,2:T(1,128)} %stack.621, f32[2,4,1,1,320]{4,3,1,0,2:T(1,128)} %stack.622, f32[2,4,1,1,320]{4,3,1,0,2:T(1,128)} %stack.623, f32[2,4,1,1,320]{4,3,1,0,2:T(1,128)} %stack.624, f32[2,4,1,1,320]{4,3,1,0,2:T(1,128)} %stack.625, ...), dimensions={3} | concatenate | bytes 1310720 | tf_op jit(solution)/shard_map/stack | solution.py:38
  106.7 1.8 convolution_convert_fusion.4
  108.5 1.7 convolution_convert_fusion.5
  111.0 1.6 copy.157
  112.6 1.6 copy.156
  114.2 1.6 copy.155
  115.9 1.6 copy.154
  117.5 1.7 multiply_reduce_fusion.5
  120.2 4.1 %fusion.143 = (f32[2,4,4,64]{3,1,2,0:T(4,128)S(1)}, f32[2,4,4,64,320]{4,3,1,2,0:T(8,128)}) fusion(f32[2,4,64,320]{3,2,1,0:T(8,128)S(1)} %bitcast.187, pred[4,320]{1,0:T(4,128)(4,1)} %add_compare_fusion, bf16[4,64,2,4,64]{1,0,4,3,2:T(4,128)(2,1)} %reshape_reshape.8, bf16[1,320,2,64]{1,3,0,2:T(8,128)(2,1)S(1)} %bitcast.198, ...), kind=kOutput, calls=%fused_computation.202 | convolution fusion | flops 88473920 | bytes 3876096 | tf_op jit(solution)/shard_map/while/body/eval_jaxpr/sub | solution.py:85
  124.3 3.2 %fusion.40 = bf16[4,64,2,4,64]{1,4,3,2,0:T(8,128)(2,1)S(1)} fusion(bf16[1,320,2,64]{1,3,2,0:T(8,128)(2,1)S(1)} %bitcast.202, bf16[1,320,2,64]{1,3,2,0:T(8,128)(2,1)S(1)} %bitcast.204, bf16[1,320,2,64]{1,3,2,0:T(8,128)(2,1)} %bitcast.205, bf16[1,320,2,64]{1,3,2,0:T(8,128)(2,1)} %bitcast.207, f32[2,4,4,64,320]{4,3,1,2,0:T(8,128)} %get-tuple-element.226, ...), kind=kOutput, calls=%fused_computation.47 | convolution fusion | flops 86638592 | bytes 3219456 | tf_op jit(solution)/shard_map/while/body/eval_jaxpr/kgnqj,njkd->nqkgd/dot_general | solution.py:87
  128.3 3.4 %convolution_convert_fusion.1 = bf16[256,2048]{1,0:T(8,128)(2,1)} fusion(bf16[256,512]{1,0:T(8,128)(2,1)S(1)} %reshape.444, bf16[2,512,2048]{2,1,0:T(8,128)(2,1)} %param.14), kind=kOutput, calls=%fused_computation.16 | convolution fusion | flops 537395200 | bytes 3407872 | tf_op jit(solution)/shard_map/dot_general | solution.py:119
  152.2 2.5 %copy.232 = bf16[512,2048]{1,0:T(8,128)(2,1)} copy(bf16[512,2048]{0,1:T(8,128)(2,1)S(1)} %get-tuple-element.42) | data formatting | bytes 4194304 | tf_op jit(solution)/shard_map/dot_general | solution.py:103
  156.1 9.7 %stack.619 = f32[2,4,1,64,320]{4,3,1,0,2:T(8,128)} concatenate(f32[2,4,1,1,320]{4,3,1,0,2:T(1,128)S(1)} %stack.684, f32[2,4,1,1,320]{4,3,1,0,2:T(1,128)S(1)} %stack.685, f32[2,4,1,1,320]{4,3,1,0,2:T(1,128)S(1)} %stack.686, f32[2,4,1,1,320]{4,3,1,0,2:T(1,128)S(1)} %stack.687, f32[2,4,1,1,320]{4,3,1,0,2:T(1,128)S(1)} %stack.688, f32[2,4,1,1,320]{4,3,1,0,2:T(1,128)S(1)} %stack.689, ...), dimensions={3} | concatenate | bytes 1310720 | tf_op jit(solution)/shard_map/stack | solution.py:38
  165.8 1.8 all-reduce.2.cloned.1.call-done
  167.6 1.9 fusion.8
  169.8 4.4 %collective-permute-start.1 = (bf16[256,2048]{1,0:T(8,128)(2,1)S(1)}, bf16[256,2048]{1,0:T(8,128)(2,1)}, u32[]{:S(2)}, u32[]{:S(2)}) collective-permute-start(bf16[256,2048]{1,0:T(8,128)(2,1)S(1)} %fusion.10), channel_id=1, source_target_pairs={{0,4},{4,8},{8,12},{12,16},{16,20},{20,24},{24,28},{1,5},{5,9},{9,... | collective-permute-start | bytes 3145736 | tf_op jit(solution)/shard_map/ppermute | solution.py:20
  177.2 1.5 convolution_convert_fusion.2
  178.7 16.3 %collective-permute-done.1 = bf16[256,2048]{1,0:T(8,128)(2,1)} collective-permute-done((bf16[256,2048]{1,0:T(8,128)(2,1)S(1)}, bf16[256,2048]{1,0:T(8,128)(2,1)}, u32[]{:S(2)}, u32[]{:S(2)}) %collective-permute-start.1) | collective-permute-done | bytes 1048608 | tf_op jit(solution)/shard_map/ppermute | solution.py:20
  195.0 1.7 convolution_convert_fusion.3
  198.5 1.7 multiply_reduce_fusion.3
  201.2 3.6 %fusion.146 = (f32[2,4,4,64]{3,1,2,0:T(4,128)S(1)}, f32[2,4,4,64,320]{4,3,1,2,0:T(8,128)}) fusion(f32[2,4,64,320]{3,2,1,0:T(8,128)S(1)} %bitcast.186, pred[4,320]{1,0:T(4,128)(4,1)} %add_compare_fusion, bf16[4,64,2,4,64]{1,0,4,3,2:T(4,128)(2,1)S(1)} %copy-done.4, bf16[1,320,2,64]{1,3,0,2:T(8,128)(2,1)S(1)} %bitcast.194, ...), kind=kOutput, calls=%fused_computation.203 | convolution fusion | flops 88473920 | bytes 3876096 | tf_op jit(solution)/shard_map/while/body/eval_jaxpr/sub | solution.py:85
  204.8 3.1 %fusion.37 = bf16[4,64,2,4,64]{1,4,3,2,0:T(8,128)(2,1)S(1)} fusion(bf16[1,320,2,64]{1,3,2,0:T(8,128)(2,1)S(1)} %bitcast.200, bf16[1,320,2,64]{1,3,2,0:T(8,128)(2,1)S(1)} %bitcast.201, bf16[1,320,2,64]{1,3,2,0:T(8,128)(2,1)S(1)} %bitcast.203, bf16[1,320,2,64]{1,3,2,0:T(8,128)(2,1)S(1)} %bitcast.206, f32[2,4,4,64,320]{4,3,1,2,0:T(8,128)} %get-tuple-element.234, ...), kind=kOutput, calls=%fused_computation.46 | convolution fusion | flops 86638592 | bytes 3219456 | tf_op jit(solution)/shard_map/while/body/eval_jaxpr/kgnqj,njkd->nqkgd/dot_general | solution.py:87
  208.5 3.3 %convolution_convert_fusion = bf16[256,2048]{1,0:T(8,128)(2,1)} fusion(bf16[256,512]{1,0:T(8,128)(2,1)S(1)} %reshape.447, bf16[2,512,2048]{2,1,0:T(8,128)(2,1)} %param.14), kind=kOutput, calls=%fused_computation.15 | convolution fusion | flops 537395200 | bytes 3407872 | tf_op jit(solution)/shard_map/dot_general | solution.py:119
  211.9 26.9 %reduce-scatter.2.cloned.1.call-done = bf16[256,512]{1,0:T(8,128)(2,1)} async-done(((bf16[256,2048]{1,0:T(8,128)(2,1)}), bf16[256,512]{1,0:T(8,128)(2,1)}) %reduce-scatter.2.cloned.1.call-update) | async-done | bytes 262160 | tf_op jit(solution)/shard_map/reduce_scatter | solution.py:124
  238.8 1.7 add_convert_fusion
  (289 shorter events, 99.7 us)
Async XLA Ops:
  6.5 11.3 %copy-start.53 = (f32[2,8,257]{2,1,0:T(8,128)S(1)}, f32[2,8,257]{2,1,0:T(8,128)}, u32[]{:S(2)}) copy-start(f32[2,8,257]{2,1,0:T(8,128)} %param.17) | copy-start | bytes 49348
  6.5 161.0 %all-reduce.2.cloned.1.call-start = ((), (), s32[]{:S(2)}) async-start(), calls=%async_computation.1 | async-start | bytes 2097152 | tf_op jit(solution)/shard_map/psum | solution.py:121
  12.0 96.6 %collective-permute-start = (bf16[256,2048]{1,0:T(8,128)(2,1)}, bf16[256,2048]{1,0:T(8,128)(2,1)}, u32[]{:S(2)}, u32[]{:S(2)}) collective-permute-start(bf16[256,2048]{1,0:T(8,128)(2,1)} %fusion.13), channel_id=1, source_target_pairs={{0,4},{4,8},{8,12},{12,16},{16,20},{20,24},{24,28},{1,5},{5,9},{9,... | collective-permute-start | bytes 3145736 | tf_op jit(solution)/shard_map/ppermute | solution.py:20
  29.0 4.7 %copy-start.2 = (bf16[2,2048,128]{2,1,0:T(8,128)(2,1)S(1)}, bf16[2,2048,128]{2,1,0:T(8,128)(2,1)}, u32[]{:S(2)}) copy-start(bf16[2,2048,128]{2,1,0:T(8,128)(2,1)} %param.12) | copy-start | bytes 3145732
  34.8 36.1 %copy-start.30 = (f32[8,320]{1,0:T(8,128)S(1)}, f32[8,320]{1,0:T(8,128)}, u32[]{:S(2)}) copy-start(f32[8,320]{1,0:T(8,128)} %get-tuple-element.122) | copy-start | bytes 30724
  34.8 36.8 %copy-start.28 = (f32[8,320]{1,0:T(8,128)S(1)}, f32[8,320]{1,0:T(8,128)}, u32[]{:S(2)}) copy-start(f32[8,320]{1,0:T(8,128)} %get-tuple-element.121) | copy-start | bytes 30724
  34.8 37.4 %copy-start.26 = (f32[8,320]{1,0:T(8,128)S(1)}, f32[8,320]{1,0:T(8,128)}, u32[]{:S(2)}) copy-start(f32[8,320]{1,0:T(8,128)} %get-tuple-element.120) | copy-start | bytes 30724
  34.8 38.0 %copy-start.24 = (f32[8,320]{1,0:T(8,128)S(1)}, f32[8,320]{1,0:T(8,128)}, u32[]{:S(2)}) copy-start(f32[8,320]{1,0:T(8,128)} %get-tuple-element.119) | copy-start | bytes 30724
  34.8 38.6 %copy-start.22 = (f32[8,320]{1,0:T(8,128)S(1)}, f32[8,320]{1,0:T(8,128)}, u32[]{:S(2)}) copy-start(f32[8,320]{1,0:T(8,128)} %get-tuple-element.118) | copy-start | bytes 30724
  34.8 39.2 %copy-start.21 = (f32[8,320]{1,0:T(8,128)S(1)}, f32[8,320]{1,0:T(8,128)}, u32[]{:S(2)}) copy-start(f32[8,320]{1,0:T(8,128)} %get-tuple-element.117) | copy-start | bytes 30724
  34.9 39.8 %copy-start.20 = (f32[8,320]{1,0:T(8,128)S(1)}, f32[8,320]{1,0:T(8,128)}, u32[]{:S(2)}) copy-start(f32[8,320]{1,0:T(8,128)} %get-tuple-element.116) | copy-start | bytes 30724
  34.9 40.4 %copy-start.19 = (f32[8,320]{1,0:T(8,128)S(1)}, f32[8,320]{1,0:T(8,128)}, u32[]{:S(2)}) copy-start(f32[8,320]{1,0:T(8,128)} %get-tuple-element.115) | copy-start | bytes 30724
  34.9 41.0 %copy-start.18 = (f32[8,320]{1,0:T(8,128)S(1)}, f32[8,320]{1,0:T(8,128)}, u32[]{:S(2)}) copy-start(f32[8,320]{1,0:T(8,128)} %get-tuple-element.114) | copy-start | bytes 30724
  34.9 41.6 %copy-start.17 = (f32[8,320]{1,0:T(8,128)S(1)}, f32[8,320]{1,0:T(8,128)}, u32[]{:S(2)}) copy-start(f32[8,320]{1,0:T(8,128)} %get-tuple-element.113) | copy-start | bytes 30724
  34.9 42.2 %copy-start.16 = (f32[8,320]{1,0:T(8,128)S(1)}, f32[8,320]{1,0:T(8,128)}, u32[]{:S(2)}) copy-start(f32[8,320]{1,0:T(8,128)} %get-tuple-element.112) | copy-start | bytes 30724
  34.9 42.8 %copy-start.15 = (f32[8,320]{1,0:T(8,128)S(1)}, f32[8,320]{1,0:T(8,128)}, u32[]{:S(2)}) copy-start(f32[8,320]{1,0:T(8,128)} %get-tuple-element.111) | copy-start | bytes 30724
  34.9 43.4 %copy-start.14 = (f32[8,320]{1,0:T(8,128)S(1)}, f32[8,320]{1,0:T(8,128)}, u32[]{:S(2)}) copy-start(f32[8,320]{1,0:T(8,128)} %get-tuple-element.110) | copy-start | bytes 30724
  34.9 44.0 %copy-start.13 = (f32[8,320]{1,0:T(8,128)S(1)}, f32[8,320]{1,0:T(8,128)}, u32[]{:S(2)}) copy-start(f32[8,320]{1,0:T(8,128)} %get-tuple-element.109) | copy-start | bytes 30724
  34.9 44.6 %copy-start.12 = (f32[8,320]{1,0:T(8,128)S(1)}, f32[8,320]{1,0:T(8,128)}, u32[]{:S(2)}) copy-start(f32[8,320]{1,0:T(8,128)} %get-tuple-element.108) | copy-start | bytes 30724
  34.9 45.2 %copy-start.11 = (f32[8,320]{1,0:T(8,128)S(1)}, f32[8,320]{1,0:T(8,128)}, u32[]{:S(2)}) copy-start(f32[8,320]{1,0:T(8,128)} %get-tuple-element.107) | copy-start | bytes 30724
  35.0 45.8 %copy-start.10 = (f32[8,320]{1,0:T(8,128)S(1)}, f32[8,320]{1,0:T(8,128)}, u32[]{:S(2)}) copy-start(f32[8,320]{1,0:T(8,128)} %get-tuple-element.106) | copy-start | bytes 30724
  35.0 46.4 %copy-start.9 = (f32[8,320]{1,0:T(8,128)S(1)}, f32[8,320]{1,0:T(8,128)}, u32[]{:S(2)}) copy-start(f32[8,320]{1,0:T(8,128)} %get-tuple-element.105) | copy-start | bytes 30724
  108.5 10.8 %copy-start.47 = (f32[256,2]{0,1:T(2,128)S(1)}, f32[256,2]{0,1:T(2,128)}, u32[]{:S(2)}) copy-start(f32[256,2]{0,1:T(2,128)} %add_rsqrt_fusion.4) | copy-start | bytes 6148
  131.8 107.0 %reduce-scatter.2.cloned.1.call-start = ((), (), s32[]{:S(2)}) async-start(), calls=%async_computation.2 | async-start | bytes 1310720 | tf_op jit(solution)/shard_map/reduce_scatter | solution.py:124
  154.7 12.8 %copy-start = (bf16[256,2048]{1,0:T(8,128)(2,1)S(1)}, bf16[256,2048]{1,0:T(8,128)(2,1)}, u32[]{:S(2)}) copy-start(bf16[256,2048]{1,0:T(8,128)(2,1)} %param.9) | copy-start | bytes 3145732
  156.1 13.4 %copy-start.46 = (f32[1,2048]{1,0:T(1,128)S(1)}, f32[1,2048]{1,0:T(1,128)}, u32[]{:S(2)}) copy-start(f32[1,2048]{1,0:T(1,128)} %get-tuple-element.81) | copy-start | bytes 24580
  167.6 6.6 %copy-start.1 = (bf16[512,2048]{1,0:T(8,128)(2,1)S(1)}, bf16[512,2048]{1,0:T(8,128)(2,1)}, u32[]{:S(2)}) copy-start(bf16[512,2048]{1,0:T(8,128)(2,1)} %copy.232) | copy-start | bytes 6291460
  169.8 5.2 %copy-start.49 = (f32[64]{0:T(128)S(1)}, f32[64]{0:T(128)}, u32[]{:S(2)}) copy-start(f32[64]{0:T(128)} %get-tuple-element.213) | copy-start | bytes 772
  169.8 25.2 %collective-permute-start.1 = (bf16[256,2048]{1,0:T(8,128)(2,1)S(1)}, bf16[256,2048]{1,0:T(8,128)(2,1)}, u32[]{:S(2)}, u32[]{:S(2)}) collective-permute-start(bf16[256,2048]{1,0:T(8,128)(2,1)S(1)} %fusion.10), channel_id=1, source_target_pairs={{0,4},{4,8},{8,12},{12,16},{16,20},{20,24},{24,28},{1,5},{5,9},{9,... | collective-permute-start | bytes 3145736 | tf_op jit(solution)/shard_map/ppermute | solution.py:20
  176.1 18.9 %copy-start.52 = (bf16[2,2048,128]{2,1,0:T(8,128)(2,1)S(1)}, bf16[2,2048,128]{2,1,0:T(8,128)(2,1)}, u32[]{:S(2)}) copy-start(bf16[2,2048,128]{2,1,0:T(8,128)(2,1)} %param.13) | copy-start | bytes 3145732
  196.7 4.5 %copy-start.3 = (f32[2,4,1,64,320]{4,3,1,0,2:T(8,128)S(1)}, f32[2,4,1,64,320]{4,3,1,0,2:T(8,128)}, u32[]{:S(2)}) copy-start(f32[2,4,1,64,320]{4,3,1,0,2:T(8,128)} %stack.619) | copy-start | bytes 1966084
  196.7 4.5 %copy-start.4 = (bf16[4,64,2,4,64]{1,0,4,3,2:T(4,128)(2,1)S(1)}, bf16[4,64,2,4,64]{1,0,4,3,2:T(4,128)(2,1)}, u32[]{:S(2)}) copy-start(bf16[4,64,2,4,64]{1,0,4,3,2:T(4,128)(2,1)} %reshape_reshape.9) | copy-start | bytes 786436
  (26 other events, 107.4 us)
Sparse Core Ops, SparseCore 0:
  131.9 35.6 all-reduce.1
  212.0 26.7 reduce-scatter.1
where the time goes:
time: 251 us; the launch traced here: 247 us
  local copies, waits for them, and re-layouts  125 us (50%)
  waiting for transfers between devices  45 us (18%)
  matrix products  38.5 us (15%)
  between operations  14.4 us (6%)
  other arithmetic  14.2 us (6%)
  starting transfers between devices  10.5 us (4%)
    another operation x130, local copies, waits for them, and re-layouts, segment_bias(): return jnp.stack(rows, axis=1)  93.1 us
    reduce_scatter x1, waiting for transfers between devices, local(): lax.psum_scatter(partial_value.astype(jnp.bfloat16), 'tp', scatter_dimens...  26.9 us
    ppermute x2, waiting for transfers between devices, passed_along(): lax.ppermute(value, axis, [(source, source + steps) for source in range(i...  16.3 us
    dot_general x3, local copies, waits for them, and re-layouts, local(): jnp.dot(normed, w_query[layer_index], preferred_element_type=jnp.float32)  10.3 us
    ppermute x2, starting transfers between devices, passed_along(): lax.ppermute(value, axis, [(source, source + steps) for source in range(i...  10.3 us
    slice x8, local copies, waits for them, and re-layouts, one_block(): value_rows[q * SEG:q * SEG + span]  8.32 us
    sub x2, matrix products, one_block(): expon = jnp.exp(scores - peak)  7.66 us
    dot_general x2, matrix products, local(): jnp.dot(mixed, w_out[layer_index], preferred_element_type=jnp.float32)  6.73 us
  transfers between devices with their start and end apart: 4, of which 3 were waited for; matrix products, arithmetic and copies ran while one was open for 52% of the time, Pallas kernels for 0%

commit v1 on v0

v1 whole, which is shorter than its diff:
```python
import functools

import jax
import jax.numpy as jnp
from jax import lax
from jax.experimental import pallas as pl
from jax.experimental.pallas import tpu as pltpu
from jax.sharding import PartitionSpec as P

HEAD_DIM = 64
SEG = 64
LEFT = 4
CLIP = 128
LAYERS = 2

REACH = LEFT * SEG
CHUNK = 2 * SEG
WINDOW = REACH + CHUNK
LINE = WINDOW + CHUNK
LANES = 128

norm_eps = 1e-06
masked_score = -1e30

bf16 = jnp.bfloat16
f32 = jnp.float32

whole = pl.BlockSpec(memory_space=pltpu.VMEM)
scalar = pl.BlockSpec(memory_space=pltpu.SMEM)
anywhere = pl.BlockSpec(memory_space=pl.ANY)


def params():
    return pltpu.CompilerParams(vmem_limit_bytes=24 * 1024 * 1024)


def fetch(source_ref, target_ref, sems, layer_index):
    share = target_ref.shape[0] // sems.shape[0]
    copies = []
    for index in range(sems.shape[0]):
        at = pl.ds(index * share, share)
        copy = pltpu.make_async_copy(
            source_ref.at[layer_index, at, :], target_ref.at[at, :], sems.at[index]
        )
        copy.start()
        copies.append(copy)
    return copies


def cost(flops, moved):
    return pl.CostEstimate(flops=int(flops), bytes_accessed=int(moved), transcendentals=0)


def head_norm(flat, gain_row):
    width = flat.shape[1]
    step = min(width, LANES)
    row = lax.broadcasted_iota(jnp.int32, (step, step), 0) // HEAD_DIM
    col = lax.broadcasted_iota(jnp.int32, (step, step), 1) // HEAD_DIM
    mean_of = jnp.where(row == col, 1.0 / HEAD_DIM, 0.0).astype(bf16)
    gain = jnp.concatenate([gain_row] * (step // HEAD_DIM), axis=1)
    pieces = []
    for lower in range(0, width, step):
        part = flat[:, lower : lower + step]
        squared = part * part
        high = squared.astype(bf16)
        low = (squared - high.astype(f32)).astype(bf16)
        mean = jnp.dot(high, mean_of, preferred_element_type=f32) + jnp.dot(
            low, mean_of, preferred_element_type=f32
        )
        pieces.append(part * lax.rsqrt(mean + norm_eps) * gain)
    return pieces


def key_value_body(normed, wk_ref, wv_ref, key_gain_ref, layer_index, kv_ref, copies):
    for copy in copies:
        copy.wait()
    keys = jnp.dot(normed, wk_ref[...], preferred_element_type=f32)
    values = jnp.dot(normed, wv_ref[...], preferred_element_type=f32)
    keys = head_norm(keys, key_gain_ref[layer_index : layer_index + 1, :])[0]
    kv_ref[...] = jnp.concatenate([keys, values], axis=1).astype(bf16)


def first_norm_kernel(
    layer_index, x_ref, gain_ref, wk_any, wv_any, kg_ref, normed_ref, kv_ref,
    wk_ref, wv_ref, sems,
):
    copies = fetch(wk_any, wk_ref, sems.at[0:1], layer_index)
    copies += fetch(wv_any, wv_ref, sems.at[1:2], layer_index)
    current = x_ref[...].astype(f32)
    mean = jnp.mean(current * current, axis=-1, keepdims=True)
    gain = gain_ref[layer_index : layer_index + 1, :]
    normed_ref[...] = (current * lax.rsqrt(mean + norm_eps) * gain).astype(bf16)
    key_value_body(normed_ref[...], wk_ref, wv_ref, kg_ref, layer_index, kv_ref, copies)


def next_norm_kernel(
    layer_index, block, place_ref, mine_ref, other_ref, gain_ref, wk_any, wv_any, kg_ref,
    normed_ref, kv_ref, wk_ref, wv_ref, sems,
):
    copies = fetch(wk_any, wk_ref, sems.at[0:1], layer_index)
    copies += fetch(wv_any, wv_ref, sems.at[1:2], layer_index)
    parity = place_ref[1]
    mine = mine_ref[...].astype(f32)
    other = other_ref[...].astype(f32)
    total = jnp.sum(mine * mine, axis=-1, keepdims=True)
    total = total + jnp.sum(other * other, axis=-1, keepdims=True)
    scale = lax.rsqrt(total / (2 * mine.shape[1]) + norm_eps)
    for index in range(mine.shape[1] // block):
        for held, side in ((mine, parity), (other, 1 - parity)):
            cols = pl.ds(pl.multiple_of((2 * index + side) * block, LANES), block)
            piece = held[:, index * block : (index + 1) * block]
            gain = gain_ref[layer_index : layer_index + 1, cols]
            normed_ref[:, cols] = (piece * scale * gain).astype(bf16)
    key_value_body(normed_ref[...], wk_ref, wv_ref, kg_ref, layer_index, kv_ref, copies)


def query_kernel(layer_index, normed_ref, wq_any, qg_ref, q_ref, wq_ref, sems):
    copies = fetch(wq_any, wq_ref, sems, layer_index)
    share = wq_ref.shape[0] // len(copies)
    flat = None
    for index, copy in enumerate(copies):
        copy.wait()
        at = slice(index * share, (index + 1) * share)
        part = jnp.dot(normed_ref[:, at], wq_ref[at, :], preferred_element_type=f32)
        flat = part if flat is None else flat + part
    pieces = head_norm(flat, qg_ref[layer_index : layer_index + 1, :])
    width = pieces[0].shape[1]
    for index, piece in enumerate(pieces):
        scaled = piece.astype(bf16) * bf16(HEAD_DIM**-0.5)
        q_ref[:, index * width : (index + 1) * width] = scaled


def bias_kernel(table_ref, tile_ref):
    layers, heads, entries = table_ref.shape
    source = lax.broadcasted_iota(jnp.int32, (entries, LINE), 0)
    offset = lax.broadcasted_iota(jnp.int32, (entries, LINE), 1)
    distance = jnp.clip(WINDOW - 1 - offset, -CLIP, CLIP) + CLIP
    onehot = (source == distance).astype(f32)
    query_seg = lax.broadcasted_iota(jnp.int32, (CHUNK, WINDOW), 0) // SEG
    key_seg = lax.broadcasted_iota(jnp.int32, (CHUNK, WINDOW), 1) // SEG
    inside = (key_seg >= query_seg) & (key_seg <= query_seg + LEFT)
    for layer_index in range(layers):
        line = jnp.dot(
            table_ref[layer_index], onehot, precision=lax.Precision.HIGHEST,
            preferred_element_type=f32,
        )
        for head in range(heads):
            spread = jnp.broadcast_to(line[head : head + 1, :], (CHUNK, LINE))
            rolled = pltpu.roll(spread, LINE - CHUNK + 1, 1, stride=1, stride_axis=0)
            tile_ref[layer_index, head] = jnp.where(inside, rolled[:, :WINDOW], masked_score)


def attention_kernel(
    block, layer_index, place_ref, q_ref, kv_ref, kvp_ref, tile_any, wout_any, keep_ref, send_ref,
    keys_ref, even_ref, odd_ref, mixed_ref, tile_ref, wout_ref, sems,
):
    tile_copy = pltpu.make_async_copy(tile_any.at[layer_index], tile_ref, sems.at[0])
    tile_copy.start()
    copies = fetch(wout_any, wout_ref, sems.at[1:2], layer_index)
    first, parity = place_ref[0], place_ref[1]
    rows = q_ref.shape[0]
    heads = q_ref.shape[1] // HEAD_DIM
    kv_width = kv_ref.shape[1] // 2
    kv_heads = kv_width // HEAD_DIM
    group = heads // kv_heads
    pairs = group // 2

    for part_ref, start in ((kvp_ref, 0), (kv_ref, REACH)):
        count = part_ref.shape[0]
        low = lax.broadcasted_iota(jnp.int32, (count, LANES), 1) < HEAD_DIM
        for kv in range(kv_heads):
            at = kv * HEAD_DIM
            key = part_ref[:, at : at + HEAD_DIM].astype(f32)
            value = part_ref[:, kv_width + at : kv_width + at + HEAD_DIM].astype(f32)
            key = jnp.concatenate([key, key], axis=1)
            value = jnp.concatenate([value, value], axis=1)
            keys_ref[kv, start : start + count, :] = key.astype(bf16)
            even_ref[kv, start : start + count, :] = jnp.where(low, value, 1.0).astype(bf16)
            odd_ref[kv, start : start + count, :] = jnp.where(low, 1.0, value).astype(bf16)

    tile_copy.wait()
    low = lax.broadcasted_iota(jnp.int32, (CHUNK, LANES), 1) < HEAD_DIM
    for chunk in range(rows // CHUNK):
        start = chunk * CHUNK
        key_index = start + lax.broadcasted_iota(jnp.int32, (1, WINDOW), 1)
        outside = (key_index < REACH) & (first == 1)
        outside = jnp.where(outside, masked_score, 0.0)
        for kv in range(kv_heads):
            evens, odds = [], []
            for pair in range(pairs):
                at = (kv * pairs + pair) * LANES
                both = q_ref[start : start + CHUNK, at : at + LANES]
                evens.append(jnp.where(low, both, jnp.zeros_like(both)))
                odds.append(jnp.where(low, jnp.zeros_like(both), both))
            stacked = jnp.concatenate(evens + odds, axis=0)
            window = slice(start, start + WINDOW)
            scores = lax.dot_general(
                stacked, keys_ref[kv, window, :], (((1,), (1,)), ((), ())),
                preferred_element_type=f32,
            )
            expons = []
            for index in range(group):
                pair, side = index % pairs, index // pairs
                head = kv * group + 2 * pair + side
                score = scores[index * CHUNK : (index + 1) * CHUNK, :] + tile_ref[head]
                score = score + outside
                peak = jnp.max(score, axis=-1, keepdims=True)
                expons.append(jnp.exp(score - peak).astype(bf16))
            even = jnp.dot(
                jnp.concatenate(expons[:pairs], axis=0), even_ref[kv, window, :],
                preferred_element_type=f32,
            )
            odd = jnp.dot(
                jnp.concatenate(expons[pairs:], axis=0), odd_ref[kv, window, :],
                preferred_element_type=f32,
            )
            for pair in range(pairs):
                at = (kv * pairs + pair) * LANES
                upper = even[pair * CHUNK : (pair + 1) * CHUNK, :]
                lower = odd[pair * CHUNK : (pair + 1) * CHUNK, :]
                total = pltpu.roll(jnp.where(low, lower, upper), HEAD_DIM, 1)
                mixed_ref[start : start + CHUNK, at : at + LANES] = (
                    jnp.where(low, upper, lower) / total
                ).astype(bf16)

    mixed = mixed_ref[...]
    for copy in copies:
        copy.wait()
    for index in range(keep_ref.shape[1] // block):
        for target, side in ((send_ref, 1 - parity), (keep_ref, parity)):
            cols = pl.ds(pl.multiple_of((2 * index + side) * block, LANES), block)
            partial_value = jnp.dot(mixed, wout_ref[:, cols], preferred_element_type=f32)
            target[:, index * block : (index + 1) * block] = partial_value.astype(bf16)


def add_kernel(a_ref, b_ref, out_ref):
    out_ref[...] = (a_ref[...].astype(f32) + b_ref[...].astype(f32)).astype(bf16)


def split_add_kernel(block, bit, place_ref, a_ref, b_ref, keep_ref, send_ref):
    parity = place_ref[bit]
    for index in range(keep_ref.shape[1] // block):
        into = slice(index * block, (index + 1) * block)
        for target, side in ((send_ref, 1 - parity), (keep_ref, parity)):
            cols = pl.ds(pl.multiple_of((2 * index + side) * block, LANES), block)
            target[:, into] = (
                a_ref[:, cols].astype(f32) + b_ref[:, cols].astype(f32)
            ).astype(bf16)


def residual_kernel(block, stride, bit, place_ref, x_ref, a_ref, b_ref, out_ref):
    for index in range(out_ref.shape[1] // block):
        into = slice(index * block, (index + 1) * block)
        cols = pl.ds(pl.multiple_of((stride * index + place_ref[bit]) * block, LANES), block)
        added = a_ref[:, into].astype(f32) + b_ref[:, into].astype(f32)
        out_ref[:, into] = (x_ref[:, cols].astype(f32) + added).astype(bf16)


def swapped(value, bit):
    size = lax.axis_size("tp")
    return lax.ppermute(value, "tp", [(d, d ^ (1 << bit)) for d in range(size)])


def local(stream, attn_gain, w_query, w_key, w_value, w_out, query_gain, key_gain, rel_bias):
    rows, width = stream.shape
    tp_size = lax.axis_size("tp")
    sp_size = lax.axis_size("sp")
    bits = tp_size.bit_length() - 1
    block = width // tp_size
    half = width // 2
    query_width = w_query.shape[2]
    kv_width = w_key.shape[2]
    heads = query_width // HEAD_DIM
    kv_heads = kv_width // HEAD_DIM
    tp_index = lax.axis_index("tp")
    sp_index = lax.axis_index("sp")
    place = jnp.stack(
        [(sp_index == 0).astype(jnp.int32), tp_index % 2]
        + [(tp_index >> bit) & 1 for bit in range(1, bits)]
        + [tp_index // 2]
    ).astype(jnp.int32)

    def out(shape, dtype=bf16):
        return jax.ShapeDtypeStruct(shape, dtype)

    tiles = pl.pallas_call(
        bias_kernel,
        out_shape=out((LAYERS, heads, CHUNK, WINDOW), f32),
        in_specs=[whole],
        out_specs=whole,
        compiler_params=params(),
        cost_estimate=cost(2e9, 1e6),
        name="bias_tiles",
    )(rel_bias)

    mine = other = None
    for layer_index in range(LAYERS):
        weights = (attn_gain, w_key, w_value, key_gain)
        weight_specs = [whole, anywhere, anywhere, whole]
        weight_scratch = [
            pltpu.VMEM((width, kv_width), bf16),
            pltpu.VMEM((width, kv_width), bf16),
            pltpu.SemaphoreType.DMA((2,)),
        ]
        norm_out = [out((rows, width)), out((rows, 2 * kv_width))]
        norm_cost = cost(4 * rows * width * kv_width, 4 * rows * width + 4 * width * kv_width)
        if layer_index == 0:
            normed, kv = pl.pallas_call(
                functools.partial(first_norm_kernel, layer_index),
                out_shape=norm_out,
                in_specs=[whole] + weight_specs,
                out_specs=[whole, whole],
                scratch_shapes=weight_scratch,
                compiler_params=params(),
                cost_estimate=norm_cost,
                name="norm_kv_first",
            )(stream, *weights)
        else:
            normed, kv = pl.pallas_call(
                functools.partial(next_norm_kernel, layer_index, block),
                out_shape=norm_out,
                in_specs=[scalar, whole, whole] + weight_specs,
                out_specs=[whole, whole],
                scratch_shapes=weight_scratch,
                compiler_params=params(),
                cost_estimate=norm_cost,
                name="norm_kv_next",
            )(place, mine, other, *weights)
        kv_prior = lax.ppermute(
            kv[rows - REACH :], "sp", [(d, d + 1) for d in range(sp_size - 1)]
        )
        queries = pl.pallas_call(
            functools.partial(query_kernel, layer_index),
            out_shape=out((rows, query_width)),
            in_specs=[whole, anywhere, whole],
            out_specs=whole,
            scratch_shapes=[
                pltpu.VMEM((width, query_width), bf16),
                pltpu.SemaphoreType.DMA((4,)),
            ],
            compiler_params=params(),
            cost_estimate=cost(2 * rows * width * query_width, 2 * width * query_width),
            name="queries",
        )(normed, w_query, query_gain)
        keep, send = pl.pallas_call(
            functools.partial(attention_kernel, block, layer_index),
            out_shape=[out((rows, half)), out((rows, half))],
            in_specs=[scalar, whole, whole, whole, anywhere, anywhere],
            out_specs=[whole, whole],
            scratch_shapes=[
                pltpu.VMEM((kv_heads, REACH + rows, LANES), bf16),
                pltpu.VMEM((kv_heads, REACH + rows, LANES), bf16),
                pltpu.VMEM((kv_heads, REACH + rows, LANES), bf16),
                pltpu.VMEM((rows, query_width), bf16),
                pltpu.VMEM((heads, CHUNK, WINDOW), f32),
                pltpu.VMEM((query_width, width), bf16),
                pltpu.SemaphoreType.DMA((2,)),
            ],
            compiler_params=params(),
            cost_estimate=cost(
                2 * rows * query_width * (width + 4 * WINDOW), 2 * width * query_width
            ),
            name="attention",
        )(place, queries, kv, kv_prior, tiles, w_out)
        received = swapped(send, 0)
        if layer_index < LAYERS - 1:
            for bit in range(1, bits):
                summed = pl.pallas_call(
                    add_kernel,
                    out_shape=out((rows, half)),
                    in_specs=[whole, whole],
                    out_specs=whole,
                    compiler_params=params(),
                    name="add",
                )(keep, received)
                keep, received = summed, swapped(summed, bit)
            mine = pl.pallas_call(
                functools.partial(residual_kernel, block, 2, 1),
                out_shape=out((rows, half)),
                in_specs=[scalar, whole, whole, whole],
                out_specs=whole,
                compiler_params=params(),
                name="residual",
            )(place, stream, keep, received)
            other = swapped(mine, 0)
        else:
            for bit in range(1, bits):
                left = keep.shape[1] // 2
                keep, send = pl.pallas_call(
                    functools.partial(split_add_kernel, block, 1 + bit),
                    out_shape=[out((rows, left)), out((rows, left))],
                    in_specs=[scalar, whole, whole],
                    out_specs=[whole, whole],
                    compiler_params=params(),
                    name="split_add",
                )(place, keep, received)
                received = swapped(send, bit)
            result = pl.pallas_call(
                functools.partial(residual_kernel, block, 1, bits + 1),
                out_shape=out((rows, block)),
                in_specs=[scalar, whole, whole, whole],
                out_specs=whole,
                compiler_params=params(),
                name="result",
            )(place, mine, keep, received)
    return result


def solution(mesh):
    return jax.shard_map(
        local,
        mesh=mesh,
        in_specs=(
            P("sp", None),
            P(),
            P(None, None, "tp"),
            P(None, None, "tp"),
            P(None, None, "tp"),
            P(None, "tp", None),
            P(),
            P(),
            P(None, "tp", None),
        ),
        out_specs=P("sp", "tp"),
        check_vma=False,
    )
```

time: 251 us -> 66.4 us (0.26)
  the two profiles are of different devices: /device:TPU:0 before, /device:TPU:26 now
where the time goes in v1:
time: 66.4 us; the launch traced here: 66 us
  waiting for transfers between devices  32.5 us (49%)
  Pallas kernels  17.5 us (26%)
  local copies, waits for them, and re-layouts  8.03 us (12%)
  starting transfers between devices  7.63 us (11%)
    ppermute x5, waiting for transfers between devices, swapped(): return lax.ppermute(value, 'tp', [(d, d ^ 1 << bit) for d in range(size)])  26.9 us
    unnamed x32, local copies, waits for them, and re-layouts  8.03 us
    pallas_call x2, Pallas kernels, local(): pl.pallas_call(functools.partial(attention_kernel, block, layer_index), o...  7.45 us
    ppermute x2, starting transfers between devices, local(): lax.ppermute(kv[rows - REACH:], 'sp', [(d, d + 1) for d in range(sp_size...  6.22 us
    ppermute x2, waiting for transfers between devices, local(): lax.ppermute(kv[rows - REACH:], 'sp', [(d, d + 1) for d in range(sp_size...  5.58 us
    pallas_call x2, Pallas kernels, local(): pl.pallas_call(functools.partial(query_kernel, layer_index), out_shape=ou...  2.65 us
    pallas_call x1, Pallas kernels, local(): pl.pallas_call(functools.partial(next_norm_kernel, layer_index, block), o...  1.89 us
    ppermute x5, starting transfers between devices, swapped(): return lax.ppermute(value, 'tp', [(d, d ^ 1 << bit) for d in range(size)])  1.42 us
  transfers between devices with their start and end apart: 7, of which 7 were waited for; matrix products, arithmetic and copies ran while one was open for 0% of the time, Pallas kernels for 6%

profile of v1, /device:TPU:26, one launch (start us, length us, event | category | flops | bytes accessed | tf_op | source)
XLA Modules:
  0.0 66.0 jit_solution(17153357459607031561)
XLA Ops:
  0.0 1.2 %copy-done.4 = bf16[256,2048]{1,0:T(8,128)(2,1)S(1)} copy-done((bf16[256,2048]{1,0:T(8,128)(2,1)S(1)}, bf16[256,2048]{1,0:T(8,128)(2,1)}, u32[]{:S(2)}) %copy-start.4) | copy-done | bytes 1048600
  1.2 1.2 %copy-done.6 = bf16[2,2048,128]{2,1,0:T(8,128)(2,1)S(1)} copy-done((bf16[2,2048,128]{2,1,0:T(8,128)(2,1)S(1)}, bf16[2,2048,128]{2,1,0:T(8,128)(2,1)}, u32[]{:S(2)}) %copy-start.6) | copy-done | bytes 1048600
  2.5 1.2 %copy-done.8 = bf16[2,2048,128]{2,1,0:T(8,128)(2,1)S(1)} copy-done((bf16[2,2048,128]{2,1,0:T(8,128)(2,1)S(1)}, bf16[2,2048,128]{2,1,0:T(8,128)(2,1)}, u32[]{:S(2)}) %copy-start.8) | copy-done | bytes 1048600
  3.7 0.7 %copy-done.10 = f32[2,2048]{1,0:T(2,128)S(1)} copy-done((f32[2,2048]{1,0:T(2,128)S(1)}, f32[2,2048]{1,0:T(2,128)}, u32[]{:S(2)}) %copy-start.10) | copy-done | bytes 16408
  4.4 0.7 %copy-done.12 = f32[2,64]{1,0:T(2,128)S(1)} copy-done((f32[2,64]{1,0:T(2,128)S(1)}, f32[2,64]{1,0:T(2,128)}, u32[]{:S(2)}) %copy-start.12) | copy-done | bytes 536
  5.1 1.3 %norm_kv_first.1 = (bf16[256,2048]{1,0:T(8,128)(2,1)S(1)}, bf16[256,256]{1,0:T(8,128)(2,1)S(1)}) custom-call(bf16[256,2048]{1,0:T(8,128)(2,1)S(1)} %copy-done.4, f32[2,2048]{1,0:T(2,128)S(1)} %copy-done.10, bf16[2,2048,128]{2,1,0:T(8,128)(2,1)S(1)} %copy-done.6, bf16[2,2048,128]{2,1,0:T(8,128)(2,1)S(1)} %copy-done.8, f32[2,64]{1,0:T(2,128)S(1)} %copy-done.12), custom_call_target="tpu_custom_call" | custom-call | flops 268435456 | bytes 3145728 | tf_op jit(solution)/shard_map/norm_kv_first/pallas_call | solution.py:308
  6.4 3.7 %collective-permute-start = (bf16[256,256]{1,0:T(8,128)(2,1)S(1)}, bf16[256,256]{1,0:T(8,128)(2,1)}, u32[]{:S(2)}, u32[]{:S(2)}) collective-permute-start(bf16[256,256]{1,0:T(8,128)(2,1)S(1)} %get-tuple-element.16.kv_ref), channel_id=1, source_target_pairs={{0,4},{4,8},{8,12},{12,16},{16,20},{20,24},{24,28},{1,5},{5,9},{9,... | collective-permute-start | bytes 393224 | tf_op jit(solution)/shard_map/ppermute | solution.py:329
  10.1 0.7 %copy-done.15 = f32[2,8,257]{2,1,0:T(8,128)S(1)} copy-done((f32[2,8,257]{2,1,0:T(8,128)S(1)}, f32[2,8,257]{2,1,0:T(8,128)}, u32[]{:S(2)}) %copy-start.15) | copy-done | bytes 16472
  10.8 1.4 %bias_tiles.1.tile_any = f32[2,8,128,384]{3,2,1,0:T(8,128)S(1)} custom-call(f32[2,8,257]{2,1,0:T(8,128)S(1)} %copy-done.15), custom_call_target="tpu_custom_call" | custom-call | flops 2000000000 | bytes 1000000 | tf_op jit(solution)/shard_map/bias_tiles/pallas_call | solution.py:286
  12.2 1.3 %queries.2.q_ref = bf16[256,512]{1,0:T(8,128)(2,1)S(1)} custom-call(bf16[256,2048]{1,0:T(8,128)(2,1)S(1)} %get-tuple-element.15.normed_ref, bf16[2,2048,512]{2,1,0:T(8,128)(2,1)S(1)} %copy-done, f32[2,64]{1,0:T(2,128)S(1)} %copy-done.14), custom_call_target="tpu_custom_call" | custom-call | flops 536870912 | bytes 2097152 | tf_op jit(solution)/shard_map/queries/pallas_call | solution.py:332
  13.6 0.1 pad_add_fusion.place_ref
  13.7 1.1 %collective-permute-done.kvp_ref = bf16[256,256]{1,0:T(8,128)(2,1)} collective-permute-done((bf16[256,256]{1,0:T(8,128)(2,1)S(1)}, bf16[256,256]{1,0:T(8,128)(2,1)}, u32[]{:S(2)}, u32[]{:S(2)}) %collective-permute-start) | collective-permute-done | bytes 131104 | tf_op jit(solution)/shard_map/ppermute | solution.py:329
  14.8 2.2 %copy-done.2 = bf16[2,512,2048]{2,1,0:T(8,128)(2,1)S(1)} copy-done((bf16[2,512,2048]{2,1,0:T(8,128)(2,1)S(1)}, bf16[2,512,2048]{2,1,0:T(8,128)(2,1)}, u32[]{:S(2)}) %copy-start.2) | copy-done | bytes 4194328
  17.0 4.0 %attention.2 = (bf16[256,1024]{1,0:T(8,128)(2,1)S(1)}, bf16[256,1024]{1,0:T(8,128)(2,1)S(1)}) custom-call(s32[4]{0:T(128)S(1)} %pad_add_fusion.place_ref, bf16[256,512]{1,0:T(8,128)(2,1)S(1)} %queries.2.q_ref, bf16[256,256]{1,0:T(8,128)(2,1)S(1)} %get-tuple-element.16.kv_ref, bf16[256,256]{1,0:T(8,128)(2,1)} %collective-permute-done.kvp_ref, ...), custom_call_target="tpu_custom_call" | custom-call | flops 939524096 | bytes 2097152 | tf_op jit(solution)/shard_map/attention/pallas_call | solution.py:345
  21.0 0.1 collective-permute-start.1
  21.1 1.9 %collective-permute-done.1.b_ref = bf16[256,1024]{1,0:T(8,128)(2,1)S(1)} collective-permute-done((bf16[256,1024]{1,0:T(8,128)(2,1)S(1)}, bf16[256,1024]{1,0:T(8,128)(2,1)S(1)}, u32[]{:S(2)}, u32[]{:S(2)}) %collective-permute-start.1) | collective-permute-done | bytes 524320 | tf_op jit(solution)/shard_map/ppermute | solution.py:261
  23.0 0.1 add.13.a_ref
  23.1 0.6 collective-permute-start.2
  23.7 13.4 %collective-permute-done.2.b_ref = bf16[256,1024]{1,0:T(8,128)(2,1)S(1)} collective-permute-done((bf16[256,1024]{1,0:T(8,128)(2,1)S(1)}, bf16[256,1024]{1,0:T(8,128)(2,1)S(1)}, u32[]{:S(2)}, u32[]{:S(2)}) %collective-permute-start.2) | collective-permute-done | bytes 524320 | tf_op jit(solution)/shard_map/ppermute | solution.py:261
  37.1 0.7 %residual.1.mine_ref.x_ref = bf16[256,1024]{1,0:T(8,128)(2,1)S(1)} custom-call(s32[4]{0:T(128)S(1)} %pad_add_fusion.place_ref, bf16[256,2048]{1,0:T(8,128)(2,1)S(1)} %copy-done.5, bf16[256,1024]{1,0:T(8,128)(2,1)S(1)} %add.13.a_ref, bf16[256,1024]{1,0:T(8,128)(2,1)S(1)} %collective-permute-done.2.b_ref), custom_call_target="tpu_custom_call" | custom-call | tf_op jit(solution)/shard_map/residual/pallas_call | solution.py:377
  37.9 0.1 collective-permute-start.3
  38.0 1.9 %collective-permute-done.3.other_ref = bf16[256,1024]{1,0:T(8,128)(2,1)S(1)} collective-permute-done((bf16[256,1024]{1,0:T(8,128)(2,1)S(1)}, bf16[256,1024]{1,0:T(8,128)(2,1)S(1)}, u32[]{:S(2)}, u32[]{:S(2)}) %collective-permute-start.3) | collective-permute-done | bytes 524320 | tf_op jit(solution)/shard_map/ppermute | solution.py:261
  39.9 1.9 %norm_kv_next.1 = (bf16[256,2048]{1,0:T(8,128)(2,1)S(1)}, bf16[256,256]{1,0:T(8,128)(2,1)S(1)}) custom-call(s32[4]{0:T(128)S(1)} %pad_add_fusion.place_ref, bf16[256,1024]{1,0:T(8,128)(2,1)S(1)} %residual.1.mine_ref.x_ref, bf16[256,1024]{1,0:T(8,128)(2,1)S(1)} %collective-permute-done.3.other_ref, f32[2,2048]{1,0:T(2,128)S(1)} %copy-done.11, ...), custom_call_target="tpu_custom_call" | custom-call | flops 268435456 | bytes 3145728 | tf_op jit(solution)/shard_map/norm_kv_next/pallas_call | solution.py:319
  41.8 2.5 %collective-permute-start.4 = (bf16[256,256]{1,0:T(8,128)(2,1)S(1)}, bf16[256,256]{1,0:T(8,128)(2,1)S(1)}, u32[]{:S(2)}, u32[]{:S(2)}) collective-permute-start(bf16[256,256]{1,0:T(8,128)(2,1)S(1)} %get-tuple-element.20.kv_ref), channel_id=1, source_target_pairs={{0,4},{4,8},{8,12},{12,16},{16,20},{20,24},{24,28},{1,5},{5,9},{9,... | collective-permute-start | bytes 393224 | tf_op jit(solution)/shard_map/ppermute | solution.py:329
  44.3 1.3 %queries.3.q_ref = bf16[256,512]{1,0:T(8,128)(2,1)S(1)} custom-call(bf16[256,2048]{1,0:T(8,128)(2,1)S(1)} %get-tuple-element.19.normed_ref, bf16[2,2048,512]{2,1,0:T(8,128)(2,1)S(1)} %copy-done.1, f32[2,64]{1,0:T(2,128)S(1)} %copy-done.14), custom_call_target="tpu_custom_call" | custom-call | flops 536870912 | bytes 2097152 | tf_op jit(solution)/shard_map/queries/pallas_call | solution.py:332
  45.7 4.5 %collective-permute-done.4.kvp_ref = bf16[256,256]{1,0:T(8,128)(2,1)S(1)} collective-permute-done((bf16[256,256]{1,0:T(8,128)(2,1)S(1)}, bf16[256,256]{1,0:T(8,128)(2,1)S(1)}, u32[]{:S(2)}, u32[]{:S(2)}) %collective-permute-start.4) | collective-permute-done | bytes 131104 | tf_op jit(solution)/shard_map/ppermute | solution.py:329
  50.1 3.5 %attention.3 = (bf16[256,1024]{1,0:T(8,128)(2,1)S(1)}, bf16[256,1024]{1,0:T(8,128)(2,1)S(1)}) custom-call(s32[4]{0:T(128)S(1)} %pad_add_fusion.place_ref, bf16[256,512]{1,0:T(8,128)(2,1)S(1)} %queries.3.q_ref, bf16[256,256]{1,0:T(8,128)(2,1)S(1)} %get-tuple-element.20.kv_ref, bf16[256,256]{1,0:T(8,128)(2,1)S(1)} %collective-permute-done.4.kvp_ref, ...), custom_call_target="tpu_custom_call" | custom-call | flops 939524096 | bytes 2097152 | tf_op jit(solution)/shard_map/attention/pallas_call | solution.py:345
  53.7 1.9 %collective-permute-done.5.b_ref = bf16[256,1024]{1,0:T(8,128)(2,1)S(1)} collective-permute-done((bf16[256,1024]{1,0:T(8,128)(2,1)S(1)}, bf16[256,1024]{1,0:T(8,128)(2,1)S(1)}, u32[]{:S(2)}, u32[]{:S(2)}) %collective-permute-start.5) | collective-permute-done | bytes 524320 | tf_op jit(solution)/shard_map/ppermute | solution.py:261
  55.6 0.7 %split_add.1 = (bf16[256,512]{1,0:T(8,128)(2,1)S(1)}, bf16[256,512]{1,0:T(8,128)(2,1)S(1)}) custom-call(s32[4]{0:T(128)S(1)} %pad_add_fusion.place_ref, bf16[256,1024]{1,0:T(8,128)(2,1)S(1)} %get-tuple-element.21.a_ref, bf16[256,1024]{1,0:T(8,128)(2,1)S(1)} %collective-permute-done.5.b_ref), custom_call_target="tpu_custom_call" | custom-call | tf_op jit(solution)/shard_map/split_add/pallas_call | solution.py:389
  56.2 0.6 collective-permute-start.6
  56.8 7.8 %collective-permute-done.6.b_ref = bf16[256,512]{1,0:T(8,128)(2,1)S(1)} collective-permute-done((bf16[256,512]{1,0:T(8,128)(2,1)S(1)}, bf16[256,512]{1,0:T(8,128)(2,1)S(1)}, u32[]{:S(2)}, u32[]{:S(2)}) %collective-permute-start.6) | collective-permute-done | bytes 262176 | tf_op jit(solution)/shard_map/ppermute | solution.py:261
  64.6 1.3 %result.1 = bf16[256,512]{1,0:T(8,128)(2,1)} custom-call(s32[4]{0:T(128)S(1)} %pad_add_fusion.place_ref, bf16[256,1024]{1,0:T(8,128)(2,1)S(1)} %residual.1.mine_ref.x_ref, bf16[256,512]{1,0:T(8,128)(2,1)S(1)} %get-tuple-element.23.a_ref, bf16[256,512]{1,0:T(8,128)(2,1)S(1)} %collective-permute-done.6.b_ref), custom_call_target="tpu_custom_call" | custom-call | tf_op jit(solution)/shard_map/result/pallas_call | solution.py:398
  (26 shorter events, 0.1 us)
Async XLA Ops:
  0.0 1.2 %copy-start.4 = (bf16[256,2048]{1,0:T(8,128)(2,1)S(1)}, bf16[256,2048]{1,0:T(8,128)(2,1)}, u32[]{:S(2)}) copy-start(bf16[256,2048]{1,0:T(8,128)(2,1)} %x_ref.3) | copy-start | bytes 3145732
  1.2 1.2 %copy-start.6 = (bf16[2,2048,128]{2,1,0:T(8,128)(2,1)S(1)}, bf16[2,2048,128]{2,1,0:T(8,128)(2,1)}, u32[]{:S(2)}) copy-start(bf16[2,2048,128]{2,1,0:T(8,128)(2,1)} %wk_any.3) | copy-start | bytes 3145732
  2.5 1.2 %copy-start.8 = (bf16[2,2048,128]{2,1,0:T(8,128)(2,1)S(1)}, bf16[2,2048,128]{2,1,0:T(8,128)(2,1)}, u32[]{:S(2)}) copy-start(bf16[2,2048,128]{2,1,0:T(8,128)(2,1)} %wv_any.3) | copy-start | bytes 3145732
  3.7 0.7 %copy-start.10 = (f32[2,2048]{1,0:T(2,128)S(1)}, f32[2,2048]{1,0:T(2,128)}, u32[]{:S(2)}) copy-start(f32[2,2048]{1,0:T(2,128)} %gain_ref.3) | copy-start | bytes 49156
  4.4 0.7 %copy-start.12 = (f32[2,64]{1,0:T(2,128)S(1)}, f32[2,64]{1,0:T(2,128)}, u32[]{:S(2)}) copy-start(f32[2,64]{1,0:T(2,128)} %kg_ref.3) | copy-start | bytes 1540
  6.4 5.8 %copy-start = (bf16[2,2048,512]{2,1,0:T(8,128)(2,1)S(1)}, bf16[2,2048,512]{2,1,0:T(8,128)(2,1)}, u32[]{:S(2)}) copy-start(bf16[2,2048,512]{2,1,0:T(8,128)(2,1)} %wq_any.3) | copy-start | bytes 12582916
  6.4 5.8 %copy-start.14 = (f32[2,64]{1,0:T(2,128)S(1)}, f32[2,64]{1,0:T(2,128)}, u32[]{:S(2)}) copy-start(f32[2,64]{1,0:T(2,128)} %qg_ref.3) | copy-start | bytes 1540
  6.4 8.4 %collective-permute-start = (bf16[256,256]{1,0:T(8,128)(2,1)S(1)}, bf16[256,256]{1,0:T(8,128)(2,1)}, u32[]{:S(2)}, u32[]{:S(2)}) collective-permute-start(bf16[256,256]{1,0:T(8,128)(2,1)S(1)} %get-tuple-element.16.kv_ref), channel_id=1, source_target_pairs={{0,4},{4,8},{8,12},{12,16},{16,20},{20,24},{24,28},{1,5},{5,9},{9,... | collective-permute-start | bytes 393224 | tf_op jit(solution)/shard_map/ppermute | solution.py:329
  10.1 0.7 %copy-start.15 = (f32[2,8,257]{2,1,0:T(8,128)S(1)}, f32[2,8,257]{2,1,0:T(8,128)}, u32[]{:S(2)}) copy-start(f32[2,8,257]{2,1,0:T(8,128)} %table_ref.1) | copy-start | bytes 49348
  14.8 2.2 %copy-start.2 = (bf16[2,512,2048]{2,1,0:T(8,128)(2,1)S(1)}, bf16[2,512,2048]{2,1,0:T(8,128)(2,1)}, u32[]{:S(2)}) copy-start(bf16[2,512,2048]{2,1,0:T(8,128)(2,1)} %wout_any.3) | copy-start | bytes 12582916
  17.0 20.2 %copy-start.5 = (bf16[256,2048]{1,0:T(8,128)(2,1)S(1)}, bf16[256,2048]{1,0:T(8,128)(2,1)}, u32[]{:S(2)}) copy-start(bf16[256,2048]{1,0:T(8,128)(2,1)} %x_ref.3) | copy-start | bytes 3145732
  17.0 22.9 %copy-start.7 = (bf16[2,2048,128]{2,1,0:T(8,128)(2,1)S(1)}, bf16[2,2048,128]{2,1,0:T(8,128)(2,1)}, u32[]{:S(2)}) copy-start(bf16[2,2048,128]{2,1,0:T(8,128)(2,1)} %wk_any.3) | copy-start | bytes 3145732
  17.0 22.9 %copy-start.9 = (bf16[2,2048,128]{2,1,0:T(8,128)(2,1)S(1)}, bf16[2,2048,128]{2,1,0:T(8,128)(2,1)}, u32[]{:S(2)}) copy-start(bf16[2,2048,128]{2,1,0:T(8,128)(2,1)} %wv_any.3) | copy-start | bytes 3145732
  17.0 22.9 %copy-start.11 = (f32[2,2048]{1,0:T(2,128)S(1)}, f32[2,2048]{1,0:T(2,128)}, u32[]{:S(2)}) copy-start(f32[2,2048]{1,0:T(2,128)} %gain_ref.3) | copy-start | bytes 49156
  17.0 22.9 %copy-start.13 = (f32[2,64]{1,0:T(2,128)S(1)}, f32[2,64]{1,0:T(2,128)}, u32[]{:S(2)}) copy-start(f32[2,64]{1,0:T(2,128)} %kg_ref.3) | copy-start | bytes 1540
  21.0 23.3 %copy-start.1 = (bf16[2,2048,512]{2,1,0:T(8,128)(2,1)S(1)}, bf16[2,2048,512]{2,1,0:T(8,128)(2,1)}, u32[]{:S(2)}) copy-start(bf16[2,2048,512]{2,1,0:T(8,128)(2,1)} %wq_any.3) | copy-start | bytes 12582916
  21.0 2.0 %collective-permute-start.1 = (bf16[256,1024]{1,0:T(8,128)(2,1)S(1)}, bf16[256,1024]{1,0:T(8,128)(2,1)S(1)}, u32[]{:S(2)}, u32[]{:S(2)}) collective-permute-start(bf16[256,1024]{1,0:T(8,128)(2,1)S(1)} %get-tuple-element.18), channel_id=1, source_target_pairs={{0,1},{1,0},{2,3},{3,2},{4,5},{5,4},{6,7},{7,6},{8,9},{9,8},{10,11... | collective-permute-start | bytes 1572872 | tf_op jit(solution)/shard_map/ppermute | solution.py:261
  23.1 14.0 %collective-permute-start.2 = (bf16[256,1024]{1,0:T(8,128)(2,1)S(1)}, bf16[256,1024]{1,0:T(8,128)(2,1)S(1)}, u32[]{:S(2)}, u32[]{:S(2)}) collective-permute-start(bf16[256,1024]{1,0:T(8,128)(2,1)S(1)} %add.13.a_ref), channel_id=1, source_target_pairs={{0,2},{1,3},{2,0},{3,1},{4,6},{5,7},{6,4},{7,5},{8,10},{9,11},{10,... | collective-permute-start | bytes 1572872 | tf_op jit(solution)/shard_map/ppermute | solution.py:261
  37.9 12.2 %copy-start.3 = (bf16[2,512,2048]{2,1,0:T(8,128)(2,1)S(1)}, bf16[2,512,2048]{2,1,0:T(8,128)(2,1)}, u32[]{:S(2)}) copy-start(bf16[2,512,2048]{2,1,0:T(8,128)(2,1)} %wout_any.3) | copy-start | bytes 12582916
  37.9 2.0 %collective-permute-start.3 = (bf16[256,1024]{1,0:T(8,128)(2,1)S(1)}, bf16[256,1024]{1,0:T(8,128)(2,1)S(1)}, u32[]{:S(2)}, u32[]{:S(2)}) collective-permute-start(bf16[256,1024]{1,0:T(8,128)(2,1)S(1)} %residual.1.mine_ref.x_ref), channel_id=1, source_target_pairs={{0,1},{1,0},{2,3},{3,2},{4,5},{5,4},{6,7},{7,6},{8,9},{9,8},{10,11... | collective-permute-start | bytes 1572872 | tf_op jit(solution)/shard_map/ppermute | solution.py:261
  41.8 8.3 %collective-permute-start.4 = (bf16[256,256]{1,0:T(8,128)(2,1)S(1)}, bf16[256,256]{1,0:T(8,128)(2,1)S(1)}, u32[]{:S(2)}, u32[]{:S(2)}) collective-permute-start(bf16[256,256]{1,0:T(8,128)(2,1)S(1)} %get-tuple-element.20.kv_ref), channel_id=1, source_target_pairs={{0,4},{4,8},{8,12},{12,16},{16,20},{20,24},{24,28},{1,5},{5,9},{9,... | collective-permute-start | bytes 393224 | tf_op jit(solution)/shard_map/ppermute | solution.py:329
  53.6 2.0 %collective-permute-start.5 = (bf16[256,1024]{1,0:T(8,128)(2,1)S(1)}, bf16[256,1024]{1,0:T(8,128)(2,1)S(1)}, u32[]{:S(2)}, u32[]{:S(2)}) collective-permute-start(bf16[256,1024]{1,0:T(8,128)(2,1)S(1)} %get-tuple-element.22), channel_id=1, source_target_pairs={{0,1},{1,0},{2,3},{3,2},{4,5},{5,4},{6,7},{7,6},{8,9},{9,8},{10,11... | collective-permute-start | bytes 1572872 | tf_op jit(solution)/shard_map/ppermute | solution.py:261
  56.2 8.4 %collective-permute-start.6 = (bf16[256,512]{1,0:T(8,128)(2,1)S(1)}, bf16[256,512]{1,0:T(8,128)(2,1)S(1)}, u32[]{:S(2)}, u32[]{:S(2)}) collective-permute-start(bf16[256,512]{1,0:T(8,128)(2,1)S(1)} %get-tuple-element.24), channel_id=1, source_target_pairs={{0,2},{1,3},{2,0},{3,1},{4,6},{5,7},{6,4},{7,5},{8,10},{9,11},{10,... | collective-permute-start | bytes 786440 | tf_op jit(solution)/shard_map/ppermute | solution.py:261

commit v2 on v1

v2 whole, which is shorter than its diff:
```python
import functools

import jax
import jax.numpy as jnp
from jax import lax
from jax.experimental import pallas as pl
from jax.experimental.pallas import tpu as pltpu
from jax.sharding import PartitionSpec as P


HEAD_DIM = 64
SEG = 64
LEFT = 4
CLIP = 128
LAYERS = 2

REACH = LEFT * SEG
CHUNK = 2 * SEG
PIECES = REACH // CHUNK + 1
WINDOW = REACH + CHUNK
LINE = WINDOW + CHUNK
LANES = 128

norm_eps = 1e-06
masked_score = -1e30

bf16 = jnp.bfloat16
f32 = jnp.float32

whole = pl.BlockSpec(memory_space=pltpu.VMEM)
scalar = pl.BlockSpec(memory_space=pltpu.SMEM)
in_hbm = pl.BlockSpec(memory_space=pltpu.HBM)


def params():
    return pltpu.CompilerParams(vmem_limit_bytes=12 * 1024 * 1024)


def cost(flops, moved):
    return pl.CostEstimate(flops=int(flops), bytes_accessed=int(moved), transcendentals=0)


def out(shape, dtype=bf16):
    return jax.ShapeDtypeStruct(shape, dtype)


def head_norm(flat, gain_row):
    width = flat.shape[1]
    step = min(width, LANES)
    row = lax.broadcasted_iota(jnp.int32, (step, step), 0) // HEAD_DIM
    col = lax.broadcasted_iota(jnp.int32, (step, step), 1) // HEAD_DIM
    mean_of = jnp.where(row == col, 1.0 / HEAD_DIM, 0.0).astype(bf16)
    gain = jnp.concatenate([gain_row] * (step // HEAD_DIM), axis=1)
    pieces = []
    for lower in range(0, width, step):
        part = flat[:, lower : lower + step]
        squared = part * part
        high = squared.astype(bf16)
        low = (squared - high.astype(f32)).astype(bf16)
        mean = jnp.dot(high, mean_of, preferred_element_type=f32) + jnp.dot(
            low, mean_of, preferred_element_type=f32
        )
        pieces.append(part * lax.rsqrt(mean + norm_eps) * gain)
    return pieces


def key_value_body(normed, wk, wv, key_gain_row, kv_ref):
    keys = jnp.dot(normed, wk, preferred_element_type=f32)
    values = jnp.dot(normed, wv, preferred_element_type=f32)
    keys = head_norm(keys, key_gain_row)[0]
    kv_ref[...] = jnp.concatenate([keys, values], axis=1).astype(bf16)


def first_norm_kernel(
    x_hbm, gain_hbm, wk_hbm, wv_hbm, kg_hbm, normed_ref, kv_ref,
    x_ref, gain_ref, wk_ref, wv_ref, kg_ref, row_sems, sems,
):
    steps = row_sems.shape[0]
    share = x_ref.shape[0] // steps
    row_copies = []
    for index in range(steps):
        at = pl.ds(index * share, share)
        row_copies.append(
            pltpu.make_async_copy(x_hbm.at[at, :], x_ref.at[at, :], row_sems.at[index])
        )
    gain_copy = pltpu.make_async_copy(gain_hbm, gain_ref, sems.at[0])
    late = [
        pltpu.make_async_copy(wk_hbm.at[0], wk_ref, sems.at[1]),
        pltpu.make_async_copy(wv_hbm.at[0], wv_ref, sems.at[2]),
        pltpu.make_async_copy(kg_hbm, kg_ref, sems.at[3]),
    ]
    for copy in [gain_copy] + row_copies + late:
        copy.start()
    gain_copy.wait()
    gain = gain_ref[0:1, :]
    for index, copy in enumerate(row_copies):
        copy.wait()
        at = slice(index * share, (index + 1) * share)
        current = x_ref[at, :].astype(f32)
        mean = jnp.mean(current * current, axis=-1, keepdims=True)
        normed_ref[at, :] = (current * lax.rsqrt(mean + norm_eps) * gain).astype(bf16)
    for copy in late:
        copy.wait()
    key_value_body(normed_ref[...], wk_ref[...], wv_ref[...], kg_ref[0:1, :], kv_ref)


def next_norm_kernel(
    layer_index, block, place_ref, mine_ref, other_ref, gain_ref, wk_ref, wv_ref, kg_ref,
    normed_ref, kv_ref,
):
    parity = place_ref[1]
    mine = mine_ref[...].astype(f32)
    other = other_ref[...].astype(f32)
    total = jnp.sum(mine * mine, axis=-1, keepdims=True)
    total = total + jnp.sum(other * other, axis=-1, keepdims=True)
    scale = lax.rsqrt(total / (2 * mine.shape[1]) + norm_eps)
    for index in range(mine.shape[1] // block):
        for held, side in ((mine, parity), (other, 1 - parity)):
            cols = pl.ds(pl.multiple_of((2 * index + side) * block, LANES), block)
            piece = held[:, index * block : (index + 1) * block]
            gain = gain_ref[layer_index : layer_index + 1, cols]
            normed_ref[:, cols] = (piece * scale * gain).astype(bf16)
    key_value_body(
        normed_ref[...], wk_ref[layer_index], wv_ref[layer_index],
        kg_ref[layer_index : layer_index + 1, :], kv_ref,
    )


def first_query_kernel(normed_ref, wq_hbm, qg_ref, q_ref, wq_ref, sems):
    share = wq_ref.shape[0] // sems.shape[0]
    copies = []
    for index in range(sems.shape[0]):
        at = pl.ds(index * share, share)
        copy = pltpu.make_async_copy(wq_hbm.at[0, at, :], wq_ref.at[at, :], sems.at[index])
        copy.start()
        copies.append(copy)
    flat = None
    for index, copy in enumerate(copies):
        copy.wait()
        at = slice(index * share, (index + 1) * share)
        piece = jnp.dot(normed_ref[:, at], wq_ref[at, :], preferred_element_type=f32)
        flat = piece if flat is None else flat + piece
    query_body(flat, qg_ref[0:1, :], q_ref)


def query_kernel(layer_index, normed_ref, wq_ref, qg_ref, q_ref):
    flat = jnp.dot(normed_ref[...], wq_ref[layer_index], preferred_element_type=f32)
    query_body(flat, qg_ref[layer_index : layer_index + 1, :], q_ref)


def query_body(flat, gain_row, q_ref):
    pieces = head_norm(flat, gain_row)
    width = pieces[0].shape[1]
    for index, piece in enumerate(pieces):
        scaled = piece.astype(bf16) * bf16(HEAD_DIM**-0.5)
        q_ref[:, index * width : (index + 1) * width] = scaled


def bias_kernel(layer_index, table_ref, tile_ref):
    heads, entries = table_ref.shape[1:]
    source = lax.broadcasted_iota(jnp.int32, (entries, LINE), 0)
    offset = lax.broadcasted_iota(jnp.int32, (entries, LINE), 1)
    distance = jnp.clip(WINDOW - 1 - offset, -CLIP, CLIP) + CLIP
    onehot = (source == distance).astype(f32)
    query_seg = lax.broadcasted_iota(jnp.int32, (CHUNK, WINDOW), 0) // SEG
    key_seg = lax.broadcasted_iota(jnp.int32, (CHUNK, WINDOW), 1) // SEG
    inside = (key_seg >= query_seg) & (key_seg <= query_seg + LEFT)
    line = jnp.dot(
        table_ref[layer_index], onehot, precision=lax.Precision.HIGHEST,
        preferred_element_type=f32,
    )
    for head in range(heads):
        spread = jnp.broadcast_to(line[head : head + 1, :], (CHUNK, LINE))
        rolled = pltpu.roll(spread, LINE - CHUNK + 1, 1, stride=1, stride_axis=0)
        tile_ref[head] = jnp.where(inside, rolled[:, :WINDOW], masked_score)


def attention_kernel(
    block, layer_index, q_start, starts, prior, place_ref, q_ref, *refs,
):
    piece_refs = refs[:PIECES]
    (
        tile_ref, wout_hbm, keep_ref, send_ref,
        keys_ref, even_ref, odd_ref, mixed_ref, wout_ref, sem,
    ) = refs[PIECES:]
    wout_copy = pltpu.make_async_copy(wout_hbm.at[layer_index], wout_ref, sem.at[0])
    wout_copy.start()
    first, parity = place_ref[0], place_ref[1]
    heads = q_ref.shape[1] // HEAD_DIM
    kv_width = piece_refs[0].shape[1] // 2
    kv_heads = kv_width // HEAD_DIM
    group = heads // kv_heads
    pairs = group // 2

    low = lax.broadcasted_iota(jnp.int32, (CHUNK, LANES), 1) < HEAD_DIM
    for index, piece_ref in enumerate(piece_refs):
        source = slice(starts[index], starts[index] + CHUNK)
        into = slice(index * CHUNK, (index + 1) * CHUNK)
        for kv in range(kv_heads):
            at = kv * HEAD_DIM
            key = piece_ref[source, at : at + HEAD_DIM].astype(f32)
            value = piece_ref[source, kv_width + at : kv_width + at + HEAD_DIM].astype(f32)
            key = jnp.concatenate([key, key], axis=1)
            value = jnp.concatenate([value, value], axis=1)
            keys_ref[kv, into, :] = key.astype(bf16)
            even_ref[kv, into, :] = jnp.where(low, value, 1.0).astype(bf16)
            odd_ref[kv, into, :] = jnp.where(low, 1.0, value).astype(bf16)

    key_index = lax.broadcasted_iota(jnp.int32, (1, WINDOW), 1)
    outside = jnp.where((key_index < prior * CHUNK) & (first == 1), masked_score, 0.0)
    for kv in range(kv_heads):
        evens, odds = [], []
        for pair in range(pairs):
            at = (kv * pairs + pair) * LANES
            both = q_ref[q_start : q_start + CHUNK, at : at + LANES]
            evens.append(jnp.where(low, both, jnp.zeros_like(both)))
            odds.append(jnp.where(low, jnp.zeros_like(both), both))
        stacked = jnp.concatenate(evens + odds, axis=0)
        scores = lax.dot_general(
            stacked, keys_ref[kv], (((1,), (1,)), ((), ())), preferred_element_type=f32
        )
        expons = []
        for index in range(group):
            pair, side = index % pairs, index // pairs
            head = kv * group + 2 * pair + side
            score = scores[index * CHUNK : (index + 1) * CHUNK, :] + tile_ref[head]
            if prior:
                score = score + outside
            peak = jnp.max(score, axis=-1, keepdims=True)
            expons.append(jnp.exp(score - peak).astype(bf16))
        even = jnp.dot(
            jnp.concatenate(expons[:pairs], axis=0), even_ref[kv], preferred_element_type=f32
        )
        odd = jnp.dot(
            jnp.concatenate(expons[pairs:], axis=0), odd_ref[kv], preferred_element_type=f32
        )
        for pair in range(pairs):
            at = (kv * pairs + pair) * LANES
            upper = even[pair * CHUNK : (pair + 1) * CHUNK, :]
            lower = odd[pair * CHUNK : (pair + 1) * CHUNK, :]
            total = pltpu.roll(jnp.where(low, lower, upper), HEAD_DIM, 1)
            mixed_ref[:, at : at + LANES] = (jnp.where(low, upper, lower) / total).astype(bf16)

    mixed = mixed_ref[...]
    wout_copy.wait()
    for index in range(keep_ref.shape[1] // block):
        for target, side in ((send_ref, 1 - parity), (keep_ref, parity)):
            cols = pl.ds(pl.multiple_of((2 * index + side) * block, LANES), block)
            partial_value = jnp.dot(mixed, wout_ref[:, cols], preferred_element_type=f32)
            target[:, index * block : (index + 1) * block] = partial_value.astype(bf16)


def add_kernel(a_ref, b_ref, out_ref):
    out_ref[...] = (a_ref[...].astype(f32) + b_ref[...].astype(f32)).astype(bf16)


def split_add_kernel(block, bit, place_ref, a_ref, b_ref, keep_ref, send_ref):
    parity = place_ref[bit]
    for index in range(keep_ref.shape[1] // block):
        into = slice(index * block, (index + 1) * block)
        for target, side in ((send_ref, 1 - parity), (keep_ref, parity)):
            cols = pl.ds(pl.multiple_of((2 * index + side) * block, LANES), block)
            target[:, into] = (
                a_ref[:, cols].astype(f32) + b_ref[:, cols].astype(f32)
            ).astype(bf16)


def residual_kernel(block, start, place_ref, x_ref, a_ref, b_ref, out_ref):
    rows = slice(start, start + out_ref.shape[0])
    for index in range(out_ref.shape[1] // block):
        into = slice(index * block, (index + 1) * block)
        cols = pl.ds(pl.multiple_of((2 * index + place_ref[1]) * block, LANES), block)
        added = a_ref[:, into].astype(f32) + b_ref[:, into].astype(f32)
        out_ref[:, into] = (x_ref[rows, cols].astype(f32) + added).astype(bf16)


def result_kernel(block, at, parts, place_ref, *refs):
    ins, out_hbm, held_ref, sems = refs[: 3 * parts], refs[-3], refs[-2], refs[-1]
    cols = pl.ds(pl.multiple_of(place_ref[at] * block, LANES), block)
    copies = []
    for part in range(parts):
        x_ref, a_ref, b_ref = ins[3 * part : 3 * part + 3]
        rows = slice(part * CHUNK, (part + 1) * CHUNK)
        added = a_ref[...].astype(f32) + b_ref[...].astype(f32)
        held_ref[rows, :] = (x_ref[:, cols].astype(f32) + added).astype(bf16)
        span = pl.ds(part * CHUNK, CHUNK)
        copy = pltpu.make_async_copy(held_ref.at[span, :], out_hbm.at[span, :], sems.at[part])
        copy.start()
        copies.append(copy)
    for copy in copies:
        copy.wait()


def swapped(value, bit):
    size = lax.axis_size("tp")
    return lax.ppermute(value, "tp", [(d, d ^ (1 << bit)) for d in range(size)])


def passed_along(value):
    return lax.ppermute(value, "sp", [(d, d + 1) for d in range(lax.axis_size("sp") - 1)])


def kept_in_hbm(*arrays):
    return [pltpu.with_memory_space_constraint(array, pltpu.HBM) for array in arrays]


def layers(stream, attn_gain, w_query, w_key, w_value, w_out, query_gain, key_gain, rel_bias):
    rows, width = stream.shape
    bits = lax.axis_size("tp").bit_length() - 1
    block = width // lax.axis_size("tp")
    half = width // 2
    query_width = w_query.shape[2]
    kv_width = w_key.shape[2]
    heads = query_width // HEAD_DIM
    kv_heads = kv_width // HEAD_DIM
    parts = rows // CHUNK
    order = list(reversed(range(parts)))
    tp_index = lax.axis_index("tp")
    place = jnp.stack(
        [(lax.axis_index("sp") == 0).astype(jnp.int32), tp_index % 2]
        + [(tp_index >> bit) & 1 for bit in range(1, bits)]
        + [tp_index // 2]
    ).astype(jnp.int32)

    def queries(layer_index, normed):
        count = normed.shape[0]
        return pl.pallas_call(
            functools.partial(query_kernel, layer_index),
            out_shape=out((count, query_width)),
            in_specs=[whole] * 3,
            out_specs=whole,
            compiler_params=params(),
            cost_estimate=cost(2 * count * width * query_width, 2 * width * query_width),
            name="queries",
        )(normed, w_query, query_gain)

    def attention(layer_index, part, query, q_start, pieces, starts):
        return pl.pallas_call(
            functools.partial(
                attention_kernel, block, layer_index, q_start, starts,
                max(0, PIECES - 1 - part),
            ),
            out_shape=[out((CHUNK, half))] * 2,
            in_specs=[scalar, whole] + [whole] * PIECES + [whole, in_hbm],
            out_specs=[whole, whole],
            scratch_shapes=[
                pltpu.VMEM((kv_heads, WINDOW, LANES), bf16),
                pltpu.VMEM((kv_heads, WINDOW, LANES), bf16),
                pltpu.VMEM((kv_heads, WINDOW, LANES), bf16),
                pltpu.VMEM((CHUNK, query_width), bf16),
                pltpu.VMEM((query_width, width), bf16),
                pltpu.SemaphoreType.DMA((1,)),
            ],
            compiler_params=params(),
            cost_estimate=cost(
                2 * CHUNK * query_width * (width + 4 * WINDOW), 2 * width * query_width
            ),
            name="attention",
        )(place, query, *pieces, tiles[layer_index], *kept_in_hbm(w_out))

    normed, kv = pl.pallas_call(
        first_norm_kernel,
        out_shape=[out((rows, width)), out((rows, 2 * kv_width))],
        in_specs=[in_hbm] * 5,
        out_specs=[whole, whole],
        scratch_shapes=[
            pltpu.VMEM(stream.shape, bf16),
            pltpu.VMEM(attn_gain.shape, f32),
            pltpu.VMEM((width, kv_width), bf16),
            pltpu.VMEM((width, kv_width), bf16),
            pltpu.VMEM(key_gain.shape, f32),
            pltpu.SemaphoreType.DMA((4,)),
            pltpu.SemaphoreType.DMA((4,)),
        ],
        compiler_params=params(),
        cost_estimate=cost(4 * rows * width * kv_width, 4 * rows * width),
        name="norm_kv_first",
    )(*kept_in_hbm(stream, attn_gain, w_key, w_value, key_gain))
    kv_prior = passed_along(kv[rows - REACH :])
    query = pl.pallas_call(
        first_query_kernel,
        out_shape=out((rows, query_width)),
        in_specs=[whole, in_hbm, whole],
        out_specs=whole,
        scratch_shapes=[
            pltpu.VMEM((width, query_width), bf16),
            pltpu.SemaphoreType.DMA((4,)),
        ],
        compiler_params=params(),
        cost_estimate=cost(2 * rows * width * query_width, 2 * width * query_width),
        name="queries",
    )(normed, *kept_in_hbm(w_query), query_gain)
    tiles = []
    for layer_index in range(LAYERS):
        tiles.append(
            pl.pallas_call(
                functools.partial(bias_kernel, layer_index),
                out_shape=out((heads, CHUNK, WINDOW), f32),
                in_specs=[whole],
                out_specs=whole,
                compiler_params=params(),
                cost_estimate=cost(5e8, 1e6),
                name="bias_tiles",
            )(rel_bias)
        )

    mine, other, kvs, normeds = {}, {}, {}, {}
    for part in order:
        pieces, starts = [], []
        for index in range(PIECES):
            behind = part - (PIECES - 1) + index
            pieces.append(kv_prior if behind < 0 else kv)
            starts.append((behind + PIECES - 1 if behind < 0 else behind) * CHUNK)
        keep, send = attention(0, part, query, part * CHUNK, pieces, starts)
        received = swapped(send, 0)
        for bit in range(1, bits):
            summed = pl.pallas_call(
                add_kernel,
                out_shape=out((CHUNK, half)),
                in_specs=[whole, whole],
                out_specs=whole,
                compiler_params=params(),
                name="add",
            )(keep, received)
            keep, received = summed, swapped(summed, bit)
        mine[part] = pl.pallas_call(
            functools.partial(residual_kernel, block, part * CHUNK),
            out_shape=out((CHUNK, half)),
            in_specs=[scalar, whole, whole, whole],
            out_specs=whole,
            compiler_params=params(),
            name="residual",
        )(place, stream, keep, received)
        other[part] = swapped(mine[part], 0)

    priors = {}
    for part in order:
        normeds[part], kvs[part] = pl.pallas_call(
            functools.partial(next_norm_kernel, 1, block),
            out_shape=[out((CHUNK, width)), out((CHUNK, 2 * kv_width))],
            in_specs=[scalar] + [whole] * 6,
            out_specs=[whole, whole],
            compiler_params=params(),
            cost_estimate=cost(4 * CHUNK * width * kv_width, 4 * CHUNK * width),
            name="norm_kv_next",
        )(place, mine[part], other[part], attn_gain, w_key, w_value, key_gain)
        if part >= parts - (PIECES - 1):
            priors[part - parts] = passed_along(kvs[part])

    outs = {}
    for part in order:
        query = queries(1, normeds[part])
        pieces = []
        for index in range(PIECES):
            behind = part - (PIECES - 1) + index
            pieces.append(priors[behind] if behind < 0 else kvs[behind])
        keep, send = attention(1, part, query, 0, pieces, [0] * PIECES)
        received = swapped(send, 0)
        for bit in range(1, bits):
            left = keep.shape[1] // 2
            keep, send = pl.pallas_call(
                functools.partial(split_add_kernel, block, 1 + bit),
                out_shape=[out((CHUNK, left))] * 2,
                in_specs=[scalar, whole, whole],
                out_specs=[whole, whole],
                compiler_params=params(),
                name="split_add",
            )(place, keep, received)
            received = swapped(send, bit)
        outs[part] = (mine[part], keep, received)

    return pl.pallas_call(
        functools.partial(result_kernel, block, bits + 1, parts),
        out_shape=out((rows, block)),
        in_specs=[scalar] + [whole] * (3 * parts),
        out_specs=in_hbm,
        scratch_shapes=[
            pltpu.VMEM((rows, block), bf16),
            pltpu.SemaphoreType.DMA((parts,)),
        ],
        compiler_params=params(),
        name="result",
    )(place, *[ref for part in range(parts) for ref in outs[part]])


def solution(mesh):
    return jax.shard_map(
        layers,
        mesh=mesh,
        in_specs=(
            P("sp", None),
            P(),
            P(None, None, "tp"),
            P(None, None, "tp"),
            P(None, None, "tp"),
            P(None, "tp", None),
            P(),
            P(),
            P(None, "tp", None),
        ),
        out_specs=P("sp", "tp"),
        check_vma=False,
    )
```

time: 66.4 us -> 64.4 us (0.970)
  the two profiles are of different devices: /device:TPU:26 before, /device:TPU:0 now
where the time goes in v2:
time: 64.4 us; the launch traced here: 64.1 us
  Pallas kernels  27.9 us (43%)
  starting transfers between devices  18.8 us (29%)
  waiting for transfers between devices  16 us (25%)
  local copies, waits for them, and re-layouts  0.72 us (1%)
    ppermute x10, waiting for transfers between devices, swapped(): return lax.ppermute(value, 'tp', [(d, d ^ 1 << bit) for d in range(size)])  16 us
    pallas_call x4, Pallas kernels, attention(): pl.pallas_call(functools.partial(attention_kernel, block, layer_index, q_...  13.7 us
    ppermute x3, starting transfers between devices, passed_along(): lax.ppermute(value, 'sp', [(d, d + 1) for d in range(lax.axis_size('sp')...  12.6 us
    ppermute x10, starting transfers between devices, swapped(): return lax.ppermute(value, 'tp', [(d, d ^ 1 << bit) for d in range(size)])  6.17 us
    pallas_call x2, Pallas kernels, layers(): pl.pallas_call(functools.partial(next_norm_kernel, 1, block), out_shape=[...  2.51 us
    pallas_call x1, Pallas kernels, layers(): pl.pallas_call(first_norm_kernel, out_shape=[out((rows, width)), out((row...  2.5 us
    pallas_call x1, Pallas kernels, layers(): pl.pallas_call(first_query_kernel, out_shape=out((rows, query_width)), in...  2.32 us
    pallas_call x2, Pallas kernels, layers(): pl.pallas_call(functools.partial(bias_kernel, layer_index), out_shape=out...  1.55 us
  transfers between devices with their start and end apart: 13, of which 4 were waited for; matrix products, arithmetic and copies ran while one was open for 0% of the time, Pallas kernels for 32%

profile of v2, /device:TPU:0, one launch (start us, length us, event | category | flops | bytes accessed | tf_op | source)
XLA Modules:
  0.0 64.1 jit_solution(14123548985753535224)
XLA Ops:
  0.0 2.5 %norm_kv_first.1 = (bf16[256,2048]{1,0:T(8,128)(2,1)S(1)}, bf16[256,256]{1,0:T(8,128)(2,1)S(1)}) custom-call(bf16[256,2048]{1,0:T(8,128)(2,1)} %x_ref.3, f32[2,2048]{1,0:T(2,128)} %gain_ref.3, bf16[2,2048,128]{2,1,0:T(8,128)(2,1)} %wk_ref.3, bf16[2,2048,128]{2,1,0:T(8,128)(2,1)} %wv_ref.3, f32[2,64]{1,0:T(2,128)} %kg_ref.3), custom_call_target="tpu_custom_call" | custom-call | flops 268435456 | bytes 2097152 | tf_op jit(solution)/shard_map/norm_kv_first/pallas_call | solution.py:361
  2.5 4.9 %collective-permute-start = (bf16[256,256]{1,0:T(8,128)(2,1)S(1)}, bf16[256,256]{1,0:T(8,128)(2,1)S(1)}, u32[]{:S(2)}, u32[]{:S(2)}) collective-permute-start(bf16[256,256]{1,0:T(8,128)(2,1)S(1)} %get-tuple-element.24.refs_2_.refs_1_), channel_id=1, source_target_pairs={{0,4},{4,8},{8,12},{12,16},{16,20},{20,24},{24,28},{1,5},{5,9},{9,... | collective-permute-start | bytes 393224 | tf_op jit(solution)/shard_map/ppermute | solution.py:300
  7.4 0.7 %copy-done.6 = f32[2,64]{1,0:T(2,128)S(1)} copy-done((f32[2,64]{1,0:T(2,128)S(1)}, f32[2,64]{1,0:T(2,128)}, u32[]{:S(2)}) %copy-start.6) | copy-done | bytes 536
  8.1 2.3 %queries.3.q_ref = bf16[256,512]{1,0:T(8,128)(2,1)S(1)} custom-call(bf16[256,2048]{1,0:T(8,128)(2,1)S(1)} %get-tuple-element.23.normed_ref, bf16[2,2048,512]{2,1,0:T(8,128)(2,1)} %wq_ref.3, f32[2,64]{1,0:T(2,128)S(1)} %copy-done.6), custom_call_target="tpu_custom_call" | custom-call | flops 536870912 | bytes 2097152 | tf_op jit(solution)/shard_map/queries/pallas_call | solution.py:380
  10.5 0.8 %bias_tiles.2.refs_3_ = f32[8,128,384]{2,1,0:T(8,128)S(1)} custom-call(f32[2,8,257]{2,1,0:T(8,128)S(1)} %copy-done.8), custom_call_target="tpu_custom_call" | custom-call | flops 500000000 | bytes 1000000 | tf_op jit(solution)/shard_map/bias_tiles/pallas_call | solution.py:396
  11.3 0.1 pad_add_fusion.place_ref
  11.3 3.5 %attention.5 = (bf16[128,1024]{1,0:T(8,128)(2,1)S(1)}, bf16[128,1024]{1,0:T(8,128)(2,1)S(1)}) custom-call(s32[4]{0:T(128)S(1)} %pad_add_fusion.place_ref, bf16[256,512]{1,0:T(8,128)(2,1)S(1)} %queries.3.q_ref, bf16[256,256]{1,0:T(8,128)(2,1)S(1)} %collective-permute-done.refs_0_.refs_1_, bf16[256,256]{1,0:T(8,128)(2,1)S(1)} %get-tuple-element.24.refs_2_.refs_1_, ...), custom_call_target="tpu_custom_call" | custom-call | flops 469762048 | bytes 2097152 | tf_op jit(solution)/shard_map/attention/pallas_call | solution.py:338
  14.9 3.5 %attention.4 = (bf16[128,1024]{1,0:T(8,128)(2,1)S(1)}, bf16[128,1024]{1,0:T(8,128)(2,1)S(1)}) custom-call(s32[4]{0:T(128)S(1)} %pad_add_fusion.place_ref, bf16[256,512]{1,0:T(8,128)(2,1)S(1)} %queries.3.q_ref, bf16[256,256]{1,0:T(8,128)(2,1)S(1)} %collective-permute-done.refs_0_.refs_1_, bf16[256,256]{1,0:T(8,128)(2,1)S(1)} %collective-permute-done.refs_0_.refs_1_, ...), custom_call_target="tpu_custom_call" | custom-call | flops 469762048 | bytes 2097152 | tf_op jit(solution)/shard_map/attention/pallas_call | solution.py:338
  18.4 0.6 collective-permute-start.1
  19.0 1.5 %collective-permute-start.6 = (bf16[128,1024]{1,0:T(8,128)(2,1)S(1)}, bf16[128,1024]{1,0:T(8,128)(2,1)S(1)}, u32[]{:S(2)}, u32[]{:S(2)}) collective-permute-start(bf16[128,1024]{1,0:T(8,128)(2,1)S(1)} %add.15.a_ref), channel_id=1, source_target_pairs={{0,2},{1,3},{2,0},{3,1},{4,6},{5,7},{6,4},{7,5},{8,10},{9,11},{10,... | collective-permute-start | bytes 786440 | tf_op jit(solution)/shard_map/ppermute | solution.py:296
  20.6 1.1 %collective-permute-start.2 = (bf16[128,1024]{1,0:T(8,128)(2,1)S(1)}, bf16[128,1024]{1,0:T(8,128)(2,1)S(1)}, u32[]{:S(2)}, u32[]{:S(2)}) collective-permute-start(bf16[128,1024]{1,0:T(8,128)(2,1)S(1)} %add.14.a_ref), channel_id=1, source_target_pairs={{0,2},{1,3},{2,0},{3,1},{4,6},{5,7},{6,4},{7,5},{8,10},{9,11},{10,... | collective-permute-start | bytes 786440 | tf_op jit(solution)/shard_map/ppermute | solution.py:296
  21.7 6.6 %collective-permute-done.6.b_ref = bf16[128,1024]{1,0:T(8,128)(2,1)S(1)} collective-permute-done((bf16[128,1024]{1,0:T(8,128)(2,1)S(1)}, bf16[128,1024]{1,0:T(8,128)(2,1)S(1)}, u32[]{:S(2)}, u32[]{:S(2)}) %collective-permute-start.6) | collective-permute-done | bytes 262176 | tf_op jit(solution)/shard_map/ppermute | solution.py:296
  28.3 0.6 %residual.3.mine_ref.refs_3_ = bf16[128,1024]{1,0:T(8,128)(2,1)S(1)} custom-call(s32[4]{0:T(128)S(1)} %pad_add_fusion.place_ref, bf16[256,2048]{1,0:T(8,128)(2,1)S(1)} %copy-done.1, bf16[128,1024]{1,0:T(8,128)(2,1)S(1)} %add.15.a_ref, bf16[128,1024]{1,0:T(8,128)(2,1)S(1)} %collective-permute-done.6.b_ref), custom_call_target="tpu_custom_call" | custom-call | tf_op jit(solution)/shard_map/residual/pallas_call | solution.py:426
  29.0 3.9 %collective-permute-done.2.b_ref = bf16[128,1024]{1,0:T(8,128)(2,1)S(1)} collective-permute-done((bf16[128,1024]{1,0:T(8,128)(2,1)S(1)}, bf16[128,1024]{1,0:T(8,128)(2,1)S(1)}, u32[]{:S(2)}, u32[]{:S(2)}) %collective-permute-start.2) | collective-permute-done | bytes 262176 | tf_op jit(solution)/shard_map/ppermute | solution.py:296
  33.0 0.6 residual.2.mine_ref.refs_0_
  33.7 1.3 %norm_kv_next.3 = (bf16[128,2048]{1,0:T(8,128)(2,1)S(1)}, bf16[128,256]{1,0:T(8,128)(2,1)S(1)}) custom-call(s32[4]{0:T(128)S(1)} %pad_add_fusion.place_ref, bf16[128,1024]{1,0:T(8,128)(2,1)S(1)} %residual.3.mine_ref.refs_3_, bf16[128,1024]{1,0:T(8,128)(2,1)S(1)} %collective-permute-done.7.other_ref, f32[2,2048]{1,0:T(2,128)S(1)} %copy-done.4, ...), custom_call_target="tpu_custom_call" | custom-call | flops 134217728 | bytes 1048576 | tf_op jit(solution)/shard_map/norm_kv_next/pallas_call | solution.py:438
  35.0 3.4 %collective-permute-start.8 = (bf16[128,256]{1,0:T(8,128)(2,1)S(1)}, bf16[128,256]{1,0:T(8,128)(2,1)S(1)}, u32[]{:S(2)}, u32[]{:S(2)}) collective-permute-start(bf16[128,256]{1,0:T(8,128)(2,1)S(1)} %get-tuple-element.31.refs_2_), channel_id=1, source_target_pairs={{0,4},{4,8},{8,12},{12,16},{16,20},{20,24},{24,28},{1,5},{5,9},{9,... | collective-permute-start | bytes 196616 | tf_op jit(solution)/shard_map/ppermute | solution.py:300
  38.4 0.8 %bias_tiles.3.refs_3_ = f32[8,128,384]{2,1,0:T(8,128)S(1)} custom-call(f32[2,8,257]{2,1,0:T(8,128)S(1)} %copy-done.8), custom_call_target="tpu_custom_call" | custom-call | flops 500000000 | bytes 1000000 | tf_op jit(solution)/shard_map/bias_tiles/pallas_call | solution.py:396
  39.2 1.3 %norm_kv_next.2 = (bf16[128,2048]{1,0:T(8,128)(2,1)S(1)}, bf16[128,256]{1,0:T(8,128)(2,1)S(1)}) custom-call(s32[4]{0:T(128)S(1)} %pad_add_fusion.place_ref, bf16[128,1024]{1,0:T(8,128)(2,1)S(1)} %residual.2.mine_ref.refs_0_, bf16[128,1024]{1,0:T(8,128)(2,1)S(1)} %collective-permute-done.3.other_ref, f32[2,2048]{1,0:T(2,128)S(1)} %copy-done.4, ...), custom_call_target="tpu_custom_call" | custom-call | flops 134217728 | bytes 1048576 | tf_op jit(solution)/shard_map/norm_kv_next/pallas_call | solution.py:438
  40.5 4.3 %collective-permute-start.4 = (bf16[128,256]{1,0:T(8,128)(2,1)S(1)}, bf16[128,256]{1,0:T(8,128)(2,1)S(1)}, u32[]{:S(2)}, u32[]{:S(2)}) collective-permute-start(bf16[128,256]{1,0:T(8,128)(2,1)S(1)} %get-tuple-element.28.refs_2_.refs_1_), channel_id=1, source_target_pairs={{0,4},{4,8},{8,12},{12,16},{16,20},{20,24},{24,28},{1,5},{5,9},{9,... | collective-permute-start | bytes 196616 | tf_op jit(solution)/shard_map/ppermute | solution.py:300
  44.8 0.7 %queries.5.q_ref = bf16[128,512]{1,0:T(8,128)(2,1)S(1)} custom-call(bf16[128,2048]{1,0:T(8,128)(2,1)S(1)} %get-tuple-element.36.normed_ref, bf16[2,2048,512]{2,1,0:T(8,128)(2,1)S(1)} %copy-done, f32[2,64]{1,0:T(2,128)S(1)} %copy-done.7), custom_call_target="tpu_custom_call" | custom-call | flops 268435456 | bytes 2097152 | tf_op jit(solution)/shard_map/queries/pallas_call | solution.py:327
  45.5 0.7 %queries.4.q_ref = bf16[128,512]{1,0:T(8,128)(2,1)S(1)} custom-call(bf16[128,2048]{1,0:T(8,128)(2,1)S(1)} %get-tuple-element.27.normed_ref, bf16[2,2048,512]{2,1,0:T(8,128)(2,1)S(1)} %copy-done, f32[2,64]{1,0:T(2,128)S(1)} %copy-done.7), custom_call_target="tpu_custom_call" | custom-call | flops 268435456 | bytes 2097152 | tf_op jit(solution)/shard_map/queries/pallas_call | solution.py:327
  46.2 3.4 %attention.7 = (bf16[128,1024]{1,0:T(8,128)(2,1)S(1)}, bf16[128,1024]{1,0:T(8,128)(2,1)S(1)}) custom-call(s32[4]{0:T(128)S(1)} %pad_add_fusion.place_ref, bf16[128,512]{1,0:T(8,128)(2,1)S(1)} %queries.5.q_ref, bf16[128,256]{1,0:T(8,128)(2,1)S(1)} %collective-permute-done.8.refs_1_.refs_0_, bf16[128,256]{1,0:T(8,128)(2,1)S(1)} %get-tuple-element.28.refs_2_.refs_1_, ...), custom_call_target="tpu_custom_call" | custom-call | flops 469762048 | bytes 2097152 | tf_op jit(solution)/shard_map/attention/pallas_call | solution.py:338
  49.7 3.4 %attention.6 = (bf16[128,1024]{1,0:T(8,128)(2,1)S(1)}, bf16[128,1024]{1,0:T(8,128)(2,1)S(1)}) custom-call(s32[4]{0:T(128)S(1)} %pad_add_fusion.place_ref, bf16[128,512]{1,0:T(8,128)(2,1)S(1)} %queries.4.q_ref, bf16[128,256]{1,0:T(8,128)(2,1)S(1)} %collective-permute-done.4.refs_0_, bf16[128,256]{1,0:T(8,128)(2,1)S(1)} %collective-permute-done.8.refs_1_.refs_0_, ...), custom_call_target="tpu_custom_call" | custom-call | flops 469762048 | bytes 2097152 | tf_op jit(solution)/shard_map/attention/pallas_call | solution.py:338
  53.1 0.6 collective-permute-start.9
  53.7 0.6 split_add.3
  54.3 1.6 %collective-permute-start.12 = (bf16[128,512]{1,0:T(8,128)(2,1)S(1)}, bf16[128,512]{1,0:T(8,128)(2,1)S(1)}, u32[]{:S(2)}, u32[]{:S(2)}) collective-permute-start(bf16[128,512]{1,0:T(8,128)(2,1)S(1)} %get-tuple-element.40), channel_id=1, source_target_pairs={{0,2},{1,3},{2,0},{3,1},{4,6},{5,7},{6,4},{7,5},{8,10},{9,11},{10,... | collective-permute-start | bytes 393224 | tf_op jit(solution)/shard_map/ppermute | solution.py:296
  55.9 0.6 split_add.2
  56.5 0.6 collective-permute-start.10
  57.1 3.6 %collective-permute-done.12.refs_5_ = bf16[128,512]{1,0:T(8,128)(2,1)S(1)} collective-permute-done((bf16[128,512]{1,0:T(8,128)(2,1)S(1)}, bf16[128,512]{1,0:T(8,128)(2,1)S(1)}, u32[]{:S(2)}, u32[]{:S(2)}) %collective-permute-start.12) | collective-permute-done | bytes 131104 | tf_op jit(solution)/shard_map/ppermute | solution.py:296
  60.7 1.9 %collective-permute-done.10.refs_2_ = bf16[128,512]{1,0:T(8,128)(2,1)S(1)} collective-permute-done((bf16[128,512]{1,0:T(8,128)(2,1)S(1)}, bf16[128,512]{1,0:T(8,128)(2,1)S(1)}, u32[]{:S(2)}, u32[]{:S(2)}) %collective-permute-start.10) | collective-permute-done | bytes 131104 | tf_op jit(solution)/shard_map/ppermute | solution.py:296
  62.6 1.3 %result.1 = bf16[256,512]{1,0:T(8,128)(2,1)} custom-call(s32[4]{0:T(128)S(1)} %pad_add_fusion.place_ref, bf16[128,1024]{1,0:T(8,128)(2,1)S(1)} %residual.2.mine_ref.refs_0_, bf16[128,512]{1,0:T(8,128)(2,1)S(1)} %get-tuple-element.34.refs_1_, bf16[128,512]{1,0:T(8,128)(2,1)S(1)} %collective-permute-done.10.refs_2_, ...), custom_call_target="tpu_custom_call" | custom-call | tf_op jit(solution)/shard_map/result/pallas_call | solution.py:472
  (32 shorter events, 0.5 us)
Async XLA Ops:
  0.0 10.4 %copy-start.8 = (f32[2,8,257]{2,1,0:T(8,128)S(1)}, f32[2,8,257]{2,1,0:T(8,128)}, u32[]{:S(2)}) copy-start(f32[2,8,257]{2,1,0:T(8,128)} %table_ref.3) | copy-start | bytes 49348
  2.5 8.8 %collective-permute-start = (bf16[256,256]{1,0:T(8,128)(2,1)S(1)}, bf16[256,256]{1,0:T(8,128)(2,1)S(1)}, u32[]{:S(2)}, u32[]{:S(2)}) collective-permute-start(bf16[256,256]{1,0:T(8,128)(2,1)S(1)} %get-tuple-element.24.refs_2_.refs_1_), channel_id=1, source_target_pairs={{0,4},{4,8},{8,12},{12,16},{16,20},{20,24},{24,28},{1,5},{5,9},{9,... | collective-permute-start | bytes 393224 | tf_op jit(solution)/shard_map/ppermute | solution.py:300
  7.4 0.7 %copy-start.6 = (f32[2,64]{1,0:T(2,128)S(1)}, f32[2,64]{1,0:T(2,128)}, u32[]{:S(2)}) copy-start(f32[2,64]{1,0:T(2,128)} %qg_ref.5) | copy-start | bytes 1540
  14.8 13.5 %copy-start.1 = (bf16[256,2048]{1,0:T(8,128)(2,1)S(1)}, bf16[256,2048]{1,0:T(8,128)(2,1)}, u32[]{:S(2)}) copy-start(bf16[256,2048]{1,0:T(8,128)(2,1)} %x_ref.3) | copy-start | bytes 3145732
  14.8 4.2 %collective-permute-start.5 = (bf16[128,1024]{1,0:T(8,128)(2,1)S(1)}, bf16[128,1024]{1,0:T(8,128)(2,1)S(1)}, u32[]{:S(2)}, u32[]{:S(2)}) collective-permute-start(bf16[128,1024]{1,0:T(8,128)(2,1)S(1)} %get-tuple-element.30), channel_id=1, source_target_pairs={{0,1},{1,0},{2,3},{3,2},{4,5},{5,4},{6,7},{7,6},{8,9},{9,8},{10,11... | collective-permute-start | bytes 786440 | tf_op jit(solution)/shard_map/ppermute | solution.py:296
  18.4 15.3 %copy-start.2 = (bf16[2,2048,128]{2,1,0:T(8,128)(2,1)S(1)}, bf16[2,2048,128]{2,1,0:T(8,128)(2,1)}, u32[]{:S(2)}) copy-start(bf16[2,2048,128]{2,1,0:T(8,128)(2,1)} %wk_ref.3) | copy-start | bytes 3145732
  18.4 15.3 %copy-start.3 = (bf16[2,2048,128]{2,1,0:T(8,128)(2,1)S(1)}, bf16[2,2048,128]{2,1,0:T(8,128)(2,1)}, u32[]{:S(2)}) copy-start(bf16[2,2048,128]{2,1,0:T(8,128)(2,1)} %wv_ref.3) | copy-start | bytes 3145732
  18.4 15.3 %copy-start.4 = (f32[2,2048]{1,0:T(2,128)S(1)}, f32[2,2048]{1,0:T(2,128)}, u32[]{:S(2)}) copy-start(f32[2,2048]{1,0:T(2,128)} %gain_ref.3) | copy-start | bytes 49156
  18.4 15.3 %copy-start.5 = (f32[2,64]{1,0:T(2,128)S(1)}, f32[2,64]{1,0:T(2,128)}, u32[]{:S(2)}) copy-start(f32[2,64]{1,0:T(2,128)} %kg_ref.3) | copy-start | bytes 1540
  18.4 2.2 %collective-permute-start.1 = (bf16[128,1024]{1,0:T(8,128)(2,1)S(1)}, bf16[128,1024]{1,0:T(8,128)(2,1)S(1)}, u32[]{:S(2)}, u32[]{:S(2)}) collective-permute-start(bf16[128,1024]{1,0:T(8,128)(2,1)S(1)} %get-tuple-element.26), channel_id=1, source_target_pairs={{0,1},{1,0},{2,3},{3,2},{4,5},{5,4},{6,7},{7,6},{8,9},{9,8},{10,11... | collective-permute-start | bytes 786440 | tf_op jit(solution)/shard_map/ppermute | solution.py:296
  19.0 9.2 %collective-permute-start.6 = (bf16[128,1024]{1,0:T(8,128)(2,1)S(1)}, bf16[128,1024]{1,0:T(8,128)(2,1)S(1)}, u32[]{:S(2)}, u32[]{:S(2)}) collective-permute-start(bf16[128,1024]{1,0:T(8,128)(2,1)S(1)} %add.15.a_ref), channel_id=1, source_target_pairs={{0,2},{1,3},{2,0},{3,1},{4,6},{5,7},{6,4},{7,5},{8,10},{9,11},{10,... | collective-permute-start | bytes 786440 | tf_op jit(solution)/shard_map/ppermute | solution.py:296
  20.6 12.3 %collective-permute-start.2 = (bf16[128,1024]{1,0:T(8,128)(2,1)S(1)}, bf16[128,1024]{1,0:T(8,128)(2,1)S(1)}, u32[]{:S(2)}, u32[]{:S(2)}) collective-permute-start(bf16[128,1024]{1,0:T(8,128)(2,1)S(1)} %add.14.a_ref), channel_id=1, source_target_pairs={{0,2},{1,3},{2,0},{3,1},{4,6},{5,7},{6,4},{7,5},{8,10},{9,11},{10,... | collective-permute-start | bytes 786440 | tf_op jit(solution)/shard_map/ppermute | solution.py:296
  28.9 15.8 %copy-start = (bf16[2,2048,512]{2,1,0:T(8,128)(2,1)S(1)}, bf16[2,2048,512]{2,1,0:T(8,128)(2,1)}, u32[]{:S(2)}) copy-start(bf16[2,2048,512]{2,1,0:T(8,128)(2,1)} %wq_ref.3) | copy-start | bytes 12582916
  28.9 15.8 %copy-start.7 = (f32[2,64]{1,0:T(2,128)S(1)}, f32[2,64]{1,0:T(2,128)}, u32[]{:S(2)}) copy-start(f32[2,64]{1,0:T(2,128)} %qg_ref.5) | copy-start | bytes 1540
  29.0 4.7 %collective-permute-start.7 = (bf16[128,1024]{1,0:T(8,128)(2,1)S(1)}, bf16[128,1024]{1,0:T(8,128)(2,1)S(1)}, u32[]{:S(2)}, u32[]{:S(2)}) collective-permute-start(bf16[128,1024]{1,0:T(8,128)(2,1)S(1)} %residual.3.mine_ref.refs_3_), channel_id=1, source_target_pairs={{0,1},{1,0},{2,3},{3,2},{4,5},{5,4},{6,7},{7,6},{8,9},{9,8},{10,11... | collective-permute-start | bytes 786440 | tf_op jit(solution)/shard_map/ppermute | solution.py:296
  33.6 5.6 %collective-permute-start.3 = (bf16[128,1024]{1,0:T(8,128)(2,1)S(1)}, bf16[128,1024]{1,0:T(8,128)(2,1)S(1)}, u32[]{:S(2)}, u32[]{:S(2)}) collective-permute-start(bf16[128,1024]{1,0:T(8,128)(2,1)S(1)} %residual.2.mine_ref.refs_0_), channel_id=1, source_target_pairs={{0,1},{1,0},{2,3},{3,2},{4,5},{5,4},{6,7},{7,6},{8,9},{9,8},{10,11... | collective-permute-start | bytes 786440 | tf_op jit(solution)/shard_map/ppermute | solution.py:296
  35.0 11.2 %collective-permute-start.8 = (bf16[128,256]{1,0:T(8,128)(2,1)S(1)}, bf16[128,256]{1,0:T(8,128)(2,1)S(1)}, u32[]{:S(2)}, u32[]{:S(2)}) collective-permute-start(bf16[128,256]{1,0:T(8,128)(2,1)S(1)} %get-tuple-element.31.refs_2_), channel_id=1, source_target_pairs={{0,4},{4,8},{8,12},{12,16},{16,20},{20,24},{24,28},{1,5},{5,9},{9,... | collective-permute-start | bytes 196616 | tf_op jit(solution)/shard_map/ppermute | solution.py:300
  40.5 9.2 %collective-permute-start.4 = (bf16[128,256]{1,0:T(8,128)(2,1)S(1)}, bf16[128,256]{1,0:T(8,128)(2,1)S(1)}, u32[]{:S(2)}, u32[]{:S(2)}) collective-permute-start(bf16[128,256]{1,0:T(8,128)(2,1)S(1)} %get-tuple-element.28.refs_2_.refs_1_), channel_id=1, source_target_pairs={{0,4},{4,8},{8,12},{12,16},{16,20},{20,24},{24,28},{1,5},{5,9},{9,... | collective-permute-start | bytes 196616 | tf_op jit(solution)/shard_map/ppermute | solution.py:300
  49.6 4.1 %collective-permute-start.11 = (bf16[128,1024]{1,0:T(8,128)(2,1)S(1)}, bf16[128,1024]{1,0:T(8,128)(2,1)S(1)}, u32[]{:S(2)}, u32[]{:S(2)}) collective-permute-start(bf16[128,1024]{1,0:T(8,128)(2,1)S(1)} %get-tuple-element.38), channel_id=1, source_target_pairs={{0,1},{1,0},{2,3},{3,2},{4,5},{5,4},{6,7},{7,6},{8,9},{9,8},{10,11... | collective-permute-start | bytes 786440 | tf_op jit(solution)/shard_map/ppermute | solution.py:296
  53.1 2.7 %collective-permute-start.9 = (bf16[128,1024]{1,0:T(8,128)(2,1)S(1)}, bf16[128,1024]{1,0:T(8,128)(2,1)S(1)}, u32[]{:S(2)}, u32[]{:S(2)}) collective-permute-start(bf16[128,1024]{1,0:T(8,128)(2,1)S(1)} %get-tuple-element.33), channel_id=1, source_target_pairs={{0,1},{1,0},{2,3},{3,2},{4,5},{5,4},{6,7},{7,6},{8,9},{9,8},{10,11... | collective-permute-start | bytes 786440 | tf_op jit(solution)/shard_map/ppermute | solution.py:296
  54.3 6.4 %collective-permute-start.12 = (bf16[128,512]{1,0:T(8,128)(2,1)S(1)}, bf16[128,512]{1,0:T(8,128)(2,1)S(1)}, u32[]{:S(2)}, u32[]{:S(2)}) collective-permute-start(bf16[128,512]{1,0:T(8,128)(2,1)S(1)} %get-tuple-element.40), channel_id=1, source_target_pairs={{0,2},{1,3},{2,0},{3,1},{4,6},{5,7},{6,4},{7,5},{8,10},{9,11},{10,... | collective-permute-start | bytes 393224 | tf_op jit(solution)/shard_map/ppermute | solution.py:296
  56.5 6.1 %collective-permute-start.10 = (bf16[128,512]{1,0:T(8,128)(2,1)S(1)}, bf16[128,512]{1,0:T(8,128)(2,1)S(1)}, u32[]{:S(2)}, u32[]{:S(2)}) collective-permute-start(bf16[128,512]{1,0:T(8,128)(2,1)S(1)} %get-tuple-element.35), channel_id=1, source_target_pairs={{0,2},{1,3},{2,0},{3,1},{4,6},{5,7},{6,4},{7,5},{8,10},{9,11},{10,... | collective-permute-start | bytes 393224 | tf_op jit(solution)/shard_map/ppermute | solution.py:296

commit v3 on v2

--- a/solution.py
+++ b/solution.py
@@ -28,7 +28,6 @@
 f32 = jnp.float32
 
 whole = pl.BlockSpec(memory_space=pltpu.VMEM)
-scalar = pl.BlockSpec(memory_space=pltpu.SMEM)
 in_hbm = pl.BlockSpec(memory_space=pltpu.HBM)
 
 
@@ -72,7 +71,7 @@
 
 
 def first_norm_kernel(
-    x_hbm, gain_hbm, wk_hbm, wv_hbm, kg_hbm, normed_ref, kv_ref,
+    x_hbm, gain_hbm, wk_hbm, wv_hbm, kg_hbm, table_hbm, normed_ref, kv_ref, table_ref,
     x_ref, gain_ref, wk_ref, wv_ref, kg_ref, row_sems, sems,
 ):
     steps = row_sems.shape[0]
@@ -88,6 +87,7 @@
         pltpu.make_async_copy(wk_hbm.at[0], wk_ref, sems.at[1]),
         pltpu.make_async_copy(wv_hbm.at[0], wv_ref, sems.at[2]),
         pltpu.make_async_copy(kg_hbm, kg_ref, sems.at[3]),
+        pltpu.make_async_copy(table_hbm, table_ref, sems.at[4]),
     ]
     for copy in [gain_copy] + row_copies + late:
         copy.start()
@@ -105,10 +105,10 @@
 
 
 def next_norm_kernel(
-    layer_index, block, place_ref, mine_ref, other_ref, gain_ref, wk_ref, wv_ref, kg_ref,
+    layer_index, block, mine_ref, other_ref, gain_ref, wk_ref, wv_ref, kg_ref,
     normed_ref, kv_ref,
 ):
-    parity = place_ref[1]
+    parity = lax.axis_index("tp") % 2
     mine = mine_ref[...].astype(f32)
     other = other_ref[...].astype(f32)
     total = jnp.sum(mine * mine, axis=-1, keepdims=True)
@@ -124,23 +124,6 @@
         normed_ref[...], wk_ref[layer_index], wv_ref[layer_index],
         kg_ref[layer_index : layer_index + 1, :], kv_ref,
     )
-
-
-def first_query_kernel(normed_ref, wq_hbm, qg_ref, q_ref, wq_ref, sems):
-    share = wq_ref.shape[0] // sems.shape[0]
-    copies = []
-    for index in range(sems.shape[0]):
-        at = pl.ds(index * share, share)
-        copy = pltpu.make_async_copy(wq_hbm.at[0, at, :], wq_ref.at[at, :], sems.at[index])
-        copy.start()
-        copies.append(copy)
-    flat = None
-    for index, copy in enumerate(copies):
-        copy.wait()
-        at = slice(index * share, (index + 1) * share)
-        piece = jnp.dot(normed_ref[:, at], wq_ref[at, :], preferred_element_type=f32)
-        flat = piece if flat is None else flat + piece
-    query_body(flat, qg_ref[0:1, :], q_ref)
 
 
 def query_kernel(layer_index, normed_ref, wq_ref, qg_ref, q_ref):
@@ -176,16 +159,14 @@
 
 
 def attention_kernel(
-    block, layer_index, q_start, starts, prior, place_ref, q_ref, *refs,
+    block, layer_index, q_start, starts, prior, q_ref, *refs,
 ):
     piece_refs = refs[:PIECES]
     (
-        tile_ref, wout_hbm, keep_ref, send_ref,
-        keys_ref, even_ref, odd_ref, mixed_ref, wout_ref, sem,
+        tile_ref, wout_ref, keep_ref, send_ref,
+        keys_ref, even_ref, odd_ref, mixed_ref,
     ) = refs[PIECES:]
-    wout_copy = pltpu.make_async_copy(wout_hbm.at[layer_index], wout_ref, sem.at[0])
-    wout_copy.start()
-    first, parity = place_ref[0], place_ref[1]
+    parity = lax.axis_index("tp") % 2
     heads = q_ref.shape[1] // HEAD_DIM
     kv_width = piece_refs[0].shape[1] // 2
     kv_heads = kv_width // HEAD_DIM
@@ -207,7 +188,7 @@
             odd_ref[kv, into, :] = jnp.where(low, 1.0, value).astype(bf16)
 
     key_index = lax.broadcasted_iota(jnp.int32, (1, WINDOW), 1)
-    outside = jnp.where((key_index < prior * CHUNK) & (first == 1), masked_score, 0.0)
+    outside = jnp.where((key_index < prior * CHUNK) & (lax.axis_index("sp") == 0), masked_score, 0.0)
     for kv in range(kv_heads):
         evens, odds = [], []
         for pair in range(pairs):
@@ -242,11 +223,10 @@
             mixed_ref[:, at : at + LANES] = (jnp.where(low, upper, lower) / total).astype(bf16)
 
     mixed = mixed_ref[...]
-    wout_copy.wait()
     for index in range(keep_ref.shape[1] // block):
         for target, side in ((send_ref, 1 - parity), (keep_ref, parity)):
             cols = pl.ds(pl.multiple_of((2 * index + side) * block, LANES), block)
-            partial_value = jnp.dot(mixed, wout_ref[:, cols], preferred_element_type=f32)
+            partial_value = jnp.dot(mixed, wout_ref[layer_index, :, cols], preferred_element_type=f32)
             target[:, index * block : (index + 1) * block] = partial_value.astype(bf16)
 
 
@@ -254,8 +234,8 @@
     out_ref[...] = (a_ref[...].astype(f32) + b_ref[...].astype(f32)).astype(bf16)
 
 
-def split_add_kernel(block, bit, place_ref, a_ref, b_ref, keep_ref, send_ref):
-    parity = place_ref[bit]
+def split_add_kernel(block, bit, a_ref, b_ref, keep_ref, send_ref):
+    parity = (lax.axis_index("tp") >> bit) & 1
     for index in range(keep_ref.shape[1] // block):
         into = slice(index * block, (index + 1) * block)
         for target, side in ((send_ref, 1 - parity), (keep_ref, parity)):
@@ -265,18 +245,19 @@
             ).astype(bf16)
 
 
-def residual_kernel(block, start, place_ref, x_ref, a_ref, b_ref, out_ref):
+def residual_kernel(block, start, x_ref, a_ref, b_ref, out_ref):
     rows = slice(start, start + out_ref.shape[0])
+    parity = lax.axis_index("tp") % 2
     for index in range(out_ref.shape[1] // block):
         into = slice(index * block, (index + 1) * block)
-        cols = pl.ds(pl.multiple_of((2 * index + place_ref[1]) * block, LANES), block)
+        cols = pl.ds(pl.multiple_of((2 * index + parity) * block, LANES), block)
         added = a_ref[:, into].astype(f32) + b_ref[:, into].astype(f32)
         out_ref[:, into] = (x_ref[rows, cols].astype(f32) + added).astype(bf16)
 
 
-def result_kernel(block, at, parts, place_ref, *refs):
+def result_kernel(block, parts, *refs):
     ins, out_hbm, held_ref, sems = refs[: 3 * parts], refs[-3], refs[-2], refs[-1]
-    cols = pl.ds(pl.multiple_of(place_ref[at] * block, LANES), block)
+    cols = pl.ds(pl.multiple_of((lax.axis_index("tp") // 2) * block, LANES), block)
     copies = []
     for part in range(parts):
         x_ref, a_ref, b_ref = ins[3 * part : 3 * part + 3]
@@ -315,12 +296,6 @@
     kv_heads = kv_width // HEAD_DIM
     parts = rows // CHUNK
     order = list(reversed(range(parts)))
-    tp_index = lax.axis_index("tp")
-    place = jnp.stack(
-        [(lax.axis_index("sp") == 0).astype(jnp.int32), tp_index % 2]
-        + [(tp_index >> bit) & 1 for bit in range(1, bits)]
-        + [tp_index // 2]
-    ).astype(jnp.int32)
 
     def queries(layer_index, normed):
         count = normed.shape[0]
@@ -330,7 +305,7 @@
             in_specs=[whole] * 3,
             out_specs=whole,
             compiler_params=params(),
-            cost_estimate=cost(2 * count * width * query_width, 2 * width * query_width),
+            cost_estimate=cost(2e9, 2 * width * query_width),
             name="queries",
         )(normed, w_query, query_gain)
 
@@ -341,28 +316,28 @@
                 max(0, PIECES - 1 - part),
             ),
             out_shape=[out((CHUNK, half))] * 2,
-            in_specs=[scalar, whole] + [whole] * PIECES + [whole, in_hbm],
+            in_specs=[whole] * (PIECES + 3),
             out_specs=[whole, whole],
             scratch_shapes=[
                 pltpu.VMEM((kv_heads, WINDOW, LANES), bf16),
                 pltpu.VMEM((kv_heads, WINDOW, LANES), bf16),
                 pltpu.VMEM((kv_heads, WINDOW, LANES), bf16),
                 pltpu.VMEM((CHUNK, query_width), bf16),
-                pltpu.VMEM((query_width, width), bf16),
-                pltpu.SemaphoreType.DMA((1,)),
             ],
             compiler_params=params(),
             cost_estimate=cost(
                 2 * CHUNK * query_width * (width + 4 * WINDOW), 2 * width * query_width
             ),
             name="attention",
-        )(place, query, *pieces, tiles[layer_index], *kept_in_hbm(w_out))
-
-    normed, kv = pl.pallas_call(
+        )(query, *pieces, tiles[layer_index], w_out)
+
+    normed, kv, table = pl.pallas_call(
         first_norm_kernel,
-        out_shape=[out((rows, width)), out((rows, 2 * kv_width))],
-        in_specs=[in_hbm] * 5,
-        out_specs=[whole, whole],
+        out_shape=[
+            out((rows, width)), out((rows, 2 * kv_width)), out(rel_bias.shape, f32)
+        ],
+        in_specs=[in_hbm] * 6,
+        out_specs=[whole] * 3,
         scratch_shapes=[
             pltpu.VMEM(stream.shape, bf16),
             pltpu.VMEM(attn_gain.shape, f32),
@@ -370,26 +345,14 @@
             pltpu.VMEM((width, kv_width), bf16),
             pltpu.VMEM(key_gain.shape, f32),
             pltpu.SemaphoreType.DMA((4,)),
-            pltpu.SemaphoreType.DMA((4,)),
+            pltpu.SemaphoreType.DMA((5,)),
         ],
         compiler_params=params(),
-        cost_estimate=cost(4 * rows * width * kv_width, 4 * rows * width),
+        cost_estimate=cost(3e9, 4 * rows * width),
         name="norm_kv_first",
-    )(*kept_in_hbm(stream, attn_gain, w_key, w_value, key_gain))
+    )(*kept_in_hbm(stream, attn_gain, w_key, w_value, key_gain, rel_bias))
     kv_prior = passed_along(kv[rows - REACH :])
-    query = pl.pallas_call(
-        first_query_kernel,
-        out_shape=out((rows, query_width)),
-        in_specs=[whole, in_hbm, whole],
-        out_specs=whole,
-        scratch_shapes=[
-            pltpu.VMEM((width, query_width), bf16),
-            pltpu.SemaphoreType.DMA((4,)),
-        ],
-        compiler_params=params(),
-        cost_estimate=cost(2 * rows * width * query_width, 2 * width * query_width),
-        name="queries",
-    )(normed, *kept_in_hbm(w_query), query_gain)
+    query = queries(0, normed)
     tiles = []
     for layer_index in range(LAYERS):
         tiles.append(
@@ -399,9 +362,9 @@
                 in_specs=[whole],
                 out_specs=whole,
                 compiler_params=params(),
-                cost_estimate=cost(5e8, 1e6),
+                cost_estimate=cost(2e9, 1e6),
                 name="bias_tiles",
-            )(rel_bias)
+            )(table)
         )
 
     mine, other, kvs, normeds = {}, {}, {}, {}
@@ -426,11 +389,11 @@
         mine[part] = pl.pallas_call(
             functools.partial(residual_kernel, block, part * CHUNK),
             out_shape=out((CHUNK, half)),
-            in_specs=[scalar, whole, whole, whole],
+            in_specs=[whole, whole, whole],
             out_specs=whole,
             compiler_params=params(),
             name="residual",
-        )(place, stream, keep, received)
+        )(stream, keep, received)
         other[part] = swapped(mine[part], 0)
 
     priors = {}
@@ -438,12 +401,12 @@
         normeds[part], kvs[part] = pl.pallas_call(
             functools.partial(next_norm_kernel, 1, block),
             out_shape=[out((CHUNK, width)), out((CHUNK, 2 * kv_width))],
-            in_specs=[scalar] + [whole] * 6,
+            in_specs=[whole] * 6,
             out_specs=[whole, whole],
             compiler_params=params(),
             cost_estimate=cost(4 * CHUNK * width * kv_width, 4 * CHUNK * width),
             name="norm_kv_next",
-        )(place, mine[part], other[part], attn_gain, w_key, w_value, key_gain)
+        )(mine[part], other[part], attn_gain, w_key, w_value, key_gain)
         if part >= parts - (PIECES - 1):
             priors[part - parts] = passed_along(kvs[part])
 
@@ -459,20 +422,20 @@
         for bit in range(1, bits):
             left = keep.shape[1] // 2
             keep, send = pl.pallas_call(
-                functools.partial(split_add_kernel, block, 1 + bit),
+                functools.partial(split_add_kernel, block, bit),
                 out_shape=[out((CHUNK, left))] * 2,
-                in_specs=[scalar, whole, whole],
+                in_specs=[whole, whole],
                 out_specs=[whole, whole],
                 compiler_params=params(),
                 name="split_add",
-            )(place, keep, received)
+            )(keep, received)
             received = swapped(send, bit)
         outs[part] = (mine[part], keep, received)
 
     return pl.pallas_call(
-        functools.partial(result_kernel, block, bits + 1, parts),
+        functools.partial(result_kernel, block, parts),
         out_shape=out((rows, block)),
-        in_specs=[scalar] + [whole] * (3 * parts),
+        in_specs=[whole] * (3 * parts),
         out_specs=in_hbm,
         scratch_shapes=[
             pltpu.VMEM((rows, block), bf16),
@@ -480,7 +443,7 @@
         ],
         compiler_params=params(),
         name="result",
-    )(place, *[ref for part in range(parts) for ref in outs[part]])
+    )(*[ref for part in range(parts) for ref in outs[part]])
 
 
 def solution(mesh):

time: 64.4 us -> 54.3 us (0.84)
  Pallas kernels: 27.9 us -> 15.2 us
  starting transfers between devices: 18.8 us -> 20.5 us
  waiting for transfers between devices: 16 us -> 17.5 us
    pallas_call x4, Pallas kernels: 13.7 us -> 6.14 us  [attention(): pl.pallas_call(functools.partial(attention_kernel, block, layer_index, q_...]
    pallas_call x4 -> x3, Pallas kernels: 4.84 us -> 0.89 us  [the longest x1 0.77 us: layers(): pl.pallas_call(functools.partial(result_kernel, block, parts), out_shape=...]
    ppermute x3, starting transfers between devices: 12.6 us -> 13.8 us  [passed_along(): lax.ppermute(value, 'sp', [(d, d + 1) for d in range(lax.axis_size('sp')...]
    pallas_call x2, Pallas kernels: 2.51 us -> 1.34 us  [layers(): pl.pallas_call(functools.partial(next_norm_kernel, 1, block), out_shape=[...]
    pallas_call x2, Pallas kernels: 1.28 us -> 0.19 us  [layers(): pl.pallas_call(functools.partial(residual_kernel, block, part * CHUNK), o...]
    pallas_call x2 -> x3, Pallas kernels: 1.38 us -> 2.36 us  [queries(): pl.pallas_call(functools.partial(query_kernel, layer_index), out_shape=ou...]
    ppermute x3, waiting for transfers between devices: 0.01 us -> 0.94 us  [passed_along(): lax.ppermute(value, 'sp', [(d, d + 1) for d in range(lax.axis_size('sp')...]
  transfers between devices with their start and end apart: 13 -> 13, of which waited for: 4 -> 5; matrix products, arithmetic and copies ran while one was open for 0% -> 0% of each run, Pallas kernels for 32% -> 19%
where the time goes in v3:
time: 54.3 us; the launch traced here: 54 us
  starting transfers between devices  20.5 us (38%)
  waiting for transfers between devices  17.5 us (32%)
  Pallas kernels  15.2 us (28%)
    ppermute x10, waiting for transfers between devices, swapped(): return lax.ppermute(value, 'tp', [(d, d ^ 1 << bit) for d in range(size)])  16.6 us
    ppermute x3, starting transfers between devices, passed_along(): lax.ppermute(value, 'sp', [(d, d + 1) for d in range(lax.axis_size('sp')...  13.8 us
    ppermute x10, starting transfers between devices, swapped(): return lax.ppermute(value, 'tp', [(d, d ^ 1 << bit) for d in range(size)])  6.68 us
    pallas_call x4, Pallas kernels, attention(): pl.pallas_call(functools.partial(attention_kernel, block, layer_index, q_...  6.14 us
    pallas_call x1, Pallas kernels, layers(): pl.pallas_call(first_norm_kernel, out_shape=[out((rows, width)), out((row...  2.61 us
    pallas_call x3, Pallas kernels, queries(): pl.pallas_call(functools.partial(query_kernel, layer_index), out_shape=ou...  2.36 us
    pallas_call x2, Pallas kernels, layers(): pl.pallas_call(functools.partial(bias_kernel, layer_index), out_shape=out...  1.55 us
    pallas_call x2, Pallas kernels, layers(): pl.pallas_call(functools.partial(next_norm_kernel, 1, block), out_shape=[...  1.34 us
  transfers between devices with their start and end apart: 13, of which 5 were waited for; matrix products, arithmetic and copies ran while one was open for 0% of the time, Pallas kernels for 19%

profile of v3, /device:TPU:0, one launch (start us, length us, event | category | flops | bytes accessed | tf_op | source)
XLA Modules:
  0.0 54.0 jit_solution(7483917334532734602)
XLA Ops:
  0.0 2.6 %norm_kv_first.1 = (bf16[256,2048]{1,0:T(8,128)(2,1)S(1)}, bf16[256,256]{1,0:T(8,128)(2,1)S(1)}, f32[2,8,257]{2,1,0:T(8,128)S(1)}) custom-call(bf16[256,2048]{1,0:T(8,128)(2,1)} %x_ref.3, f32[2,2048]{1,0:T(2,128)} %gain_ref.3, bf16[2,2048,128]{2,1,0:T(8,128)(2,1)} %wk_ref.3, bf16[2,2048,128]{2,1,0:T(8,128)(2,1)} %wv_ref.3, f32[2,64]{1,0:T(2,128)} %kg_ref.3, ...), custom_call_target="tpu_custom_call" | custom-call | flops 3000000000 | bytes 2097152 | tf_op jit(solution)/shard_map/norm_kv_first/pallas_call | solution.py:334
  2.6 5.2 %collective-permute-start = (bf16[256,256]{1,0:T(8,128)(2,1)S(1)}, bf16[256,256]{1,0:T(8,128)(2,1)S(1)}, u32[]{:S(2)}, u32[]{:S(2)}) collective-permute-start(bf16[256,256]{1,0:T(8,128)(2,1)S(1)} %get-tuple-element.25.refs_2_.refs_1_), channel_id=1, source_target_pairs={{0,4},{4,8},{8,12},{12,16},{16,20},{20,24},{24,28},{1,5},{5,9},{9,... | collective-permute-start | bytes 393224 | tf_op jit(solution)/shard_map/ppermute | solution.py:281
  7.8 0.8 %bias_tiles.2.refs_3_ = f32[8,128,384]{2,1,0:T(8,128)S(1)} custom-call(f32[2,8,257]{2,1,0:T(8,128)S(1)} %get-tuple-element.26.table_ref), custom_call_target="tpu_custom_call" | custom-call | flops 2000000000 | bytes 1000000 | tf_op jit(solution)/shard_map/bias_tiles/pallas_call | solution.py:359
  8.6 1.0 %queries.3.q_ref = bf16[256,512]{1,0:T(8,128)(2,1)S(1)} custom-call(bf16[256,2048]{1,0:T(8,128)(2,1)S(1)} %get-tuple-element.24.normed_ref, bf16[2,2048,512]{2,1,0:T(8,128)(2,1)S(1)} %copy-done.6, f32[2,64]{1,0:T(2,128)S(1)} %copy-done.7), custom_call_target="tpu_custom_call" | custom-call | flops 2000000000 | bytes 2097152 | tf_op jit(solution)/shard_map/queries/pallas_call | solution.py:302
  9.6 0.9 %collective-permute-done.refs_0_.refs_1_ = bf16[256,256]{1,0:T(8,128)(2,1)S(1)} collective-permute-done((bf16[256,256]{1,0:T(8,128)(2,1)S(1)}, bf16[256,256]{1,0:T(8,128)(2,1)S(1)}, u32[]{:S(2)}, u32[]{:S(2)}) %collective-permute-start) | collective-permute-done | bytes 131104 | tf_op jit(solution)/shard_map/ppermute | solution.py:281
  10.5 0.2 copy-done
  10.8 1.5 %attention.5 = (bf16[128,1024]{1,0:T(8,128)(2,1)S(1)}, bf16[128,1024]{1,0:T(8,128)(2,1)S(1)}) custom-call(bf16[256,512]{1,0:T(8,128)(2,1)S(1)} %queries.3.q_ref, bf16[256,256]{1,0:T(8,128)(2,1)S(1)} %collective-permute-done.refs_0_.refs_1_, bf16[256,256]{1,0:T(8,128)(2,1)S(1)} %get-tuple-element.25.refs_2_.refs_1_, ...), custom_call_target="tpu_custom_call" | custom-call | flops 469762048 | bytes 2097152 | tf_op jit(solution)/shard_map/attention/pallas_call | solution.py:313
  12.3 0.1 collective-permute-start.5
  12.4 1.5 %attention.4 = (bf16[128,1024]{1,0:T(8,128)(2,1)S(1)}, bf16[128,1024]{1,0:T(8,128)(2,1)S(1)}) custom-call(bf16[256,512]{1,0:T(8,128)(2,1)S(1)} %queries.3.q_ref, bf16[256,256]{1,0:T(8,128)(2,1)S(1)} %collective-permute-done.refs_0_.refs_1_, bf16[256,256]{1,0:T(8,128)(2,1)S(1)} %collective-permute-done.refs_0_.refs_1_, ...), custom_call_target="tpu_custom_call" | custom-call | flops 469762048 | bytes 2097152 | tf_op jit(solution)/shard_map/attention/pallas_call | solution.py:313
  14.0 0.5 %collective-permute-start.1 = (bf16[128,1024]{1,0:T(8,128)(2,1)S(1)}, bf16[128,1024]{1,0:T(8,128)(2,1)S(1)}, u32[]{:S(2)}, u32[]{:S(2)}) collective-permute-start(bf16[128,1024]{1,0:T(8,128)(2,1)S(1)} %get-tuple-element.28), channel_id=1, source_target_pairs={{0,1},{1,0},{2,3},{3,2},{4,5},{5,4},{6,7},{7,6},{8,9},{9,8},{10,11... | collective-permute-start | bytes 786440 | tf_op jit(solution)/shard_map/ppermute | solution.py:277
  14.6 1.6 %collective-permute-start.6 = (bf16[128,1024]{1,0:T(8,128)(2,1)S(1)}, bf16[128,1024]{1,0:T(8,128)(2,1)S(1)}, u32[]{:S(2)}, u32[]{:S(2)}) collective-permute-start(bf16[128,1024]{1,0:T(8,128)(2,1)S(1)} %add.3.a_ref), channel_id=1, source_target_pairs={{0,2},{1,3},{2,0},{3,1},{4,6},{5,7},{6,4},{7,5},{8,10},{9,11},{10,... | collective-permute-start | bytes 786440 | tf_op jit(solution)/shard_map/ppermute | solution.py:277
  16.2 1.1 %collective-permute-start.2 = (bf16[128,1024]{1,0:T(8,128)(2,1)S(1)}, bf16[128,1024]{1,0:T(8,128)(2,1)S(1)}, u32[]{:S(2)}, u32[]{:S(2)}) collective-permute-start(bf16[128,1024]{1,0:T(8,128)(2,1)S(1)} %add.2.a_ref), channel_id=1, source_target_pairs={{0,2},{1,3},{2,0},{3,1},{4,6},{5,7},{6,4},{7,5},{8,10},{9,11},{10,... | collective-permute-start | bytes 786440 | tf_op jit(solution)/shard_map/ppermute | solution.py:277
  17.3 6.5 %collective-permute-done.6.b_ref = bf16[128,1024]{1,0:T(8,128)(2,1)S(1)} collective-permute-done((bf16[128,1024]{1,0:T(8,128)(2,1)S(1)}, bf16[128,1024]{1,0:T(8,128)(2,1)S(1)}, u32[]{:S(2)}, u32[]{:S(2)}) %collective-permute-start.6) | collective-permute-done | bytes 262176 | tf_op jit(solution)/shard_map/ppermute | solution.py:277
  23.8 0.1 residual.3.mine_ref.refs_3_
  24.1 4.4 %collective-permute-done.2.b_ref = bf16[128,1024]{1,0:T(8,128)(2,1)S(1)} collective-permute-done((bf16[128,1024]{1,0:T(8,128)(2,1)S(1)}, bf16[128,1024]{1,0:T(8,128)(2,1)S(1)}, u32[]{:S(2)}, u32[]{:S(2)}) %collective-permute-start.2) | collective-permute-done | bytes 262176 | tf_op jit(solution)/shard_map/ppermute | solution.py:277
  28.5 0.1 residual.2.mine_ref.refs_0_
  28.6 0.1 collective-permute-start.3
  28.7 0.8 %bias_tiles.3.refs_3_ = f32[8,128,384]{2,1,0:T(8,128)S(1)} custom-call(f32[2,8,257]{2,1,0:T(8,128)S(1)} %get-tuple-element.26.table_ref), custom_call_target="tpu_custom_call" | custom-call | flops 2000000000 | bytes 1000000 | tf_op jit(solution)/shard_map/bias_tiles/pallas_call | solution.py:359
  29.5 0.7 %norm_kv_next.3 = (bf16[128,2048]{1,0:T(8,128)(2,1)S(1)}, bf16[128,256]{1,0:T(8,128)(2,1)S(1)}) custom-call(bf16[128,1024]{1,0:T(8,128)(2,1)S(1)} %residual.3.mine_ref.refs_3_, bf16[128,1024]{1,0:T(8,128)(2,1)S(1)} %collective-permute-done.7.other_ref, f32[2,2048]{1,0:T(2,128)S(1)} %copy-done.4, bf16[2,2048,128]{2,1,0:T(8,128)(2,1)S(1)} %copy-done.1, ...), custom_call_target="tpu_custom_call" | custom-call | flops 134217728 | bytes 1048576 | tf_op jit(solution)/shard_map/norm_kv_next/pallas_call | solution.py:401
  30.2 4.2 %collective-permute-start.8 = (bf16[128,256]{1,0:T(8,128)(2,1)S(1)}, bf16[128,256]{1,0:T(8,128)(2,1)S(1)}, u32[]{:S(2)}, u32[]{:S(2)}) collective-permute-start(bf16[128,256]{1,0:T(8,128)(2,1)S(1)} %get-tuple-element.33.refs_2_), channel_id=1, source_target_pairs={{0,4},{4,8},{8,12},{12,16},{16,20},{20,24},{24,28},{1,5},{5,9},{9,... | collective-permute-start | bytes 196616 | tf_op jit(solution)/shard_map/ppermute | solution.py:281
  34.4 0.7 %queries.5.q_ref = bf16[128,512]{1,0:T(8,128)(2,1)S(1)} custom-call(bf16[128,2048]{1,0:T(8,128)(2,1)S(1)} %get-tuple-element.38.normed_ref, bf16[2,2048,512]{2,1,0:T(8,128)(2,1)S(1)} %copy-done.6, f32[2,64]{1,0:T(2,128)S(1)} %copy-done.7), custom_call_target="tpu_custom_call" | custom-call | flops 2000000000 | bytes 2097152 | tf_op jit(solution)/shard_map/queries/pallas_call | solution.py:302
  35.1 0.7 %norm_kv_next.2 = (bf16[128,2048]{1,0:T(8,128)(2,1)S(1)}, bf16[128,256]{1,0:T(8,128)(2,1)S(1)}) custom-call(bf16[128,1024]{1,0:T(8,128)(2,1)S(1)} %residual.2.mine_ref.refs_0_, bf16[128,1024]{1,0:T(8,128)(2,1)S(1)} %collective-permute-done.3.other_ref, f32[2,2048]{1,0:T(2,128)S(1)} %copy-done.4, bf16[2,2048,128]{2,1,0:T(8,128)(2,1)S(1)} %copy-done.1, ...), custom_call_target="tpu_custom_call" | custom-call | flops 134217728 | bytes 1048576 | tf_op jit(solution)/shard_map/norm_kv_next/pallas_call | solution.py:401
  35.8 4.5 %collective-permute-start.4 = (bf16[128,256]{1,0:T(8,128)(2,1)S(1)}, bf16[128,256]{1,0:T(8,128)(2,1)S(1)}, u32[]{:S(2)}, u32[]{:S(2)}) collective-permute-start(bf16[128,256]{1,0:T(8,128)(2,1)S(1)} %get-tuple-element.30.refs_2_.refs_1_), channel_id=1, source_target_pairs={{0,4},{4,8},{8,12},{12,16},{16,20},{20,24},{24,28},{1,5},{5,9},{9,... | collective-permute-start | bytes 196616 | tf_op jit(solution)/shard_map/ppermute | solution.py:281
  40.3 0.7 %queries.4.q_ref = bf16[128,512]{1,0:T(8,128)(2,1)S(1)} custom-call(bf16[128,2048]{1,0:T(8,128)(2,1)S(1)} %get-tuple-element.29.normed_ref, bf16[2,2048,512]{2,1,0:T(8,128)(2,1)S(1)} %copy-done.6, f32[2,64]{1,0:T(2,128)S(1)} %copy-done.7), custom_call_target="tpu_custom_call" | custom-call | flops 2000000000 | bytes 2097152 | tf_op jit(solution)/shard_map/queries/pallas_call | solution.py:302
  41.0 1.5 %attention.7 = (bf16[128,1024]{1,0:T(8,128)(2,1)S(1)}, bf16[128,1024]{1,0:T(8,128)(2,1)S(1)}) custom-call(bf16[128,512]{1,0:T(8,128)(2,1)S(1)} %queries.5.q_ref, bf16[128,256]{1,0:T(8,128)(2,1)S(1)} %collective-permute-done.8.refs_1_.refs_0_, bf16[128,256]{1,0:T(8,128)(2,1)S(1)} %get-tuple-element.30.refs_2_.refs_1_, ...), custom_call_target="tpu_custom_call" | custom-call | flops 469762048 | bytes 2097152 | tf_op jit(solution)/shard_map/attention/pallas_call | solution.py:313
  42.6 1.5 %attention.6 = (bf16[128,1024]{1,0:T(8,128)(2,1)S(1)}, bf16[128,1024]{1,0:T(8,128)(2,1)S(1)}) custom-call(bf16[128,512]{1,0:T(8,128)(2,1)S(1)} %queries.4.q_ref, bf16[128,256]{1,0:T(8,128)(2,1)S(1)} %collective-permute-done.4.refs_0_, bf16[128,256]{1,0:T(8,128)(2,1)S(1)} %collective-permute-done.8.refs_1_.refs_0_, ...), custom_call_target="tpu_custom_call" | custom-call | flops 469762048 | bytes 2097152 | tf_op jit(solution)/shard_map/attention/pallas_call | solution.py:313
  44.2 0.6 %collective-permute-start.9 = (bf16[128,1024]{1,0:T(8,128)(2,1)S(1)}, bf16[128,1024]{1,0:T(8,128)(2,1)S(1)}, u32[]{:S(2)}, u32[]{:S(2)}) collective-permute-start(bf16[128,1024]{1,0:T(8,128)(2,1)S(1)} %get-tuple-element.35), channel_id=1, source_target_pairs={{0,1},{1,0},{2,3},{3,2},{4,5},{5,4},{6,7},{7,6},{8,9},{9,8},{10,11... | collective-permute-start | bytes 786440 | tf_op jit(solution)/shard_map/ppermute | solution.py:277
  44.8 1.6 %collective-permute-start.12 = (bf16[128,512]{1,0:T(8,128)(2,1)S(1)}, bf16[128,512]{1,0:T(8,128)(2,1)S(1)}, u32[]{:S(2)}, u32[]{:S(2)}) collective-permute-start(bf16[128,512]{1,0:T(8,128)(2,1)S(1)} %get-tuple-element.42), channel_id=1, source_target_pairs={{0,2},{1,3},{2,0},{3,1},{4,6},{5,7},{6,4},{7,5},{8,10},{9,11},{10,... | collective-permute-start | bytes 393224 | tf_op jit(solution)/shard_map/ppermute | solution.py:277
  46.4 1.1 %collective-permute-start.10 = (bf16[128,512]{1,0:T(8,128)(2,1)S(1)}, bf16[128,512]{1,0:T(8,128)(2,1)S(1)}, u32[]{:S(2)}, u32[]{:S(2)}) collective-permute-start(bf16[128,512]{1,0:T(8,128)(2,1)S(1)} %get-tuple-element.37), channel_id=1, source_target_pairs={{0,2},{1,3},{2,0},{3,1},{4,6},{5,7},{6,4},{7,5},{8,10},{9,11},{10,... | collective-permute-start | bytes 393224 | tf_op jit(solution)/shard_map/ppermute | solution.py:277
  47.5 3.7 %collective-permute-done.12.refs_5_ = bf16[128,512]{1,0:T(8,128)(2,1)S(1)} collective-permute-done((bf16[128,512]{1,0:T(8,128)(2,1)S(1)}, bf16[128,512]{1,0:T(8,128)(2,1)S(1)}, u32[]{:S(2)}, u32[]{:S(2)}) %collective-permute-start.12) | collective-permute-done | bytes 131104 | tf_op jit(solution)/shard_map/ppermute | solution.py:277
  51.2 1.9 %collective-permute-done.10.refs_2_ = bf16[128,512]{1,0:T(8,128)(2,1)S(1)} collective-permute-done((bf16[128,512]{1,0:T(8,128)(2,1)S(1)}, bf16[128,512]{1,0:T(8,128)(2,1)S(1)}, u32[]{:S(2)}, u32[]{:S(2)}) %collective-permute-start.10) | collective-permute-done | bytes 131104 | tf_op jit(solution)/shard_map/ppermute | solution.py:277
  53.1 0.8 %result.1 = bf16[256,512]{1,0:T(8,128)(2,1)} custom-call(bf16[128,1024]{1,0:T(8,128)(2,1)S(1)} %residual.2.mine_ref.refs_0_, bf16[128,512]{1,0:T(8,128)(2,1)S(1)} %get-tuple-element.36.refs_1_, bf16[128,512]{1,0:T(8,128)(2,1)S(1)} %collective-permute-done.10.refs_2_, bf16[128,1024]{1,0:T(8,128)(2,1)S(1)} %residual.3.mine_ref.refs_3_, ...), custom_call_target="tpu_custom_call" | custom-call | tf_op jit(solution)/shard_map/result/pallas_call | solution.py:435
  (29 shorter events, 0.5 us)
Async XLA Ops:
  2.6 6.0 %copy-start.6 = (bf16[2,2048,512]{2,1,0:T(8,128)(2,1)S(1)}, bf16[2,2048,512]{2,1,0:T(8,128)(2,1)}, u32[]{:S(2)}) copy-start(bf16[2,2048,512]{2,1,0:T(8,128)(2,1)} %wq_ref.5) | copy-start | bytes 12582916
  2.6 6.0 %copy-start.7 = (f32[2,64]{1,0:T(2,128)S(1)}, f32[2,64]{1,0:T(2,128)}, u32[]{:S(2)}) copy-start(f32[2,64]{1,0:T(2,128)} %qg_ref.5) | copy-start | bytes 1540
  2.6 7.9 %collective-permute-start = (bf16[256,256]{1,0:T(8,128)(2,1)S(1)}, bf16[256,256]{1,0:T(8,128)(2,1)S(1)}, u32[]{:S(2)}, u32[]{:S(2)}) collective-permute-start(bf16[256,256]{1,0:T(8,128)(2,1)S(1)} %get-tuple-element.25.refs_2_.refs_1_), channel_id=1, source_target_pairs={{0,4},{4,8},{8,12},{12,16},{16,20},{20,24},{24,28},{1,5},{5,9},{9,... | collective-permute-start | bytes 393224 | tf_op jit(solution)/shard_map/ppermute | solution.py:281
  8.6 2.2 %copy-start = (bf16[2,512,2048]{2,1,0:T(8,128)(2,1)S(1)}, bf16[2,512,2048]{2,1,0:T(8,128)(2,1)}, u32[]{:S(2)}) copy-start(bf16[2,512,2048]{2,1,0:T(8,128)(2,1)} %refs_4_.7) | copy-start | bytes 12582916
  12.3 11.5 %copy-start.3 = (bf16[256,2048]{1,0:T(8,128)(2,1)S(1)}, bf16[256,2048]{1,0:T(8,128)(2,1)}, u32[]{:S(2)}) copy-start(bf16[256,2048]{1,0:T(8,128)(2,1)} %x_ref.3) | copy-start | bytes 3145732
  12.3 2.2 %collective-permute-start.5 = (bf16[128,1024]{1,0:T(8,128)(2,1)S(1)}, bf16[128,1024]{1,0:T(8,128)(2,1)S(1)}, u32[]{:S(2)}, u32[]{:S(2)}) collective-permute-start(bf16[128,1024]{1,0:T(8,128)(2,1)S(1)} %get-tuple-element.32), channel_id=1, source_target_pairs={{0,1},{1,0},{2,3},{3,2},{4,5},{5,4},{6,7},{7,6},{8,9},{9,8},{10,11... | collective-permute-start | bytes 786440 | tf_op jit(solution)/shard_map/ppermute | solution.py:277
  14.0 2.2 %collective-permute-start.1 = (bf16[128,1024]{1,0:T(8,128)(2,1)S(1)}, bf16[128,1024]{1,0:T(8,128)(2,1)S(1)}, u32[]{:S(2)}, u32[]{:S(2)}) collective-permute-start(bf16[128,1024]{1,0:T(8,128)(2,1)S(1)} %get-tuple-element.28), channel_id=1, source_target_pairs={{0,1},{1,0},{2,3},{3,2},{4,5},{5,4},{6,7},{7,6},{8,9},{9,8},{10,11... | collective-permute-start | bytes 786440 | tf_op jit(solution)/shard_map/ppermute | solution.py:277
  14.6 9.2 %collective-permute-start.6 = (bf16[128,1024]{1,0:T(8,128)(2,1)S(1)}, bf16[128,1024]{1,0:T(8,128)(2,1)S(1)}, u32[]{:S(2)}, u32[]{:S(2)}) collective-permute-start(bf16[128,1024]{1,0:T(8,128)(2,1)S(1)} %add.3.a_ref), channel_id=1, source_target_pairs={{0,2},{1,3},{2,0},{3,1},{4,6},{5,7},{6,4},{7,5},{8,10},{9,11},{10,... | collective-permute-start | bytes 786440 | tf_op jit(solution)/shard_map/ppermute | solution.py:277
  16.2 12.3 %collective-permute-start.2 = (bf16[128,1024]{1,0:T(8,128)(2,1)S(1)}, bf16[128,1024]{1,0:T(8,128)(2,1)S(1)}, u32[]{:S(2)}, u32[]{:S(2)}) collective-permute-start(bf16[128,1024]{1,0:T(8,128)(2,1)S(1)} %add.2.a_ref), channel_id=1, source_target_pairs={{0,2},{1,3},{2,0},{3,1},{4,6},{5,7},{6,4},{7,5},{8,10},{9,11},{10,... | collective-permute-start | bytes 786440 | tf_op jit(solution)/shard_map/ppermute | solution.py:277
  23.9 5.6 %copy-start.1 = (bf16[2,2048,128]{2,1,0:T(8,128)(2,1)S(1)}, bf16[2,2048,128]{2,1,0:T(8,128)(2,1)}, u32[]{:S(2)}) copy-start(bf16[2,2048,128]{2,1,0:T(8,128)(2,1)} %wk_ref.3) | copy-start | bytes 3145732
  23.9 5.6 %copy-start.2 = (bf16[2,2048,128]{2,1,0:T(8,128)(2,1)S(1)}, bf16[2,2048,128]{2,1,0:T(8,128)(2,1)}, u32[]{:S(2)}) copy-start(bf16[2,2048,128]{2,1,0:T(8,128)(2,1)} %wv_ref.3) | copy-start | bytes 3145732
  24.0 5.5 %copy-start.4 = (f32[2,2048]{1,0:T(2,128)S(1)}, f32[2,2048]{1,0:T(2,128)}, u32[]{:S(2)}) copy-start(f32[2,2048]{1,0:T(2,128)} %gain_ref.3) | copy-start | bytes 49156
  24.0 5.5 %copy-start.5 = (f32[2,64]{1,0:T(2,128)S(1)}, f32[2,64]{1,0:T(2,128)}, u32[]{:S(2)}) copy-start(f32[2,64]{1,0:T(2,128)} %kg_ref.3) | copy-start | bytes 1540
  24.0 5.5 %collective-permute-start.7 = (bf16[128,1024]{1,0:T(8,128)(2,1)S(1)}, bf16[128,1024]{1,0:T(8,128)(2,1)S(1)}, u32[]{:S(2)}, u32[]{:S(2)}) collective-permute-start(bf16[128,1024]{1,0:T(8,128)(2,1)S(1)} %residual.3.mine_ref.refs_3_), channel_id=1, source_target_pairs={{0,1},{1,0},{2,3},{3,2},{4,5},{5,4},{6,7},{7,6},{8,9},{9,8},{10,11... | collective-permute-start | bytes 786440 | tf_op jit(solution)/shard_map/ppermute | solution.py:277
  28.6 6.5 %collective-permute-start.3 = (bf16[128,1024]{1,0:T(8,128)(2,1)S(1)}, bf16[128,1024]{1,0:T(8,128)(2,1)S(1)}, u32[]{:S(2)}, u32[]{:S(2)}) collective-permute-start(bf16[128,1024]{1,0:T(8,128)(2,1)S(1)} %residual.2.mine_ref.refs_0_), channel_id=1, source_target_pairs={{0,1},{1,0},{2,3},{3,2},{4,5},{5,4},{6,7},{7,6},{8,9},{9,8},{10,11... | collective-permute-start | bytes 786440 | tf_op jit(solution)/shard_map/ppermute | solution.py:277
  30.2 10.8 %collective-permute-start.8 = (bf16[128,256]{1,0:T(8,128)(2,1)S(1)}, bf16[128,256]{1,0:T(8,128)(2,1)S(1)}, u32[]{:S(2)}, u32[]{:S(2)}) collective-permute-start(bf16[128,256]{1,0:T(8,128)(2,1)S(1)} %get-tuple-element.33.refs_2_), channel_id=1, source_target_pairs={{0,4},{4,8},{8,12},{12,16},{16,20},{20,24},{24,28},{1,5},{5,9},{9,... | collective-permute-start | bytes 196616 | tf_op jit(solution)/shard_map/ppermute | solution.py:281
  35.8 6.9 %collective-permute-start.4 = (bf16[128,256]{1,0:T(8,128)(2,1)S(1)}, bf16[128,256]{1,0:T(8,128)(2,1)S(1)}, u32[]{:S(2)}, u32[]{:S(2)}) collective-permute-start(bf16[128,256]{1,0:T(8,128)(2,1)S(1)} %get-tuple-element.30.refs_2_.refs_1_), channel_id=1, source_target_pairs={{0,4},{4,8},{8,12},{12,16},{16,20},{20,24},{24,28},{1,5},{5,9},{9,... | collective-permute-start | bytes 196616 | tf_op jit(solution)/shard_map/ppermute | solution.py:281
  42.5 2.2 %collective-permute-start.11 = (bf16[128,1024]{1,0:T(8,128)(2,1)S(1)}, bf16[128,1024]{1,0:T(8,128)(2,1)S(1)}, u32[]{:S(2)}, u32[]{:S(2)}) collective-permute-start(bf16[128,1024]{1,0:T(8,128)(2,1)S(1)} %get-tuple-element.40), channel_id=1, source_target_pairs={{0,1},{1,0},{2,3},{3,2},{4,5},{5,4},{6,7},{7,6},{8,9},{9,8},{10,11... | collective-permute-start | bytes 786440 | tf_op jit(solution)/shard_map/ppermute | solution.py:277
  44.2 2.2 %collective-permute-start.9 = (bf16[128,1024]{1,0:T(8,128)(2,1)S(1)}, bf16[128,1024]{1,0:T(8,128)(2,1)S(1)}, u32[]{:S(2)}, u32[]{:S(2)}) collective-permute-start(bf16[128,1024]{1,0:T(8,128)(2,1)S(1)} %get-tuple-element.35), channel_id=1, source_target_pairs={{0,1},{1,0},{2,3},{3,2},{4,5},{5,4},{6,7},{7,6},{8,9},{9,8},{10,11... | collective-permute-start | bytes 786440 | tf_op jit(solution)/shard_map/ppermute | solution.py:277
  44.8 6.4 %collective-permute-start.12 = (bf16[128,512]{1,0:T(8,128)(2,1)S(1)}, bf16[128,512]{1,0:T(8,128)(2,1)S(1)}, u32[]{:S(2)}, u32[]{:S(2)}) collective-permute-start(bf16[128,512]{1,0:T(8,128)(2,1)S(1)} %get-tuple-element.42), channel_id=1, source_target_pairs={{0,2},{1,3},{2,0},{3,1},{4,6},{5,7},{6,4},{7,5},{8,10},{9,11},{10,... | collective-permute-start | bytes 393224 | tf_op jit(solution)/shard_map/ppermute | solution.py:277
  46.4 6.7 %collective-permute-start.10 = (bf16[128,512]{1,0:T(8,128)(2,1)S(1)}, bf16[128,512]{1,0:T(8,128)(2,1)S(1)}, u32[]{:S(2)}, u32[]{:S(2)}) collective-permute-start(bf16[128,512]{1,0:T(8,128)(2,1)S(1)} %get-tuple-element.37), channel_id=1, source_target_pairs={{0,2},{1,3},{2,0},{3,1},{4,6},{5,7},{6,4},{7,5},{8,10},{9,11},{10,... | collective-permute-start | bytes 393224 | tf_op jit(solution)/shard_map/ppermute | solution.py:277

commit v4 on v3

--- a/solution.py
+++ b/solution.py
@@ -23,6 +23,8 @@
 
 norm_eps = 1e-06
 masked_score = -1e30
+
+LOG2_E = 1.4426950408889634
 
 bf16 = jnp.bfloat16
 f32 = jnp.float32
@@ -132,11 +134,19 @@
 
 
 def query_body(flat, gain_row, q_ref):
-    pieces = head_norm(flat, gain_row)
-    width = pieces[0].shape[1]
-    for index, piece in enumerate(pieces):
-        scaled = piece.astype(bf16) * bf16(HEAD_DIM**-0.5)
-        q_ref[:, index * width : (index + 1) * width] = scaled
+    pieces = head_norm(flat, gain_row * (HEAD_DIM**-0.5 * LOG2_E))
+    kv_width = q_ref.shape[2]
+    group = q_ref.shape[0] * HEAD_DIM // kv_width
+    lanes = pieces[0].shape[1]
+    for head in range(q_ref.shape[0]):
+        at = head * HEAD_DIM
+        piece = pieces[at // lanes][:, at % lanes : at % lanes + HEAD_DIM]
+        before = head // group * HEAD_DIM
+        after = kv_width - HEAD_DIM - before
+        rows = piece.shape[0]
+        spread = [jnp.zeros((rows, before), f32)] if before else []
+        spread += [piece] + ([jnp.zeros((rows, after), f32)] if after else [])
+        q_ref[head] = jnp.concatenate(spread, axis=1).astype(bf16)
 
 
 def bias_kernel(layer_index, table_ref, tile_ref):
@@ -149,7 +159,7 @@
     key_seg = lax.broadcasted_iota(jnp.int32, (CHUNK, WINDOW), 1) // SEG
     inside = (key_seg >= query_seg) & (key_seg <= query_seg + LEFT)
     line = jnp.dot(
-        table_ref[layer_index], onehot, precision=lax.Precision.HIGHEST,
+        table_ref[layer_index] * LOG2_E, onehot, precision=lax.Precision.HIGHEST,
         preferred_element_type=f32,
     )
     for head in range(heads):
@@ -159,75 +169,139 @@
 
 
 def attention_kernel(
-    block, layer_index, q_start, starts, prior, q_ref, *refs,
+    block, layer_index, q_start, row_start, step, starts, prior, q_ref, *refs,
 ):
     piece_refs = refs[:PIECES]
-    (
-        tile_ref, wout_ref, keep_ref, send_ref,
-        keys_ref, even_ref, odd_ref, mixed_ref,
-    ) = refs[PIECES:]
-    parity = lax.axis_index("tp") % 2
-    heads = q_ref.shape[1] // HEAD_DIM
-    kv_width = piece_refs[0].shape[1] // 2
-    kv_heads = kv_width // HEAD_DIM
-    group = heads // kv_heads
-    pairs = group // 2
-
-    low = lax.broadcasted_iota(jnp.int32, (CHUNK, LANES), 1) < HEAD_DIM
-    for index, piece_ref in enumerate(piece_refs):
-        source = slice(starts[index], starts[index] + CHUNK)
-        into = slice(index * CHUNK, (index + 1) * CHUNK)
-        for kv in range(kv_heads):
-            at = kv * HEAD_DIM
-            key = piece_ref[source, at : at + HEAD_DIM].astype(f32)
-            value = piece_ref[source, kv_width + at : kv_width + at + HEAD_DIM].astype(f32)
-            key = jnp.concatenate([key, key], axis=1)
-            value = jnp.concatenate([value, value], axis=1)
-            keys_ref[kv, into, :] = key.astype(bf16)
-            even_ref[kv, into, :] = jnp.where(low, value, 1.0).astype(bf16)
-            odd_ref[kv, into, :] = jnp.where(low, 1.0, value).astype(bf16)
-
+    tile_ref, wout_ref, keep_ref, send_ref, mixed_ref = refs[PIECES:]
+    heads = q_ref.shape[0]
+    kv_width = q_ref.shape[2]
+    group = heads * HEAD_DIM // kv_width
+    count = keep_ref.shape[0]
+    rows = slice(q_start, q_start + count)
+
+    pieces = [
+        ref[start : start + CHUNK, :] for ref, start in zip(piece_refs, starts, strict=True)
+    ]
+    keys = jnp.concatenate([piece[:, :kv_width] for piece in pieces], axis=0)
+    values = jnp.concatenate([piece[:, kv_width:] for piece in pieces], axis=0)
+    values = jnp.concatenate([values, jnp.ones_like(values)], axis=1)
     key_index = lax.broadcasted_iota(jnp.int32, (1, WINDOW), 1)
-    outside = jnp.where((key_index < prior * CHUNK) & (lax.axis_index("sp") == 0), masked_score, 0.0)
-    for kv in range(kv_heads):
-        evens, odds = [], []
-        for pair in range(pairs):
-            at = (kv * pairs + pair) * LANES
-            both = q_ref[q_start : q_start + CHUNK, at : at + LANES]
-            evens.append(jnp.where(low, both, jnp.zeros_like(both)))
-            odds.append(jnp.where(low, jnp.zeros_like(both), both))
-        stacked = jnp.concatenate(evens + odds, axis=0)
+    outside = (key_index < prior * CHUNK) & (lax.axis_index("sp") == 0)
+    outside = jnp.where(outside, masked_score, 0.0)
+    for first in range(0, heads, step):
+        stacked = jnp.concatenate([q_ref[first + index, rows, :] for index in range(step)], axis=0)
         scores = lax.dot_general(
-            stacked, keys_ref[kv], (((1,), (1,)), ((), ())), preferred_element_type=f32
+            stacked, keys, (((1,), (1,)), ((), ())), preferred_element_type=f32
         )
         expons = []
-        for index in range(group):
-            pair, side = index % pairs, index // pairs
-            head = kv * group + 2 * pair + side
-            score = scores[index * CHUNK : (index + 1) * CHUNK, :] + tile_ref[head]
+        for index in range(step):
+            score = scores[index * count : (index + 1) * count, :]
+            score = score + tile_ref[first + index, row_start : row_start + count, :]
             if prior:
                 score = score + outside
             peak = jnp.max(score, axis=-1, keepdims=True)
-            expons.append(jnp.exp(score - peak).astype(bf16))
-        even = jnp.dot(
-            jnp.concatenate(expons[:pairs], axis=0), even_ref[kv], preferred_element_type=f32
+            expons.append(jnp.exp2(score - peak).astype(bf16))
+        summed = jnp.dot(
+            jnp.concatenate(expons, axis=0), values, preferred_element_type=f32
         )
-        odd = jnp.dot(
-            jnp.concatenate(expons[pairs:], axis=0), odd_ref[kv], preferred_element_type=f32
-        )
-        for pair in range(pairs):
-            at = (kv * pairs + pair) * LANES
-            upper = even[pair * CHUNK : (pair + 1) * CHUNK, :]
-            lower = odd[pair * CHUNK : (pair + 1) * CHUNK, :]
-            total = pltpu.roll(jnp.where(low, lower, upper), HEAD_DIM, 1)
-            mixed_ref[:, at : at + LANES] = (jnp.where(low, upper, lower) / total).astype(bf16)
-
+        ratio = summed[:, :kv_width] / summed[:, kv_width:]
+        for index in range(step):
+            at = (first + index) // group * HEAD_DIM
+            into = (first + index) * HEAD_DIM
+            part = ratio[index * count : (index + 1) * count, at : at + HEAD_DIM]
+            mixed_ref[:, into : into + HEAD_DIM] = part.astype(bf16)
+
+    out_projection(block, layer_index, mixed_ref, wout_ref, keep_ref, send_ref)
+
+
+def out_projection(block, layer_index, mixed_ref, wout_ref, keep_ref, send_ref):
+    parity = lax.axis_index("tp") % 2
     mixed = mixed_ref[...]
     for index in range(keep_ref.shape[1] // block):
         for target, side in ((send_ref, 1 - parity), (keep_ref, parity)):
             cols = pl.ds(pl.multiple_of((2 * index + side) * block, LANES), block)
-            partial_value = jnp.dot(mixed, wout_ref[layer_index, :, cols], preferred_element_type=f32)
+            partial_value = jnp.dot(
+                mixed, wout_ref[layer_index, :, cols], preferred_element_type=f32
+            )
             target[:, index * block : (index + 1) * block] = partial_value.astype(bf16)
+
+
+def own_kernel(q_start, starts, q_ref, *refs):
+    piece_refs = refs[: len(starts)]
+    tile_ref, peak_ref, summed_ref = refs[len(starts) :]
+    kv_width = q_ref.shape[2]
+    rows = slice(q_start, q_start + CHUNK)
+    pieces = [
+        ref[start : start + CHUNK, :] for ref, start in zip(piece_refs, starts, strict=True)
+    ]
+    keys = jnp.concatenate([piece[:, :kv_width] for piece in pieces], axis=0)
+    values = jnp.concatenate([piece[:, kv_width:] for piece in pieces], axis=0)
+    values = jnp.concatenate([values, jnp.ones_like(values)], axis=1)
+    lower = WINDOW - len(starts) * CHUNK
+    heads = q_ref.shape[0]
+    scores = lax.dot_general(
+        q_ref[:, rows, :].reshape(heads * CHUNK, kv_width), keys, (((1,), (1,)), ((), ())),
+        preferred_element_type=f32,
+    ).reshape(heads, CHUNK, keys.shape[0])
+    scores = scores + tile_ref[:, :, lower:]
+    peaks = jnp.max(scores, axis=-1, keepdims=True)
+    expons = jnp.exp2(scores - peaks).astype(bf16)
+    peak_ref[...] = jnp.broadcast_to(peaks, peak_ref.shape)
+    summed = jnp.dot(
+        expons.reshape(heads * CHUNK, keys.shape[0]), values, preferred_element_type=f32
+    )
+    summed_ref[...] = summed.reshape(summed_ref.shape)
+
+
+def joined_kernel(block, layer_index, q_start, starts, q_ref, *refs):
+    piece_refs = refs[: len(starts)]
+    (
+        tile_ref, peak_ref, summed_ref, wout_ref, keep_ref, send_ref, mixed_ref,
+    ) = refs[len(starts) :]
+    heads = q_ref.shape[0]
+    kv_width = q_ref.shape[2]
+    group = heads * HEAD_DIM // kv_width
+    rows = slice(q_start, q_start + CHUNK)
+    upper = len(starts) * CHUNK
+
+    def put(head, summed):
+        ratio = summed[:, :kv_width] / summed[:, kv_width:]
+        at = head // group * HEAD_DIM
+        into = head * HEAD_DIM
+        mixed_ref[:, into : into + HEAD_DIM] = ratio[:, at : at + HEAD_DIM].astype(bf16)
+
+    @pl.when(lax.axis_index("sp") == 0)
+    def _():
+        for head in range(heads):
+            put(head, summed_ref[head])
+
+    @pl.when(lax.axis_index("sp") > 0)
+    def _():
+        pieces = [
+            ref[start : start + CHUNK, :] for ref, start in zip(piece_refs, starts, strict=True)
+        ]
+        keys = jnp.concatenate([piece[:, :kv_width] for piece in pieces], axis=0)
+        values = jnp.concatenate([piece[:, kv_width:] for piece in pieces], axis=0)
+        values = jnp.concatenate([values, jnp.ones_like(values)], axis=1)
+        scores = lax.dot_general(
+            q_ref[:, rows, :].reshape(heads * CHUNK, kv_width), keys, (((1,), (1,)), ((), ())),
+            preferred_element_type=f32,
+        ).reshape(heads, CHUNK, upper)
+        scores = scores + tile_ref[:, :, :upper]
+        before = peak_ref[...]
+        peaks = jnp.max(scores, axis=-1, keepdims=True)
+        peaks = jnp.maximum(before, jnp.broadcast_to(peaks, before.shape))
+        spread = jnp.concatenate([peaks] * len(starts), axis=2)
+        expons = jnp.exp2(scores - spread).astype(bf16)
+        summed = jnp.dot(
+            expons.reshape(heads * CHUNK, upper), values, preferred_element_type=f32
+        ).reshape(summed_ref.shape)
+        scale = jnp.exp2(before - peaks)
+        for head in range(heads):
+            wide = jnp.concatenate([scale[head]] * (summed.shape[2] // LANES), axis=1)
+            put(head, summed_ref[head] * wide + summed[head])
+
+    out_projection(block, layer_index, mixed_ref, wout_ref, keep_ref, send_ref)
 
 
 def add_kernel(a_ref, b_ref, out_ref):
@@ -245,27 +319,33 @@
             ).astype(bf16)
 
 
-def residual_kernel(block, start, x_ref, a_ref, b_ref, out_ref):
-    rows = slice(start, start + out_ref.shape[0])
+def residual_kernel(block, start, x_ref, *refs):
+    out_ref = refs[-1]
     parity = lax.axis_index("tp") % 2
-    for index in range(out_ref.shape[1] // block):
-        into = slice(index * block, (index + 1) * block)
-        cols = pl.ds(pl.multiple_of((2 * index + parity) * block, LANES), block)
-        added = a_ref[:, into].astype(f32) + b_ref[:, into].astype(f32)
-        out_ref[:, into] = (x_ref[rows, cols].astype(f32) + added).astype(bf16)
-
-
-def result_kernel(block, parts, *refs):
-    ins, out_hbm, held_ref, sems = refs[: 3 * parts], refs[-3], refs[-2], refs[-1]
+    at = 0
+    for a_ref, b_ref in zip(refs[:-1:2], refs[1:-1:2], strict=True):
+        count = a_ref.shape[0]
+        for index in range(out_ref.shape[1] // block):
+            into = slice(index * block, (index + 1) * block)
+            cols = pl.ds(pl.multiple_of((2 * index + parity) * block, LANES), block)
+            added = a_ref[:, into].astype(f32) + b_ref[:, into].astype(f32)
+            held = x_ref[start + at : start + at + count, cols].astype(f32)
+            out_ref[at : at + count, into] = (held + added).astype(bf16)
+        at += count
+
+
+def result_kernel(block, places, *refs):
+    out_hbm, held_ref, sems = refs[-3:]
     cols = pl.ds(pl.multiple_of((lax.axis_index("tp") // 2) * block, LANES), block)
     copies = []
-    for part in range(parts):
-        x_ref, a_ref, b_ref = ins[3 * part : 3 * part + 3]
-        rows = slice(part * CHUNK, (part + 1) * CHUNK)
+    for index, (start, inner) in enumerate(places):
+        x_ref, a_ref, b_ref = refs[3 * index : 3 * index + 3]
+        count = a_ref.shape[0]
         added = a_ref[...].astype(f32) + b_ref[...].astype(f32)
-        held_ref[rows, :] = (x_ref[:, cols].astype(f32) + added).astype(bf16)
-        span = pl.ds(part * CHUNK, CHUNK)
-        copy = pltpu.make_async_copy(held_ref.at[span, :], out_hbm.at[span, :], sems.at[part])
+        held = x_ref[inner : inner + count, cols].astype(f32)
+        held_ref[start : start + count, :] = (held + added).astype(bf16)
+        span = pl.ds(start, count)
+        copy = pltpu.make_async_copy(held_ref.at[span, :], out_hbm.at[span, :], sems.at[index])
         copy.start()
         copies.append(copy)
     for copy in copies:
@@ -277,8 +357,10 @@
     return lax.ppermute(value, "tp", [(d, d ^ (1 << bit)) for d in range(size)])
 
 
-def passed_along(value):
-    return lax.ppermute(value, "sp", [(d, d + 1) for d in range(lax.axis_size("sp") - 1)])
+def passed_along(value, closed):
+    size = lax.axis_size("sp")
+    edges = [(d, (d + 1) % size) for d in range(size if closed else size - 1)]
+    return lax.ppermute(value, "sp", edges)
 
 
 def kept_in_hbm(*arrays):
@@ -293,7 +375,6 @@
     query_width = w_query.shape[2]
     kv_width = w_key.shape[2]
     heads = query_width // HEAD_DIM
-    kv_heads = kv_width // HEAD_DIM
     parts = rows // CHUNK
     order = list(reversed(range(parts)))
 
@@ -301,7 +382,7 @@
         count = normed.shape[0]
         return pl.pallas_call(
             functools.partial(query_kernel, layer_index),
-            out_shape=out((count, query_width)),
+            out_shape=out((heads, count, kv_width)),
             in_specs=[whole] * 3,
             out_specs=whole,
             compiler_params=params(),
@@ -309,27 +390,49 @@
             name="queries",
         )(normed, w_query, query_gain)
 
-    def attention(layer_index, part, query, q_start, pieces, starts):
+    def attention(layer_index, part, inner, count, query, q_start, pieces, starts):
         return pl.pallas_call(
             functools.partial(
-                attention_kernel, block, layer_index, q_start, starts,
-                max(0, PIECES - 1 - part),
+                attention_kernel, block, layer_index, q_start, inner,
+                STEPS[count], starts, max(0, PIECES - 1 - part),
             ),
-            out_shape=[out((CHUNK, half))] * 2,
+            out_shape=[out((count, half))] * 2,
             in_specs=[whole] * (PIECES + 3),
             out_specs=[whole, whole],
-            scratch_shapes=[
-                pltpu.VMEM((kv_heads, WINDOW, LANES), bf16),
-                pltpu.VMEM((kv_heads, WINDOW, LANES), bf16),
-                pltpu.VMEM((kv_heads, WINDOW, LANES), bf16),
-                pltpu.VMEM((CHUNK, query_width), bf16),
-            ],
+            scratch_shapes=[pltpu.VMEM((count, query_width), bf16)],
             compiler_params=params(),
             cost_estimate=cost(
                 2 * CHUNK * query_width * (width + 4 * WINDOW), 2 * width * query_width
             ),
             name="attention",
         )(query, *pieces, tiles[layer_index], w_out)
+
+    def own_part(layer_index, part, query, q_start, pieces, starts):
+        prior = max(0, PIECES - 1 - part)
+        return pl.pallas_call(
+            functools.partial(own_kernel, q_start, starts[prior:]),
+            out_shape=[
+                out((heads, CHUNK, LANES), f32), out((heads, CHUNK, 2 * kv_width), f32)
+            ],
+            in_specs=[whole] * (PIECES - prior + 2),
+            out_specs=[whole, whole],
+            compiler_params=params(),
+            cost_estimate=cost(5e8, 1e6),
+            name="own_part",
+        )(query, *pieces[prior:], tiles[layer_index])
+
+    def joined(layer_index, part, query, q_start, pieces, starts, own):
+        prior = max(0, PIECES - 1 - part)
+        return pl.pallas_call(
+            functools.partial(joined_kernel, block, layer_index, q_start, starts[:prior]),
+            out_shape=[out((CHUNK, half))] * 2,
+            in_specs=[whole] * (prior + 5),
+            out_specs=[whole, whole],
+            scratch_shapes=[pltpu.VMEM((CHUNK, query_width), bf16)],
+            compiler_params=params(),
+            cost_estimate=cost(1e9, 2 * width * query_width),
+            name="joined",
+        )(query, *pieces[:prior], tiles[layer_index], *own, w_out)
 
     normed, kv, table = pl.pallas_call(
         first_norm_kernel,
@@ -351,7 +454,7 @@
         cost_estimate=cost(3e9, 4 * rows * width),
         name="norm_kv_first",
     )(*kept_in_hbm(stream, attn_gain, w_key, w_value, key_gain, rel_bias))
-    kv_prior = passed_along(kv[rows - REACH :])
+    kv_prior = passed_along(kv[rows - REACH :], False)
     query = queries(0, normed)
     tiles = []
     for layer_index in range(LAYERS):
@@ -374,26 +477,35 @@
             behind = part - (PIECES - 1) + index
             pieces.append(kv_prior if behind < 0 else kv)
             starts.append((behind + PIECES - 1 if behind < 0 else behind) * CHUNK)
-        keep, send = attention(0, part, query, part * CHUNK, pieces, starts)
-        received = swapped(send, 0)
-        for bit in range(1, bits):
-            summed = pl.pallas_call(
-                add_kernel,
-                out_shape=out((CHUNK, half)),
-                in_specs=[whole, whole],
-                out_specs=whole,
-                compiler_params=params(),
-                name="add",
-            )(keep, received)
-            keep, received = summed, swapped(summed, bit)
+        sums = []
+        for inner, count in split_rows(False):
+            if part < PIECES - 1:
+                own = own_part(0, part, query, part * CHUNK, pieces, starts)
+                keep, send = joined(0, part, query, part * CHUNK, pieces, starts, own)
+            else:
+                keep, send = attention(
+                    0, part, inner, count, query, part * CHUNK + inner, pieces, starts
+                )
+            received = swapped(send, 0)
+            for bit in range(1, bits):
+                summed = pl.pallas_call(
+                    add_kernel,
+                    out_shape=out((count, half)),
+                    in_specs=[whole, whole],
+                    out_specs=whole,
+                    compiler_params=params(),
+                    name="add",
+                )(keep, received)
+                keep, received = summed, swapped(summed, bit)
+            sums += [keep, received]
         mine[part] = pl.pallas_call(
             functools.partial(residual_kernel, block, part * CHUNK),
             out_shape=out((CHUNK, half)),
-            in_specs=[whole, whole, whole],
+            in_specs=[whole] * (1 + len(sums)),
             out_specs=whole,
             compiler_params=params(),
             name="residual",
-        )(stream, keep, received)
+        )(stream, *sums)
         other[part] = swapped(mine[part], 0)
 
     priors = {}
@@ -408,42 +520,52 @@
             name="norm_kv_next",
         )(mine[part], other[part], attn_gain, w_key, w_value, key_gain)
         if part >= parts - (PIECES - 1):
-            priors[part - parts] = passed_along(kvs[part])
-
-    outs = {}
+            priors[part - parts] = passed_along(kvs[part], True)
+
+    places, outs = [], []
     for part in order:
         query = queries(1, normeds[part])
         pieces = []
         for index in range(PIECES):
             behind = part - (PIECES - 1) + index
             pieces.append(priors[behind] if behind < 0 else kvs[behind])
-        keep, send = attention(1, part, query, 0, pieces, [0] * PIECES)
-        received = swapped(send, 0)
-        for bit in range(1, bits):
-            left = keep.shape[1] // 2
-            keep, send = pl.pallas_call(
-                functools.partial(split_add_kernel, block, bit),
-                out_shape=[out((CHUNK, left))] * 2,
-                in_specs=[whole, whole],
-                out_specs=[whole, whole],
-                compiler_params=params(),
-                name="split_add",
-            )(keep, received)
-            received = swapped(send, bit)
-        outs[part] = (mine[part], keep, received)
+        for inner, count in split_rows(False):
+            if part == 0:
+                own = own_part(1, part, query, 0, pieces, [0] * PIECES)
+                keep, send = joined(1, part, query, 0, pieces, [0] * PIECES, own)
+            else:
+                keep, send = attention(1, part, inner, count, query, inner, pieces, [0] * PIECES)
+            received = swapped(send, 0)
+            for bit in range(1, bits):
+                left = keep.shape[1] // 2
+                keep, send = pl.pallas_call(
+                    functools.partial(split_add_kernel, block, bit),
+                    out_shape=[out((count, left))] * 2,
+                    in_specs=[whole, whole],
+                    out_specs=[whole, whole],
+                    compiler_params=params(),
+                    name="split_add",
+                )(keep, received)
+                received = swapped(send, bit)
+            places.append((part * CHUNK + inner, inner))
+            outs += [mine[part], keep, received]
 
     return pl.pallas_call(
-        functools.partial(result_kernel, block, parts),
+        functools.partial(result_kernel, block, places),
         out_shape=out((rows, block)),
-        in_specs=[whole] * (3 * parts),
+        in_specs=[whole] * len(outs),
         out_specs=in_hbm,
-        scratch_shapes=[
-            pltpu.VMEM((rows, block), bf16),
-            pltpu.SemaphoreType.DMA((parts,)),
-        ],
+        scratch_shapes=[pltpu.VMEM((rows, block), bf16), pltpu.SemaphoreType.DMA((len(places),))],
         compiler_params=params(),
         name="result",
-    )(*[ref for part in range(parts) for ref in outs[part]])
+    )(*outs)
+
+
+def split_rows(fine):
+    return [(at, SEG) for at in range(0, CHUNK, SEG)] if fine else [(0, CHUNK)]
+
+
+STEPS = {CHUNK: 1, SEG: 2}
 
 
 def solution(mesh):

time: 54.3 us -> 51.5 us (0.948)
  starting transfers between devices: 20.5 us -> 16.6 us
  waiting for transfers between devices: 17.5 us -> 20 us
  Pallas kernels: 15.2 us -> 14.3 us
    pallas_call x4 -> x1, Pallas kernels: 6.14 us -> 1.37 us  [attention(): pl.pallas_call(functools.partial(attention_kernel, block, layer_index, q_...]
    pallas_call x3 -> x9, Pallas kernels: 0.89 us -> 4.53 us  [the longest x3 1.83 us: joined(): pl.pallas_call(functools.partial(joined_kernel, block, layer_index, q_sta...]
    ppermute x3, starting transfers between devices: 13.8 us -> 10.4 us  [passed_along(): return lax.ppermute(value, 'sp', edges)]
    ppermute x3, waiting for transfers between devices: 0.94 us -> 2.5 us  [passed_along(): return lax.ppermute(value, 'sp', edges)]
    ppermute x10, waiting for transfers between devices: 16.6 us -> 17.5 us  [swapped(): return lax.ppermute(value, 'tp', [(d, d ^ 1 << bit) for d in range(size)])]
  transfers between devices with their start and end apart: 13 -> 13, of which waited for: 5 -> 7; matrix products, arithmetic and copies ran while one was open for 0% -> 0% of each run, Pallas kernels for 19% -> 20%
where the time goes in v4:
time: 51.5 us; the launch traced here: 51.2 us
  waiting for transfers between devices  20 us (39%)
  starting transfers between devices  16.6 us (32%)
  Pallas kernels  14.3 us (28%)
    ppermute x10, waiting for transfers between devices, swapped(): return lax.ppermute(value, 'tp', [(d, d ^ 1 << bit) for d in range(size)])  17.5 us
    ppermute x3, starting transfers between devices, passed_along(): return lax.ppermute(value, 'sp', edges)  10.4 us
    ppermute x10, starting transfers between devices, swapped(): return lax.ppermute(value, 'tp', [(d, d ^ 1 << bit) for d in range(size)])  6.17 us
    pallas_call x1, Pallas kernels, layers(): pl.pallas_call(first_norm_kernel, out_shape=[out((rows, width)), out((row...  2.61 us
    pallas_call x3, Pallas kernels, queries(): pl.pallas_call(functools.partial(query_kernel, layer_index), out_shape=ou...  2.54 us
    ppermute x3, waiting for transfers between devices, passed_along(): return lax.ppermute(value, 'sp', edges)  2.5 us
    pallas_call x3, Pallas kernels, joined(): pl.pallas_call(functools.partial(joined_kernel, block, layer_index, q_sta...  1.83 us
    pallas_call x3, Pallas kernels, own_part(): pl.pallas_call(functools.partial(own_kernel, q_start, starts[prior:]), ou...  1.81 us
  transfers between devices with their start and end apart: 13, of which 7 were waited for; matrix products, arithmetic and copies ran while one was open for 0% of the time, Pallas kernels for 20%

profile of v4, /device:TPU:0, one launch (start us, length us, event | category | flops | bytes accessed | tf_op | source)
XLA Modules:
  0.0 51.2 jit_solution(5458202335662243770)
XLA Ops:
  0.0 2.6 %norm_kv_first.1 = (bf16[256,2048]{1,0:T(8,128)(2,1)S(1)}, bf16[256,256]{1,0:T(8,128)(2,1)S(1)}, f32[2,8,257]{2,1,0:T(8,128)S(1)}) custom-call(bf16[256,2048]{1,0:T(8,128)(2,1)} %x_ref.3, f32[2,2048]{1,0:T(2,128)} %gain_ref.3, bf16[2,2048,128]{2,1,0:T(8,128)(2,1)} %wk_ref.3, bf16[2,2048,128]{2,1,0:T(8,128)(2,1)} %wv_ref.3, f32[2,64]{1,0:T(2,128)} %kg_ref.3, ...), custom_call_target="tpu_custom_call" | custom-call | flops 3000000000 | bytes 2097152 | tf_op jit(solution)/shard_map/norm_kv_first/pallas_call | solution.py:437
  2.6 5.2 %collective-permute-start = (bf16[256,256]{1,0:T(8,128)(2,1)S(1)}, bf16[256,256]{1,0:T(8,128)(2,1)S(1)}, u32[]{:S(2)}, u32[]{:S(2)}) collective-permute-start(bf16[256,256]{1,0:T(8,128)(2,1)S(1)} %get-tuple-element.31.refs_0_.refs_1_), channel_id=1, source_target_pairs={{0,4},{4,8},{8,12},{12,16},{16,20},{20,24},{24,28},{1,5},{5,9},{9,... | collective-permute-start | bytes 393224 | tf_op jit(solution)/shard_map/ppermute | solution.py:363
  7.8 0.8 %bias_tiles.2.refs_2_.refs_1_ = f32[8,128,384]{2,1,0:T(8,128)S(1)} custom-call(f32[2,8,257]{2,1,0:T(8,128)S(1)} %get-tuple-element.32.table_ref), custom_call_target="tpu_custom_call" | custom-call | flops 2000000000 | bytes 1000000 | tf_op jit(solution)/shard_map/bias_tiles/pallas_call | solution.py:462
  8.6 1.1 %queries.3.q_ref = bf16[8,256,128]{2,1,0:T(8,128)(2,1)S(1)} custom-call(bf16[256,2048]{1,0:T(8,128)(2,1)S(1)} %get-tuple-element.30.normed_ref, bf16[2,2048,512]{2,1,0:T(8,128)(2,1)S(1)} %copy-done.6, f32[2,64]{1,0:T(2,128)S(1)} %copy-done.7), custom_call_target="tpu_custom_call" | custom-call | flops 2000000000 | bytes 2097152 | tf_op jit(solution)/shard_map/queries/pallas_call | solution.py:383
  9.7 0.6 %own_part.3 = (f32[8,128,128]{2,1,0:T(8,128)S(1)}, f32[8,128,256]{2,1,0:T(8,128)S(1)}) custom-call(bf16[8,256,128]{2,1,0:T(8,128)(2,1)S(1)} %queries.3.q_ref, bf16[256,256]{1,0:T(8,128)(2,1)S(1)} %get-tuple-element.31.refs_0_.refs_1_, bf16[256,256]{1,0:T(8,128)(2,1)S(1)} %get-tuple-element.31.refs_0_.refs_1_, f32[8,128,384]{2,1,0:T(8,128)S(1)} %bias_tiles.2.refs_2_.refs_1_), custom_call_target="tpu_custom_call" | custom-call | flops 500000000 | bytes 1000000 | tf_op jit(solution)/shard_map/own_part/pallas_call | solution.py:412
  10.3 0.6 %own_part.4 = (f32[8,128,128]{2,1,0:T(8,128)S(1)}, f32[8,128,256]{2,1,0:T(8,128)S(1)}) custom-call(bf16[8,256,128]{2,1,0:T(8,128)(2,1)S(1)} %queries.3.q_ref, bf16[256,256]{1,0:T(8,128)(2,1)S(1)} %get-tuple-element.31.refs_0_.refs_1_, f32[8,128,384]{2,1,0:T(8,128)S(1)} %bias_tiles.2.refs_2_.refs_1_), custom_call_target="tpu_custom_call" | custom-call | flops 500000000 | bytes 1000000 | tf_op jit(solution)/shard_map/own_part/pallas_call | solution.py:412
  10.9 0.6 %joined.3 = (bf16[128,1024]{1,0:T(8,128)(2,1)S(1)}, bf16[128,1024]{1,0:T(8,128)(2,1)S(1)}) custom-call(bf16[8,256,128]{2,1,0:T(8,128)(2,1)S(1)} %queries.3.q_ref, bf16[256,256]{1,0:T(8,128)(2,1)S(1)} %collective-permute-done.refs_0_.refs_1_, f32[8,128,384]{2,1,0:T(8,128)S(1)} %bias_tiles.2.refs_2_.refs_1_, f32[8,128,128]{2,1,0:T(8,128)S(1)} %get-tuple-element.33.refs_2_, ...), custom_call_target="tpu_custom_call" | custom-call | flops 1000000000 | bytes 2097152 | tf_op jit(solution)/shard_map/joined/pallas_call | solution.py:426
  11.7 0.6 %joined.4 = (bf16[128,1024]{1,0:T(8,128)(2,1)S(1)}, bf16[128,1024]{1,0:T(8,128)(2,1)S(1)}) custom-call(bf16[8,256,128]{2,1,0:T(8,128)(2,1)S(1)} %queries.3.q_ref, bf16[256,256]{1,0:T(8,128)(2,1)S(1)} %collective-permute-done.refs_0_.refs_1_, bf16[256,256]{1,0:T(8,128)(2,1)S(1)} %collective-permute-done.refs_0_.refs_1_, ...), custom_call_target="tpu_custom_call" | custom-call | flops 1000000000 | bytes 2097152 | tf_op jit(solution)/shard_map/joined/pallas_call | solution.py:426
  12.3 0.5 %collective-permute-start.5 = (bf16[128,1024]{1,0:T(8,128)(2,1)S(1)}, bf16[128,1024]{1,0:T(8,128)(2,1)S(1)}, u32[]{:S(2)}, u32[]{:S(2)}) collective-permute-start(bf16[128,1024]{1,0:T(8,128)(2,1)S(1)} %get-tuple-element.42), channel_id=1, source_target_pairs={{0,1},{1,0},{2,3},{3,2},{4,5},{5,4},{6,7},{7,6},{8,9},{9,8},{10,11... | collective-permute-start | bytes 786440 | tf_op jit(solution)/shard_map/ppermute | solution.py:357
  12.8 0.4 collective-permute-done.1.b_ref
  13.2 1.6 %collective-permute-start.2 = (bf16[128,1024]{1,0:T(8,128)(2,1)S(1)}, bf16[128,1024]{1,0:T(8,128)(2,1)S(1)}, u32[]{:S(2)}, u32[]{:S(2)}) collective-permute-start(bf16[128,1024]{1,0:T(8,128)(2,1)S(1)} %add.2.refs_0_), channel_id=1, source_target_pairs={{0,2},{1,3},{2,0},{3,1},{4,6},{5,7},{6,4},{7,5},{8,10},{9,11},{10,... | collective-permute-start | bytes 786440 | tf_op jit(solution)/shard_map/ppermute | solution.py:357
  14.9 0.7 %collective-permute-start.6 = (bf16[128,1024]{1,0:T(8,128)(2,1)S(1)}, bf16[128,1024]{1,0:T(8,128)(2,1)S(1)}, u32[]{:S(2)}, u32[]{:S(2)}) collective-permute-start(bf16[128,1024]{1,0:T(8,128)(2,1)S(1)} %add.3.refs_0_), channel_id=1, source_target_pairs={{0,2},{1,3},{2,0},{3,1},{4,6},{5,7},{6,4},{7,5},{8,10},{9,11},{10,... | collective-permute-start | bytes 786440 | tf_op jit(solution)/shard_map/ppermute | solution.py:357
  15.6 6.9 %collective-permute-done.2.refs_1_ = bf16[128,1024]{1,0:T(8,128)(2,1)S(1)} collective-permute-done((bf16[128,1024]{1,0:T(8,128)(2,1)S(1)}, bf16[128,1024]{1,0:T(8,128)(2,1)S(1)}, u32[]{:S(2)}, u32[]{:S(2)}) %collective-permute-start.2) | collective-permute-done | bytes 262176 | tf_op jit(solution)/shard_map/ppermute | solution.py:357
  22.5 0.1 residual.2.mine_ref.refs_0_
  22.7 4.6 %collective-permute-done.6.refs_1_ = bf16[128,1024]{1,0:T(8,128)(2,1)S(1)} collective-permute-done((bf16[128,1024]{1,0:T(8,128)(2,1)S(1)}, bf16[128,1024]{1,0:T(8,128)(2,1)S(1)}, u32[]{:S(2)}, u32[]{:S(2)}) %collective-permute-start.6) | collective-permute-done | bytes 262176 | tf_op jit(solution)/shard_map/ppermute | solution.py:357
  27.4 0.8 %bias_tiles.3.refs_3_.refs_1_.refs_2_ = f32[8,128,384]{2,1,0:T(8,128)S(1)} custom-call(f32[2,8,257]{2,1,0:T(8,128)S(1)} %get-tuple-element.32.table_ref), custom_call_target="tpu_custom_call" | custom-call | flops 2000000000 | bytes 1000000 | tf_op jit(solution)/shard_map/bias_tiles/pallas_call | solution.py:462
  28.3 0.7 %norm_kv_next.2 = (bf16[128,2048]{1,0:T(8,128)(2,1)S(1)}, bf16[128,256]{1,0:T(8,128)(2,1)S(1)}) custom-call(bf16[128,1024]{1,0:T(8,128)(2,1)S(1)} %residual.2.mine_ref.refs_0_, bf16[128,1024]{1,0:T(8,128)(2,1)S(1)} %collective-permute-done.3.other_ref, f32[2,2048]{1,0:T(2,128)S(1)} %copy-done.4, bf16[2,2048,128]{2,1,0:T(8,128)(2,1)S(1)} %copy-done.1, ...), custom_call_target="tpu_custom_call" | custom-call | flops 134217728 | bytes 1048576 | tf_op jit(solution)/shard_map/norm_kv_next/pallas_call | solution.py:513
  29.0 2.7 %collective-permute-start.4 = (bf16[128,256]{1,0:T(8,128)(2,1)S(1)}, bf16[128,256]{1,0:T(8,128)(2,1)S(1)}, u32[]{:S(2)}, u32[]{:S(2)}) collective-permute-start(bf16[128,256]{1,0:T(8,128)(2,1)S(1)} %get-tuple-element.38.refs_2_), channel_id=1, source_target_pairs={{0,4},{4,8},{8,12},{12,16},{16,20},{20,24},{24,28},{28,0},{1,5},{5... | collective-permute-start | bytes 196616 | tf_op jit(solution)/shard_map/ppermute | solution.py:363
  31.7 0.7 %queries.4.q_ref = bf16[8,128,128]{2,1,0:T(8,128)(2,1)S(1)} custom-call(bf16[128,2048]{1,0:T(8,128)(2,1)S(1)} %get-tuple-element.37.normed_ref, bf16[2,2048,512]{2,1,0:T(8,128)(2,1)S(1)} %copy-done.6, f32[2,64]{1,0:T(2,128)S(1)} %copy-done.7), custom_call_target="tpu_custom_call" | custom-call | flops 2000000000 | bytes 2097152 | tf_op jit(solution)/shard_map/queries/pallas_call | solution.py:383
  32.5 0.7 %norm_kv_next.3 = (bf16[128,2048]{1,0:T(8,128)(2,1)S(1)}, bf16[128,256]{1,0:T(8,128)(2,1)S(1)}) custom-call(bf16[128,1024]{1,0:T(8,128)(2,1)S(1)} %residual.3.mine_ref.refs_3_, bf16[128,1024]{1,0:T(8,128)(2,1)S(1)} %collective-permute-done.7.other_ref, f32[2,2048]{1,0:T(2,128)S(1)} %copy-done.4, bf16[2,2048,128]{2,1,0:T(8,128)(2,1)S(1)} %copy-done.1, ...), custom_call_target="tpu_custom_call" | custom-call | flops 134217728 | bytes 1048576 | tf_op jit(solution)/shard_map/norm_kv_next/pallas_call | solution.py:513
  33.2 0.7 %queries.5.q_ref = bf16[8,128,128]{2,1,0:T(8,128)(2,1)S(1)} custom-call(bf16[128,2048]{1,0:T(8,128)(2,1)S(1)} %get-tuple-element.48.normed_ref, bf16[2,2048,512]{2,1,0:T(8,128)(2,1)S(1)} %copy-done.6, f32[2,64]{1,0:T(2,128)S(1)} %copy-done.7), custom_call_target="tpu_custom_call" | custom-call | flops 2000000000 | bytes 2097152 | tf_op jit(solution)/shard_map/queries/pallas_call | solution.py:383
  33.9 2.5 %collective-permute-start.10 = (bf16[128,256]{1,0:T(8,128)(2,1)S(1)}, bf16[128,256]{1,0:T(8,128)(2,1)S(1)}, u32[]{:S(2)}, u32[]{:S(2)}) collective-permute-start(bf16[128,256]{1,0:T(8,128)(2,1)S(1)} %get-tuple-element.43.refs_1_.refs_0_), channel_id=1, source_target_pairs={{0,4},{4,8},{8,12},{12,16},{16,20},{20,24},{24,28},{28,0},{1,5},{5... | collective-permute-start | bytes 196616 | tf_op jit(solution)/shard_map/ppermute | solution.py:363
  36.4 0.6 %own_part.5 = (f32[8,128,128]{2,1,0:T(8,128)S(1)}, f32[8,128,256]{2,1,0:T(8,128)S(1)}) custom-call(bf16[8,128,128]{2,1,0:T(8,128)(2,1)S(1)} %queries.5.q_ref, bf16[128,256]{1,0:T(8,128)(2,1)S(1)} %get-tuple-element.43.refs_1_.refs_0_, f32[8,128,384]{2,1,0:T(8,128)S(1)} %bias_tiles.3.refs_3_.refs_1_.refs_2_), custom_call_target="tpu_custom_call" | custom-call | flops 500000000 | bytes 1000000 | tf_op jit(solution)/shard_map/own_part/pallas_call | solution.py:412
  37.0 0.5 collective-permute-done.4.refs_0_.refs_1_
  37.5 1.4 %attention.1 = (bf16[128,1024]{1,0:T(8,128)(2,1)S(1)}, bf16[128,1024]{1,0:T(8,128)(2,1)S(1)}) custom-call(bf16[8,128,128]{2,1,0:T(8,128)(2,1)S(1)} %queries.4.q_ref, bf16[128,256]{1,0:T(8,128)(2,1)S(1)} %collective-permute-done.4.refs_0_.refs_1_, bf16[128,256]{1,0:T(8,128)(2,1)S(1)} %get-tuple-element.43.refs_1_.refs_0_, ...), custom_call_target="tpu_custom_call" | custom-call | flops 469762048 | bytes 2097152 | tf_op jit(solution)/shard_map/attention/pallas_call | solution.py:394
  38.9 2.0 %collective-permute-done.10.refs_0_ = bf16[128,256]{1,0:T(8,128)(2,1)S(1)} collective-permute-done((bf16[128,256]{1,0:T(8,128)(2,1)S(1)}, bf16[128,256]{1,0:T(8,128)(2,1)S(1)}, u32[]{:S(2)}, u32[]{:S(2)}) %collective-permute-start.10) | collective-permute-done | bytes 65568 | tf_op jit(solution)/shard_map/ppermute | solution.py:363
  40.9 0.6 %joined.5 = (bf16[128,1024]{1,0:T(8,128)(2,1)S(1)}, bf16[128,1024]{1,0:T(8,128)(2,1)S(1)}) custom-call(bf16[8,128,128]{2,1,0:T(8,128)(2,1)S(1)} %queries.5.q_ref, bf16[128,256]{1,0:T(8,128)(2,1)S(1)} %collective-permute-done.10.refs_0_, bf16[128,256]{1,0:T(8,128)(2,1)S(1)} %collective-permute-done.4.refs_0_.refs_1_, ...), custom_call_target="tpu_custom_call" | custom-call | flops 1000000000 | bytes 2097152 | tf_op jit(solution)/shard_map/joined/pallas_call | solution.py:426
  41.7 1.6 %collective-permute-start.9 = (bf16[128,512]{1,0:T(8,128)(2,1)S(1)}, bf16[128,512]{1,0:T(8,128)(2,1)S(1)}, u32[]{:S(2)}, u32[]{:S(2)}) collective-permute-start(bf16[128,512]{1,0:T(8,128)(2,1)S(1)} %get-tuple-element.47), channel_id=1, source_target_pairs={{0,2},{1,3},{2,0},{3,1},{4,6},{5,7},{6,4},{7,5},{8,10},{9,11},{10,... | collective-permute-start | bytes 393224 | tf_op jit(solution)/shard_map/ppermute | solution.py:357
  43.3 1.4 %collective-permute-start.12 = (bf16[128,512]{1,0:T(8,128)(2,1)S(1)}, bf16[128,512]{1,0:T(8,128)(2,1)S(1)}, u32[]{:S(2)}, u32[]{:S(2)}) collective-permute-start(bf16[128,512]{1,0:T(8,128)(2,1)S(1)} %get-tuple-element.54), channel_id=1, source_target_pairs={{0,2},{1,3},{2,0},{3,1},{4,6},{5,7},{6,4},{7,5},{8,10},{9,11},{10,... | collective-permute-start | bytes 393224 | tf_op jit(solution)/shard_map/ppermute | solution.py:357
  44.7 3.4 %collective-permute-done.9.refs_2_ = bf16[128,512]{1,0:T(8,128)(2,1)S(1)} collective-permute-done((bf16[128,512]{1,0:T(8,128)(2,1)S(1)}, bf16[128,512]{1,0:T(8,128)(2,1)S(1)}, u32[]{:S(2)}, u32[]{:S(2)}) %collective-permute-start.9) | collective-permute-done | bytes 131104 | tf_op jit(solution)/shard_map/ppermute | solution.py:357
  48.1 2.3 %collective-permute-done.12.refs_5_ = bf16[128,512]{1,0:T(8,128)(2,1)S(1)} collective-permute-done((bf16[128,512]{1,0:T(8,128)(2,1)S(1)}, bf16[128,512]{1,0:T(8,128)(2,1)S(1)}, u32[]{:S(2)}, u32[]{:S(2)}) %collective-permute-start.12) | collective-permute-done | bytes 131104 | tf_op jit(solution)/shard_map/ppermute | solution.py:357
  50.4 0.8 %result.1 = bf16[256,512]{1,0:T(8,128)(2,1)} custom-call(bf16[128,1024]{1,0:T(8,128)(2,1)S(1)} %residual.2.mine_ref.refs_0_, bf16[128,512]{1,0:T(8,128)(2,1)S(1)} %get-tuple-element.46.refs_1_, bf16[128,512]{1,0:T(8,128)(2,1)S(1)} %collective-permute-done.9.refs_2_, bf16[128,1024]{1,0:T(8,128)(2,1)S(1)} %residual.3.mine_ref.refs_3_, ...), custom_call_target="tpu_custom_call" | custom-call | tf_op jit(solution)/shard_map/result/pallas_call | solution.py:553
  (32 shorter events, 0.8 us)
Async XLA Ops:
  2.6 6.0 %copy-start.6 = (bf16[2,2048,512]{2,1,0:T(8,128)(2,1)S(1)}, bf16[2,2048,512]{2,1,0:T(8,128)(2,1)}, u32[]{:S(2)}) copy-start(bf16[2,2048,512]{2,1,0:T(8,128)(2,1)} %wq_ref.5) | copy-start | bytes 12582916
  2.6 6.0 %copy-start.7 = (f32[2,64]{1,0:T(2,128)S(1)}, f32[2,64]{1,0:T(2,128)}, u32[]{:S(2)}) copy-start(f32[2,64]{1,0:T(2,128)} %qg_ref.5) | copy-start | bytes 1540
  2.6 8.3 %collective-permute-start = (bf16[256,256]{1,0:T(8,128)(2,1)S(1)}, bf16[256,256]{1,0:T(8,128)(2,1)S(1)}, u32[]{:S(2)}, u32[]{:S(2)}) collective-permute-start(bf16[256,256]{1,0:T(8,128)(2,1)S(1)} %get-tuple-element.31.refs_0_.refs_1_), channel_id=1, source_target_pairs={{0,4},{4,8},{8,12},{12,16},{16,20},{20,24},{24,28},{1,5},{5,9},{9,... | collective-permute-start | bytes 393224 | tf_op jit(solution)/shard_map/ppermute | solution.py:363
  8.6 2.3 %copy-start = (bf16[2,512,2048]{2,1,0:T(8,128)(2,1)S(1)}, bf16[2,512,2048]{2,1,0:T(8,128)(2,1)}, u32[]{:S(2)}) copy-start(bf16[2,512,2048]{2,1,0:T(8,128)(2,1)} %refs_5_.3) | copy-start | bytes 12582916
  11.6 1.6 %collective-permute-start.1 = (bf16[128,1024]{1,0:T(8,128)(2,1)S(1)}, bf16[128,1024]{1,0:T(8,128)(2,1)S(1)}, u32[]{:S(2)}, u32[]{:S(2)}) collective-permute-start(bf16[128,1024]{1,0:T(8,128)(2,1)S(1)} %get-tuple-element.36), channel_id=1, source_target_pairs={{0,1},{1,0},{2,3},{3,2},{4,5},{5,4},{6,7},{7,6},{8,9},{9,8},{10,11... | collective-permute-start | bytes 786440 | tf_op jit(solution)/shard_map/ppermute | solution.py:357
  11.6 10.8 %copy-start.3 = (bf16[256,2048]{1,0:T(8,128)(2,1)S(1)}, bf16[256,2048]{1,0:T(8,128)(2,1)}, u32[]{:S(2)}) copy-start(bf16[256,2048]{1,0:T(8,128)(2,1)} %x_ref.3) | copy-start | bytes 3145732
  12.3 2.5 %collective-permute-start.5 = (bf16[128,1024]{1,0:T(8,128)(2,1)S(1)}, bf16[128,1024]{1,0:T(8,128)(2,1)S(1)}, u32[]{:S(2)}, u32[]{:S(2)}) collective-permute-start(bf16[128,1024]{1,0:T(8,128)(2,1)S(1)} %get-tuple-element.42), channel_id=1, source_target_pairs={{0,1},{1,0},{2,3},{3,2},{4,5},{5,4},{6,7},{7,6},{8,9},{9,8},{10,11... | collective-permute-start | bytes 786440 | tf_op jit(solution)/shard_map/ppermute | solution.py:357
  13.2 9.2 %collective-permute-start.2 = (bf16[128,1024]{1,0:T(8,128)(2,1)S(1)}, bf16[128,1024]{1,0:T(8,128)(2,1)S(1)}, u32[]{:S(2)}, u32[]{:S(2)}) collective-permute-start(bf16[128,1024]{1,0:T(8,128)(2,1)S(1)} %add.2.refs_0_), channel_id=1, source_target_pairs={{0,2},{1,3},{2,0},{3,1},{4,6},{5,7},{6,4},{7,5},{8,10},{9,11},{10,... | collective-permute-start | bytes 786440 | tf_op jit(solution)/shard_map/ppermute | solution.py:357
  14.9 12.4 %collective-permute-start.6 = (bf16[128,1024]{1,0:T(8,128)(2,1)S(1)}, bf16[128,1024]{1,0:T(8,128)(2,1)S(1)}, u32[]{:S(2)}, u32[]{:S(2)}) collective-permute-start(bf16[128,1024]{1,0:T(8,128)(2,1)S(1)} %add.3.refs_0_), channel_id=1, source_target_pairs={{0,2},{1,3},{2,0},{3,1},{4,6},{5,7},{6,4},{7,5},{8,10},{9,11},{10,... | collective-permute-start | bytes 786440 | tf_op jit(solution)/shard_map/ppermute | solution.py:357
  22.6 5.7 %copy-start.1 = (bf16[2,2048,128]{2,1,0:T(8,128)(2,1)S(1)}, bf16[2,2048,128]{2,1,0:T(8,128)(2,1)}, u32[]{:S(2)}) copy-start(bf16[2,2048,128]{2,1,0:T(8,128)(2,1)} %wk_ref.3) | copy-start | bytes 3145732
  22.6 5.7 %copy-start.2 = (bf16[2,2048,128]{2,1,0:T(8,128)(2,1)S(1)}, bf16[2,2048,128]{2,1,0:T(8,128)(2,1)}, u32[]{:S(2)}) copy-start(bf16[2,2048,128]{2,1,0:T(8,128)(2,1)} %wv_ref.3) | copy-start | bytes 3145732
  22.6 5.7 %copy-start.4 = (f32[2,2048]{1,0:T(2,128)S(1)}, f32[2,2048]{1,0:T(2,128)}, u32[]{:S(2)}) copy-start(f32[2,2048]{1,0:T(2,128)} %gain_ref.3) | copy-start | bytes 49156
  22.6 5.7 %copy-start.5 = (f32[2,64]{1,0:T(2,128)S(1)}, f32[2,64]{1,0:T(2,128)}, u32[]{:S(2)}) copy-start(f32[2,64]{1,0:T(2,128)} %kg_ref.3) | copy-start | bytes 1540
  22.6 5.6 %collective-permute-start.3 = (bf16[128,1024]{1,0:T(8,128)(2,1)S(1)}, bf16[128,1024]{1,0:T(8,128)(2,1)S(1)}, u32[]{:S(2)}, u32[]{:S(2)}) collective-permute-start(bf16[128,1024]{1,0:T(8,128)(2,1)S(1)} %residual.2.mine_ref.refs_0_), channel_id=1, source_target_pairs={{0,1},{1,0},{2,3},{3,2},{4,5},{5,4},{6,7},{7,6},{8,9},{9,8},{10,11... | collective-permute-start | bytes 786440 | tf_op jit(solution)/shard_map/ppermute | solution.py:357
  27.4 5.1 %collective-permute-start.7 = (bf16[128,1024]{1,0:T(8,128)(2,1)S(1)}, bf16[128,1024]{1,0:T(8,128)(2,1)S(1)}, u32[]{:S(2)}, u32[]{:S(2)}) collective-permute-start(bf16[128,1024]{1,0:T(8,128)(2,1)S(1)} %residual.3.mine_ref.refs_3_), channel_id=1, source_target_pairs={{0,1},{1,0},{2,3},{3,2},{4,5},{5,4},{6,7},{7,6},{8,9},{9,8},{10,11... | collective-permute-start | bytes 786440 | tf_op jit(solution)/shard_map/ppermute | solution.py:357
  29.0 8.5 %collective-permute-start.4 = (bf16[128,256]{1,0:T(8,128)(2,1)S(1)}, bf16[128,256]{1,0:T(8,128)(2,1)S(1)}, u32[]{:S(2)}, u32[]{:S(2)}) collective-permute-start(bf16[128,256]{1,0:T(8,128)(2,1)S(1)} %get-tuple-element.38.refs_2_), channel_id=1, source_target_pairs={{0,4},{4,8},{8,12},{12,16},{16,20},{20,24},{24,28},{28,0},{1,5},{5... | collective-permute-start | bytes 196616 | tf_op jit(solution)/shard_map/ppermute | solution.py:363
  33.9 7.0 %collective-permute-start.10 = (bf16[128,256]{1,0:T(8,128)(2,1)S(1)}, bf16[128,256]{1,0:T(8,128)(2,1)S(1)}, u32[]{:S(2)}, u32[]{:S(2)}) collective-permute-start(bf16[128,256]{1,0:T(8,128)(2,1)S(1)} %get-tuple-element.43.refs_1_.refs_0_), channel_id=1, source_target_pairs={{0,4},{4,8},{8,12},{12,16},{16,20},{20,24},{24,28},{28,0},{1,5},{5... | collective-permute-start | bytes 196616 | tf_op jit(solution)/shard_map/ppermute | solution.py:363
  38.8 2.8 %collective-permute-start.8 = (bf16[128,1024]{1,0:T(8,128)(2,1)S(1)}, bf16[128,1024]{1,0:T(8,128)(2,1)S(1)}, u32[]{:S(2)}, u32[]{:S(2)}) collective-permute-start(bf16[128,1024]{1,0:T(8,128)(2,1)S(1)} %get-tuple-element.45), channel_id=1, source_target_pairs={{0,1},{1,0},{2,3},{3,2},{4,5},{5,4},{6,7},{7,6},{8,9},{9,8},{10,11... | collective-permute-start | bytes 786440 | tf_op jit(solution)/shard_map/ppermute | solution.py:357
  41.5 1.7 %collective-permute-start.11 = (bf16[128,1024]{1,0:T(8,128)(2,1)S(1)}, bf16[128,1024]{1,0:T(8,128)(2,1)S(1)}, u32[]{:S(2)}, u32[]{:S(2)}) collective-permute-start(bf16[128,1024]{1,0:T(8,128)(2,1)S(1)} %get-tuple-element.52), channel_id=1, source_target_pairs={{0,1},{1,0},{2,3},{3,2},{4,5},{5,4},{6,7},{7,6},{8,9},{9,8},{10,11... | collective-permute-start | bytes 786440 | tf_op jit(solution)/shard_map/ppermute | solution.py:357
  41.7 6.4 %collective-permute-start.9 = (bf16[128,512]{1,0:T(8,128)(2,1)S(1)}, bf16[128,512]{1,0:T(8,128)(2,1)S(1)}, u32[]{:S(2)}, u32[]{:S(2)}) collective-permute-start(bf16[128,512]{1,0:T(8,128)(2,1)S(1)} %get-tuple-element.47), channel_id=1, source_target_pairs={{0,2},{1,3},{2,0},{3,1},{4,6},{5,7},{6,4},{7,5},{8,10},{9,11},{10,... | collective-permute-start | bytes 393224 | tf_op jit(solution)/shard_map/ppermute | solution.py:357
  43.3 7.1 %collective-permute-start.12 = (bf16[128,512]{1,0:T(8,128)(2,1)S(1)}, bf16[128,512]{1,0:T(8,128)(2,1)S(1)}, u32[]{:S(2)}, u32[]{:S(2)}) collective-permute-start(bf16[128,512]{1,0:T(8,128)(2,1)S(1)} %get-tuple-element.54), channel_id=1, source_target_pairs={{0,2},{1,3},{2,0},{3,1},{4,6},{5,7},{6,4},{7,5},{8,10},{9,11},{10,... | collective-permute-start | bytes 393224 | tf_op jit(solution)/shard_map/ppermute | solution.py:357

commit v5 on v4

--- a/solution.py
+++ b/solution.py
@@ -65,17 +65,20 @@
     return pieces
 
 
-def key_value_body(normed, wk, wv, key_gain_row, kv_ref):
-    keys = jnp.dot(normed, wk, preferred_element_type=f32)
-    values = jnp.dot(normed, wv, preferred_element_type=f32)
-    keys = head_norm(keys, key_gain_row)[0]
-    kv_ref[...] = jnp.concatenate([keys, values], axis=1).astype(bf16)
+def key_value_body(normed, weights, key_gain_row, kv_refs):
+    flat = jnp.dot(normed, weights, preferred_element_type=f32)
+    kv_width = flat.shape[1] // 2
+    keys = head_norm(flat[:, :kv_width], key_gain_row)[0]
+    values = flat[:, kv_width:]
+    both = jnp.concatenate([keys, values], axis=1).astype(bf16)
+    for index, kv_ref in enumerate(kv_refs):
+        kv_ref[...] = both[index * CHUNK : (index + 1) * CHUNK, :]
 
 
 def first_norm_kernel(
-    x_hbm, gain_hbm, wk_hbm, wv_hbm, kg_hbm, table_hbm, normed_ref, kv_ref, table_ref,
-    x_ref, gain_ref, wk_ref, wv_ref, kg_ref, row_sems, sems,
+    x_hbm, gain_hbm, wk_hbm, wv_hbm, kg_hbm, table_hbm, normed_ref, table_ref, *refs,
 ):
+    *kv_refs, x_ref, gain_ref, weight_ref, kg_ref, row_sems, sems = refs
     steps = row_sems.shape[0]
     share = x_ref.shape[0] // steps
     row_copies = []
@@ -86,8 +89,8 @@
         )
     gain_copy = pltpu.make_async_copy(gain_hbm, gain_ref, sems.at[0])
     late = [
-        pltpu.make_async_copy(wk_hbm.at[0], wk_ref, sems.at[1]),
-        pltpu.make_async_copy(wv_hbm.at[0], wv_ref, sems.at[2]),
+        pltpu.make_async_copy(wk_hbm.at[0], weight_ref.at[0], sems.at[1]),
+        pltpu.make_async_copy(wv_hbm.at[0], weight_ref.at[1], sems.at[2]),
         pltpu.make_async_copy(kg_hbm, kg_ref, sems.at[3]),
         pltpu.make_async_copy(table_hbm, table_ref, sems.at[4]),
     ]
@@ -103,7 +106,8 @@
         normed_ref[at, :] = (current * lax.rsqrt(mean + norm_eps) * gain).astype(bf16)
     for copy in late:
         copy.wait()
-    key_value_body(normed_ref[...], wk_ref[...], wv_ref[...], kg_ref[0:1, :], kv_ref)
+    weights = jnp.concatenate([weight_ref[0], weight_ref[1]], axis=1)
+    key_value_body(normed_ref[...], weights, kg_ref[0:1, :], kv_refs)
 
 
 def next_norm_kernel(
@@ -123,8 +127,9 @@
             gain = gain_ref[layer_index : layer_index + 1, cols]
             normed_ref[:, cols] = (piece * scale * gain).astype(bf16)
     key_value_body(
-        normed_ref[...], wk_ref[layer_index], wv_ref[layer_index],
-        kg_ref[layer_index : layer_index + 1, :], kv_ref,
+        normed_ref[...],
+        jnp.concatenate([wk_ref[layer_index], wv_ref[layer_index]], axis=1),
+        kg_ref[layer_index : layer_index + 1, :], [kv_ref],
     )
 
 
@@ -172,11 +177,11 @@
     block, layer_index, q_start, row_start, step, starts, prior, q_ref, *refs,
 ):
     piece_refs = refs[:PIECES]
-    tile_ref, wout_ref, keep_ref, send_ref, mixed_ref = refs[PIECES:]
+    tile_ref, wout_ref, *out_refs, mixed_ref = refs[PIECES:]
     heads = q_ref.shape[0]
     kv_width = q_ref.shape[2]
     group = heads * HEAD_DIM // kv_width
-    count = keep_ref.shape[0]
+    count = mixed_ref.shape[0]
     rows = slice(q_start, q_start + count)
 
     pieces = [
@@ -211,19 +216,49 @@
             part = ratio[index * count : (index + 1) * count, at : at + HEAD_DIM]
             mixed_ref[:, into : into + HEAD_DIM] = part.astype(bf16)
 
-    out_projection(block, layer_index, mixed_ref, wout_ref, keep_ref, send_ref)
-
-
-def out_projection(block, layer_index, mixed_ref, wout_ref, keep_ref, send_ref):
+    out_projection(block, layer_index, mixed_ref, wout_ref, *out_refs)
+
+
+def out_projection(block, layer_index, mixed_ref, wout_ref, keep_ref, send_ref=None):
+    parity = lax.axis_index("tp") % 2
+    mixed = mixed_ref[...]
+
+    def project(place):
+        cols = pl.ds(pl.multiple_of(place * block, LANES), block)
+        value = jnp.dot(mixed, wout_ref[layer_index, :, cols], preferred_element_type=f32)
+        return value.astype(bf16)
+
+    if send_ref is None and keep_ref.shape[1] == block:
+        chip = lax.axis_index("tp") // 2
+        keep_ref[...] = project(2 * (1 - chip) + 1 - parity)
+        return
+    for index in range(keep_ref.shape[1] // block):
+        into = slice(index * block, (index + 1) * block)
+        if send_ref is None:
+            keep_ref[:, into] = project(2 * index + 1 - parity)
+        else:
+            send_ref[:, into] = project(2 * index + 1 - parity)
+            keep_ref[:, into] = project(2 * index + parity)
+
+
+def keep_kernel(block, layer_index, mixed_ref, wout_ref, keep_ref):
     parity = lax.axis_index("tp") % 2
     mixed = mixed_ref[...]
     for index in range(keep_ref.shape[1] // block):
-        for target, side in ((send_ref, 1 - parity), (keep_ref, parity)):
-            cols = pl.ds(pl.multiple_of((2 * index + side) * block, LANES), block)
-            partial_value = jnp.dot(
-                mixed, wout_ref[layer_index, :, cols], preferred_element_type=f32
-            )
-            target[:, index * block : (index + 1) * block] = partial_value.astype(bf16)
+        cols = pl.ds(pl.multiple_of((2 * index + parity) * block, LANES), block)
+        value = jnp.dot(mixed, wout_ref[layer_index, :, cols], preferred_element_type=f32)
+        keep_ref[:, index * block : (index + 1) * block] = value.astype(bf16)
+
+
+def project_kernel(block, layer_index, which, mixed_ref, wout_ref, *out_refs):
+    parity = lax.axis_index("tp") % 2
+    chip = lax.axis_index("tp") // 2
+    mixed = mixed_ref[...]
+    for (near_chip, near_core), target in zip(which, out_refs, strict=True):
+        place = 2 * (chip if near_chip else 1 - chip) + (parity if near_core else 1 - parity)
+        cols = pl.ds(pl.multiple_of(place * block, LANES), block)
+        value = jnp.dot(mixed, wout_ref[layer_index, :, cols], preferred_element_type=f32)
+        target[...] = value.astype(bf16)
 
 
 def own_kernel(q_start, starts, q_ref, *refs):
@@ -255,9 +290,7 @@
 
 def joined_kernel(block, layer_index, q_start, starts, q_ref, *refs):
     piece_refs = refs[: len(starts)]
-    (
-        tile_ref, peak_ref, summed_ref, wout_ref, keep_ref, send_ref, mixed_ref,
-    ) = refs[len(starts) :]
+    tile_ref, peak_ref, summed_ref, wout_ref, *out_refs, mixed_ref = refs[len(starts) :]
     heads = q_ref.shape[0]
     kv_width = q_ref.shape[2]
     group = heads * HEAD_DIM // kv_width
@@ -301,7 +334,7 @@
             wide = jnp.concatenate([scale[head]] * (summed.shape[2] // LANES), axis=1)
             put(head, summed_ref[head] * wide + summed[head])
 
-    out_projection(block, layer_index, mixed_ref, wout_ref, keep_ref, send_ref)
+    out_projection(block, layer_index, mixed_ref, wout_ref, *out_refs)
 
 
 def add_kernel(a_ref, b_ref, out_ref):
@@ -338,16 +371,16 @@
     out_hbm, held_ref, sems = refs[-3:]
     cols = pl.ds(pl.multiple_of((lax.axis_index("tp") // 2) * block, LANES), block)
     copies = []
-    for index, (start, inner) in enumerate(places):
-        x_ref, a_ref, b_ref = refs[3 * index : 3 * index + 3]
-        count = a_ref.shape[0]
-        added = a_ref[...].astype(f32) + b_ref[...].astype(f32)
-        held = x_ref[inner : inner + count, cols].astype(f32)
+    at = 0
+    for index, (start, count, addends) in enumerate(places):
+        added = sum(ref[...].astype(f32) for ref in refs[at + 1 : at + 1 + addends])
+        held = refs[at][:, cols].astype(f32)
         held_ref[start : start + count, :] = (held + added).astype(bf16)
         span = pl.ds(start, count)
         copy = pltpu.make_async_copy(held_ref.at[span, :], out_hbm.at[span, :], sems.at[index])
         copy.start()
         copies.append(copy)
+        at += 1 + addends
     for copy in copies:
         copy.wait()
 
@@ -390,16 +423,26 @@
             name="queries",
         )(normed, w_query, query_gain)
 
-    def attention(layer_index, part, inner, count, query, q_start, pieces, starts):
+    def attention_out(early, count):
+        if early:
+            return dict(
+                out_shape=[out((count, early)), out((count, query_width))],
+                out_specs=[whole, whole],
+            )
+        return dict(
+            out_shape=[out((count, half))] * 2,
+            out_specs=[whole, whole],
+            scratch_shapes=[pltpu.VMEM((count, query_width), bf16)],
+        )
+
+    def attention(layer_index, part, inner, count, query, q_start, pieces, starts, early=0):
         return pl.pallas_call(
             functools.partial(
                 attention_kernel, block, layer_index, q_start, inner,
                 STEPS[count], starts, max(0, PIECES - 1 - part),
             ),
-            out_shape=[out((count, half))] * 2,
+            **attention_out(early, count),
             in_specs=[whole] * (PIECES + 3),
-            out_specs=[whole, whole],
-            scratch_shapes=[pltpu.VMEM((count, query_width), bf16)],
             compiler_params=params(),
             cost_estimate=cost(
                 2 * CHUNK * query_width * (width + 4 * WINDOW), 2 * width * query_width
@@ -421,31 +464,50 @@
             name="own_part",
         )(query, *pieces[prior:], tiles[layer_index])
 
-    def joined(layer_index, part, query, q_start, pieces, starts, own):
+    def joined(layer_index, part, query, q_start, pieces, starts, own, early=0):
         prior = max(0, PIECES - 1 - part)
         return pl.pallas_call(
             functools.partial(joined_kernel, block, layer_index, q_start, starts[:prior]),
-            out_shape=[out((CHUNK, half))] * 2,
+            **attention_out(early, CHUNK),
             in_specs=[whole] * (prior + 5),
-            out_specs=[whole, whole],
-            scratch_shapes=[pltpu.VMEM((CHUNK, query_width), bf16)],
             compiler_params=params(),
             cost_estimate=cost(1e9, 2 * width * query_width),
             name="joined",
         )(query, *pieces[:prior], tiles[layer_index], *own, w_out)
 
-    normed, kv, table = pl.pallas_call(
+    def project(layer_index, mixed, which):
+        return pl.pallas_call(
+            functools.partial(project_kernel, block, layer_index, which),
+            out_shape=[out((mixed.shape[0], block))] * len(which),
+            in_specs=[whole, whole],
+            out_specs=[whole] * len(which),
+            compiler_params=params(),
+            cost_estimate=cost(3e8, 1e6),
+            name="project",
+        )(mixed, w_out)
+
+    def added(one, two):
+        return pl.pallas_call(
+            add_kernel,
+            out_shape=out(one.shape),
+            in_specs=[whole, whole],
+            out_specs=whole,
+            compiler_params=params(),
+            name="add",
+        )(one, two)
+
+    normed, table, *kvs_first = pl.pallas_call(
         first_norm_kernel,
         out_shape=[
-            out((rows, width)), out((rows, 2 * kv_width)), out(rel_bias.shape, f32)
+            out((rows, width)), out(rel_bias.shape, f32),
+            *[out((CHUNK, 2 * kv_width))] * parts,
         ],
         in_specs=[in_hbm] * 6,
-        out_specs=[whole] * 3,
+        out_specs=[whole] * (2 + parts),
         scratch_shapes=[
             pltpu.VMEM(stream.shape, bf16),
             pltpu.VMEM(attn_gain.shape, f32),
-            pltpu.VMEM((width, kv_width), bf16),
-            pltpu.VMEM((width, kv_width), bf16),
+            pltpu.VMEM((2, width, kv_width), bf16),
             pltpu.VMEM(key_gain.shape, f32),
             pltpu.SemaphoreType.DMA((4,)),
             pltpu.SemaphoreType.DMA((5,)),
@@ -454,7 +516,9 @@
         cost_estimate=cost(3e9, 4 * rows * width),
         name="norm_kv_first",
     )(*kept_in_hbm(stream, attn_gain, w_key, w_value, key_gain, rel_bias))
-    kv_prior = passed_along(kv[rows - REACH :], False)
+    first_priors = {}
+    for part in order[: PIECES - 1]:
+        first_priors[part - parts] = passed_along(kvs_first[part], True)
     query = queries(0, normed)
     tiles = []
     for layer_index in range(LAYERS):
@@ -472,30 +536,33 @@
 
     mine, other, kvs, normeds = {}, {}, {}, {}
     for part in order:
-        pieces, starts = [], []
+        pieces, starts = [], [0] * PIECES
         for index in range(PIECES):
             behind = part - (PIECES - 1) + index
-            pieces.append(kv_prior if behind < 0 else kv)
-            starts.append((behind + PIECES - 1 if behind < 0 else behind) * CHUNK)
+            pieces.append(first_priors[behind] if behind < 0 else kvs_first[behind])
         sums = []
         for inner, count in split_rows(False):
             if part < PIECES - 1:
                 own = own_part(0, part, query, part * CHUNK, pieces, starts)
-                keep, send = joined(0, part, query, part * CHUNK, pieces, starts, own)
+                send, mixed = joined(
+                    0, part, query, part * CHUNK, pieces, starts, own, half
+                )
+                keep = pl.pallas_call(
+                    functools.partial(keep_kernel, block, 0),
+                    out_shape=out((CHUNK, half)),
+                    in_specs=[whole, whole],
+                    out_specs=whole,
+                    compiler_params=params(),
+                    cost_estimate=cost(3e8, 1e6),
+                    name="keep",
+                )(mixed, w_out)
             else:
                 keep, send = attention(
                     0, part, inner, count, query, part * CHUNK + inner, pieces, starts
                 )
             received = swapped(send, 0)
             for bit in range(1, bits):
-                summed = pl.pallas_call(
-                    add_kernel,
-                    out_shape=out((count, half)),
-                    in_specs=[whole, whole],
-                    out_specs=whole,
-                    compiler_params=params(),
-                    name="add",
-                )(keep, received)
+                summed = added(keep, received)
                 keep, received = summed, swapped(summed, bit)
             sums += [keep, received]
         mine[part] = pl.pallas_call(
@@ -529,26 +596,39 @@
         for index in range(PIECES):
             behind = part - (PIECES - 1) + index
             pieces.append(priors[behind] if behind < 0 else kvs[behind])
-        for inner, count in split_rows(False):
-            if part == 0:
-                own = own_part(1, part, query, 0, pieces, [0] * PIECES)
-                keep, send = joined(1, part, query, 0, pieces, [0] * PIECES, own)
-            else:
-                keep, send = attention(1, part, inner, count, query, inner, pieces, [0] * PIECES)
+        early = block if bits == 2 and part == 0 else 0
+        if part == 0:
+            own = own_part(1, part, query, 0, pieces, [0] * PIECES)
+            keep, send = joined(1, part, query, 0, pieces, [0] * PIECES, own, early)
+        else:
+            keep, send = attention(
+                1, part, 0, CHUNK, query, 0, pieces, [0] * PIECES, early
+            )
+        if early:
+            first, mixed = keep, send
+            received = swapped(first, 0)
+            send = project(1, mixed, ((False, True),))[0]
+            summed = added(send, received)
+            received = swapped(summed, 1)
+            keep, other = project(1, mixed, ((True, True), (True, False)))
+            aside = swapped(other, 0)
+            addends = [keep, aside, received]
+        else:
             received = swapped(send, 0)
             for bit in range(1, bits):
                 left = keep.shape[1] // 2
                 keep, send = pl.pallas_call(
                     functools.partial(split_add_kernel, block, bit),
-                    out_shape=[out((count, left))] * 2,
+                    out_shape=[out((CHUNK, left))] * 2,
                     in_specs=[whole, whole],
                     out_specs=[whole, whole],
                     compiler_params=params(),
                     name="split_add",
                 )(keep, received)
                 received = swapped(send, bit)
-            places.append((part * CHUNK + inner, inner))
-            outs += [mine[part], keep, received]
+            addends = [keep, received]
+        places.append((part * CHUNK, CHUNK, len(addends)))
+        outs += [mine[part], *addends]
 
     return pl.pallas_call(
         functools.partial(result_kernel, block, places),

time: 51.5 us -> 50.9 us (0.988)
  starting transfers between devices: 16.6 us -> 12.5 us
  waiting for transfers between devices: 20 us -> 23 us
    ppermute x3 -> x4, starting transfers between devices: 10.4 us -> 7.03 us  [passed_along(): return lax.ppermute(value, 'sp', edges)]
    ppermute x3 -> x4, waiting for transfers between devices: 2.5 us -> 5.17 us  [passed_along(): return lax.ppermute(value, 'sp', edges)]
    pallas_call x3 -> x8, Pallas kernels: 2.73 us -> 3.86 us  [the longest x1 2.5 us: layers(): pl.pallas_call(first_norm_kernel, out_shape=[out((rows, width)), out(rel_...]
    ppermute x10 -> x11, starting transfers between devices: 6.17 us -> 5.45 us  [swapped(): return lax.ppermute(value, 'tp', [(d, d ^ 1 << bit) for d in range(size)])]
    pallas_call x3, Pallas kernels: 1.83 us -> 1.31 us  [joined(): pl.pallas_call(functools.partial(joined_kernel, block, layer_index, q_sta...]
    ppermute x10 -> x11, waiting for transfers between devices: 17.5 us -> 17.8 us  [swapped(): return lax.ppermute(value, 'tp', [(d, d ^ 1 << bit) for d in range(size)])]
  transfers between devices with their start and end apart: 13 -> 15, of which waited for: 7 -> 9; matrix products, arithmetic and copies ran while one was open for 0% -> 0% of each run, Pallas kernels for 20% -> 23%
where the time goes in v5:
time: 50.9 us; the launch traced here: 50.7 us
  waiting for transfers between devices  23 us (45%)
  Pallas kernels  14.8 us (29%)
  starting transfers between devices  12.5 us (25%)
    ppermute x11, waiting for transfers between devices, swapped(): return lax.ppermute(value, 'tp', [(d, d ^ 1 << bit) for d in range(size)])  17.8 us
    ppermute x4, starting transfers between devices, passed_along(): return lax.ppermute(value, 'sp', edges)  7.03 us
    ppermute x11, starting transfers between devices, swapped(): return lax.ppermute(value, 'tp', [(d, d ^ 1 << bit) for d in range(size)])  5.45 us
    ppermute x4, waiting for transfers between devices, passed_along(): return lax.ppermute(value, 'sp', edges)  5.17 us
    pallas_call x3, Pallas kernels, queries(): pl.pallas_call(functools.partial(query_kernel, layer_index), out_shape=ou...  2.54 us
    pallas_call x1, Pallas kernels, layers(): pl.pallas_call(first_norm_kernel, out_shape=[out((rows, width)), out(rel_...  2.5 us
    pallas_call x3, Pallas kernels, own_part(): pl.pallas_call(functools.partial(own_kernel, q_start, starts[prior:]), ou...  1.82 us
    pallas_call x2, Pallas kernels, layers(): pl.pallas_call(functools.partial(bias_kernel, layer_index), out_shape=out...  1.55 us
  transfers between devices with their start and end apart: 15, of which 9 were waited for; matrix products, arithmetic and copies ran while one was open for 0% of the time, Pallas kernels for 23%

profile of v5, /device:TPU:0, one launch (start us, length us, event | category | flops | bytes accessed | tf_op | source)
XLA Modules:
  0.0 50.7 jit_solution(8726674828358372471)
XLA Ops:
  0.0 2.5 %norm_kv_first.1 = (bf16[256,2048]{1,0:T(8,128)(2,1)S(1)}, f32[2,8,257]{2,1,0:T(8,128)S(1)}, bf16[128,256]{1,0:T(8,128)(2,1)S(1)}, bf16[128,256]{1,0:T(8,128)(2,1)S(1)}) custom-call(bf16[256,2048]{1,0:T(8,128)(2,1)} %x_ref.3, f32[2,2048]{1,0:T(2,128)} %gain_ref.3, bf16[2,2048,128]{2,1,0:T(8,128)(2,1)} %wk_ref.3, bf16[2,2048,128]{2,1,0:T(8,128)(2,1)} %wv_ref.3, ...), custom_call_target="tpu_custom_call" | custom-call | flops 3000000000 | bytes 2097152 | tf_op jit(solution)/shard_map/norm_kv_first/pallas_call | solution.py:499
  2.5 3.0 %collective-permute-start = (bf16[128,256]{1,0:T(8,128)(2,1)S(1)}, bf16[128,256]{1,0:T(8,128)(2,1)S(1)}, u32[]{:S(2)}, u32[]{:S(2)}) collective-permute-start(bf16[128,256]{1,0:T(8,128)(2,1)S(1)} %get-tuple-element.32.refs_1_), channel_id=1, source_target_pairs={{0,4},{4,8},{8,12},{12,16},{16,20},{20,24},{24,28},{28,0},{1,5},{5... | collective-permute-start | bytes 196616 | tf_op jit(solution)/shard_map/ppermute | solution.py:396
  5.6 1.5 %collective-permute-start.5 = (bf16[128,256]{1,0:T(8,128)(2,1)S(1)}, bf16[128,256]{1,0:T(8,128)(2,1)S(1)}, u32[]{:S(2)}, u32[]{:S(2)}) collective-permute-start(bf16[128,256]{1,0:T(8,128)(2,1)S(1)} %get-tuple-element.34.refs_0_), channel_id=1, source_target_pairs={{0,4},{4,8},{8,12},{12,16},{16,20},{20,24},{24,28},{28,0},{1,5},{5... | collective-permute-start | bytes 196616 | tf_op jit(solution)/shard_map/ppermute | solution.py:396
  7.1 0.8 %bias_tiles.2.refs_2_.refs_1_ = f32[8,128,384]{2,1,0:T(8,128)S(1)} custom-call(f32[2,8,257]{2,1,0:T(8,128)S(1)} %get-tuple-element.33.table_ref), custom_call_target="tpu_custom_call" | custom-call | flops 2000000000 | bytes 1000000 | tf_op jit(solution)/shard_map/bias_tiles/pallas_call | solution.py:526
  7.9 1.1 %queries.3.q_ref = bf16[8,256,128]{2,1,0:T(8,128)(2,1)S(1)} custom-call(bf16[256,2048]{1,0:T(8,128)(2,1)S(1)} %get-tuple-element.31.normed_ref, bf16[2,2048,512]{2,1,0:T(8,128)(2,1)S(1)} %copy-done.6, f32[2,64]{1,0:T(2,128)S(1)} %copy-done.7), custom_call_target="tpu_custom_call" | custom-call | flops 2000000000 | bytes 2097152 | tf_op jit(solution)/shard_map/queries/pallas_call | solution.py:416
  9.0 0.6 %own_part.3 = (f32[8,128,128]{2,1,0:T(8,128)S(1)}, f32[8,128,256]{2,1,0:T(8,128)S(1)}) custom-call(bf16[8,256,128]{2,1,0:T(8,128)(2,1)S(1)} %queries.3.q_ref, bf16[128,256]{1,0:T(8,128)(2,1)S(1)} %get-tuple-element.34.refs_0_, bf16[128,256]{1,0:T(8,128)(2,1)S(1)} %get-tuple-element.32.refs_1_, f32[8,128,384]{2,1,0:T(8,128)S(1)} %bias_tiles.2.refs_2_.refs_1_), custom_call_target="tpu_custom_call" | custom-call | flops 500000000 | bytes 1000000 | tf_op jit(solution)/shard_map/own_part/pallas_call | solution.py:455
  9.6 0.6 %own_part.4 = (f32[8,128,128]{2,1,0:T(8,128)S(1)}, f32[8,128,256]{2,1,0:T(8,128)S(1)}) custom-call(bf16[8,256,128]{2,1,0:T(8,128)(2,1)S(1)} %queries.3.q_ref, bf16[128,256]{1,0:T(8,128)(2,1)S(1)} %get-tuple-element.34.refs_0_, f32[8,128,384]{2,1,0:T(8,128)S(1)} %bias_tiles.2.refs_2_.refs_1_), custom_call_target="tpu_custom_call" | custom-call | flops 500000000 | bytes 1000000 | tf_op jit(solution)/shard_map/own_part/pallas_call | solution.py:455
  10.2 1.1 %collective-permute-done.refs_0_.refs_1_ = bf16[128,256]{1,0:T(8,128)(2,1)S(1)} collective-permute-done((bf16[128,256]{1,0:T(8,128)(2,1)S(1)}, bf16[128,256]{1,0:T(8,128)(2,1)S(1)}, u32[]{:S(2)}, u32[]{:S(2)}) %collective-permute-start) | collective-permute-done | bytes 65568 | tf_op jit(solution)/shard_map/ppermute | solution.py:396
  11.3 0.5 joined.3
  11.9 0.7 %collective-permute-done.5.refs_0_ = bf16[128,256]{1,0:T(8,128)(2,1)S(1)} collective-permute-done((bf16[128,256]{1,0:T(8,128)(2,1)S(1)}, bf16[128,256]{1,0:T(8,128)(2,1)S(1)}, u32[]{:S(2)}, u32[]{:S(2)}) %collective-permute-start.5) | collective-permute-done | bytes 65568 | tf_op jit(solution)/shard_map/ppermute | solution.py:396
  12.5 0.5 joined.4
  13.5 1.8 %collective-permute-start.2 = (bf16[128,1024]{1,0:T(8,128)(2,1)S(1)}, bf16[128,1024]{1,0:T(8,128)(2,1)S(1)}, u32[]{:S(2)}, u32[]{:S(2)}) collective-permute-start(bf16[128,1024]{1,0:T(8,128)(2,1)S(1)} %add.3.refs_0_), channel_id=1, source_target_pairs={{0,2},{1,3},{2,0},{3,1},{4,6},{5,7},{6,4},{7,5},{8,10},{9,11},{10,... | collective-permute-start | bytes 786440 | tf_op jit(solution)/shard_map/ppermute | solution.py:390
  15.7 0.5 %collective-permute-start.7 = (bf16[128,1024]{1,0:T(8,128)(2,1)S(1)}, bf16[128,1024]{1,0:T(8,128)(2,1)S(1)}, u32[]{:S(2)}, u32[]{:S(2)}) collective-permute-start(bf16[128,1024]{1,0:T(8,128)(2,1)S(1)} %add.4.refs_0_), channel_id=1, source_target_pairs={{0,2},{1,3},{2,0},{3,1},{4,6},{5,7},{6,4},{7,5},{8,10},{9,11},{10,... | collective-permute-start | bytes 786440 | tf_op jit(solution)/shard_map/ppermute | solution.py:390
  16.2 6.5 %collective-permute-done.2.refs_1_ = bf16[128,1024]{1,0:T(8,128)(2,1)S(1)} collective-permute-done((bf16[128,1024]{1,0:T(8,128)(2,1)S(1)}, bf16[128,1024]{1,0:T(8,128)(2,1)S(1)}, u32[]{:S(2)}, u32[]{:S(2)}) %collective-permute-start.2) | collective-permute-done | bytes 262176 | tf_op jit(solution)/shard_map/ppermute | solution.py:390
  23.0 4.9 %collective-permute-done.7.refs_1_ = bf16[128,1024]{1,0:T(8,128)(2,1)S(1)} collective-permute-done((bf16[128,1024]{1,0:T(8,128)(2,1)S(1)}, bf16[128,1024]{1,0:T(8,128)(2,1)S(1)}, u32[]{:S(2)}, u32[]{:S(2)}) %collective-permute-start.7) | collective-permute-done | bytes 262176 | tf_op jit(solution)/shard_map/ppermute | solution.py:390
  28.1 0.8 %bias_tiles.3.refs_3_.refs_1_.refs_2_ = f32[8,128,384]{2,1,0:T(8,128)S(1)} custom-call(f32[2,8,257]{2,1,0:T(8,128)S(1)} %get-tuple-element.33.table_ref), custom_call_target="tpu_custom_call" | custom-call | flops 2000000000 | bytes 1000000 | tf_op jit(solution)/shard_map/bias_tiles/pallas_call | solution.py:526
  28.9 0.6 %norm_kv_next.2 = (bf16[128,2048]{1,0:T(8,128)(2,1)S(1)}, bf16[128,256]{1,0:T(8,128)(2,1)S(1)}) custom-call(bf16[128,1024]{1,0:T(8,128)(2,1)S(1)} %residual.2.mine_ref.refs_0_, bf16[128,1024]{1,0:T(8,128)(2,1)S(1)} %collective-permute-done.3.other_ref, f32[2,2048]{1,0:T(2,128)S(1)} %copy-done.4, bf16[2,2048,128]{2,1,0:T(8,128)(2,1)S(1)} %copy-done.1, ...), custom_call_target="tpu_custom_call" | custom-call | flops 134217728 | bytes 1048576 | tf_op jit(solution)/shard_map/norm_kv_next/pallas_call | solution.py:580
  29.6 0.9 %collective-permute-start.4 = (bf16[128,256]{1,0:T(8,128)(2,1)S(1)}, bf16[128,256]{1,0:T(8,128)(2,1)S(1)}, u32[]{:S(2)}, u32[]{:S(2)}) collective-permute-start(bf16[128,256]{1,0:T(8,128)(2,1)S(1)} %get-tuple-element.40.refs_2_), channel_id=1, source_target_pairs={{0,4},{4,8},{8,12},{12,16},{16,20},{20,24},{24,28},{28,0},{1,5},{5... | collective-permute-start | bytes 196616 | tf_op jit(solution)/shard_map/ppermute | solution.py:396
  30.5 0.7 %queries.4.q_ref = bf16[8,128,128]{2,1,0:T(8,128)(2,1)S(1)} custom-call(bf16[128,2048]{1,0:T(8,128)(2,1)S(1)} %get-tuple-element.39.normed_ref, bf16[2,2048,512]{2,1,0:T(8,128)(2,1)S(1)} %copy-done.6, f32[2,64]{1,0:T(2,128)S(1)} %copy-done.7), custom_call_target="tpu_custom_call" | custom-call | flops 2000000000 | bytes 2097152 | tf_op jit(solution)/shard_map/queries/pallas_call | solution.py:416
  31.2 0.6 %norm_kv_next.3 = (bf16[128,2048]{1,0:T(8,128)(2,1)S(1)}, bf16[128,256]{1,0:T(8,128)(2,1)S(1)}) custom-call(bf16[128,1024]{1,0:T(8,128)(2,1)S(1)} %residual.3.mine_ref.refs_3_, bf16[128,1024]{1,0:T(8,128)(2,1)S(1)} %collective-permute-done.8.other_ref, f32[2,2048]{1,0:T(2,128)S(1)} %copy-done.4, bf16[2,2048,128]{2,1,0:T(8,128)(2,1)S(1)} %copy-done.1, ...), custom_call_target="tpu_custom_call" | custom-call | flops 134217728 | bytes 1048576 | tf_op jit(solution)/shard_map/norm_kv_next/pallas_call | solution.py:580
  31.9 0.8 %queries.5.q_ref = bf16[8,128,128]{2,1,0:T(8,128)(2,1)S(1)} custom-call(bf16[128,2048]{1,0:T(8,128)(2,1)S(1)} %get-tuple-element.50.normed_ref, bf16[2,2048,512]{2,1,0:T(8,128)(2,1)S(1)} %copy-done.6, f32[2,64]{1,0:T(2,128)S(1)} %copy-done.7), custom_call_target="tpu_custom_call" | custom-call | flops 2000000000 | bytes 2097152 | tf_op jit(solution)/shard_map/queries/pallas_call | solution.py:416
  32.6 1.6 %collective-permute-start.11 = (bf16[128,256]{1,0:T(8,128)(2,1)S(1)}, bf16[128,256]{1,0:T(8,128)(2,1)S(1)}, u32[]{:S(2)}, u32[]{:S(2)}) collective-permute-start(bf16[128,256]{1,0:T(8,128)(2,1)S(1)} %get-tuple-element.45.refs_1_.refs_0_), channel_id=1, source_target_pairs={{0,4},{4,8},{8,12},{12,16},{16,20},{20,24},{24,28},{28,0},{1,5},{5... | collective-permute-start | bytes 196616 | tf_op jit(solution)/shard_map/ppermute | solution.py:396
  34.2 2.6 %collective-permute-done.4.refs_0_.refs_1_ = bf16[128,256]{1,0:T(8,128)(2,1)S(1)} collective-permute-done((bf16[128,256]{1,0:T(8,128)(2,1)S(1)}, bf16[128,256]{1,0:T(8,128)(2,1)S(1)}, u32[]{:S(2)}, u32[]{:S(2)}) %collective-permute-start.4) | collective-permute-done | bytes 65568 | tf_op jit(solution)/shard_map/ppermute | solution.py:396
  36.8 1.4 %attention.1 = (bf16[128,1024]{1,0:T(8,128)(2,1)S(1)}, bf16[128,1024]{1,0:T(8,128)(2,1)S(1)}) custom-call(bf16[8,128,128]{2,1,0:T(8,128)(2,1)S(1)} %queries.4.q_ref, bf16[128,256]{1,0:T(8,128)(2,1)S(1)} %collective-permute-done.4.refs_0_.refs_1_, bf16[128,256]{1,0:T(8,128)(2,1)S(1)} %get-tuple-element.45.refs_1_.refs_0_, ...), custom_call_target="tpu_custom_call" | custom-call | flops 469762048 | bytes 2097152 | tf_op jit(solution)/shard_map/attention/pallas_call | solution.py:439
  38.3 0.6 %own_part.5 = (f32[8,128,128]{2,1,0:T(8,128)S(1)}, f32[8,128,256]{2,1,0:T(8,128)S(1)}) custom-call(bf16[8,128,128]{2,1,0:T(8,128)(2,1)S(1)} %queries.5.q_ref, bf16[128,256]{1,0:T(8,128)(2,1)S(1)} %get-tuple-element.45.refs_1_.refs_0_, f32[8,128,384]{2,1,0:T(8,128)S(1)} %bias_tiles.3.refs_3_.refs_1_.refs_2_), custom_call_target="tpu_custom_call" | custom-call | flops 500000000 | bytes 1000000 | tf_op jit(solution)/shard_map/own_part/pallas_call | solution.py:455
  38.9 0.8 %collective-permute-done.11.refs_0_ = bf16[128,256]{1,0:T(8,128)(2,1)S(1)} collective-permute-done((bf16[128,256]{1,0:T(8,128)(2,1)S(1)}, bf16[128,256]{1,0:T(8,128)(2,1)S(1)}, u32[]{:S(2)}, u32[]{:S(2)}) %collective-permute-start.11) | collective-permute-done | bytes 65568 | tf_op jit(solution)/shard_map/ppermute | solution.py:396
  40.5 0.5 %collective-permute-start.12 = (bf16[128,512]{1,0:T(8,128)(2,1)S(1)}, bf16[128,512]{1,0:T(8,128)(2,1)S(1)}, u32[]{:S(2)}, u32[]{:S(2)}) collective-permute-start(bf16[128,512]{1,0:T(8,128)(2,1)S(1)} %get-tuple-element.55), channel_id=1, source_target_pairs={{0,1},{1,0},{2,3},{3,2},{4,5},{5,4},{6,7},{7,6},{8,9},{9,8},{10,11... | collective-permute-start | bytes 393224 | tf_op jit(solution)/shard_map/ppermute | solution.py:390
  41.5 1.6 %collective-permute-start.14 = (bf16[128,512]{1,0:T(8,128)(2,1)S(1)}, bf16[128,512]{1,0:T(8,128)(2,1)S(1)}, u32[]{:S(2)}, u32[]{:S(2)}) collective-permute-start(bf16[128,512]{1,0:T(8,128)(2,1)S(1)} %add.5), channel_id=1, source_target_pairs={{0,2},{1,3},{2,0},{3,1},{4,6},{5,7},{6,4},{7,5},{8,10},{9,11},{10,... | collective-permute-start | bytes 393224 | tf_op jit(solution)/shard_map/ppermute | solution.py:390
  43.1 0.6 %collective-permute-start.10 = (bf16[128,512]{1,0:T(8,128)(2,1)S(1)}, bf16[128,512]{1,0:T(8,128)(2,1)S(1)}, u32[]{:S(2)}, u32[]{:S(2)}) collective-permute-start(bf16[128,512]{1,0:T(8,128)(2,1)S(1)} %get-tuple-element.49), channel_id=1, source_target_pairs={{0,2},{1,3},{2,0},{3,1},{4,6},{5,7},{6,4},{7,5},{8,10},{9,11},{10,... | collective-permute-start | bytes 393224 | tf_op jit(solution)/shard_map/ppermute | solution.py:390
  43.7 4.2 %collective-permute-done.14.refs_6_ = bf16[128,512]{1,0:T(8,128)(2,1)S(1)} collective-permute-done((bf16[128,512]{1,0:T(8,128)(2,1)S(1)}, bf16[128,512]{1,0:T(8,128)(2,1)S(1)}, u32[]{:S(2)}, u32[]{:S(2)}) %collective-permute-start.14) | collective-permute-done | bytes 131104 | tf_op jit(solution)/shard_map/ppermute | solution.py:390
  47.9 2.0 %collective-permute-done.10.refs_2_ = bf16[128,512]{1,0:T(8,128)(2,1)S(1)} collective-permute-done((bf16[128,512]{1,0:T(8,128)(2,1)S(1)}, bf16[128,512]{1,0:T(8,128)(2,1)S(1)}, u32[]{:S(2)}, u32[]{:S(2)}) %collective-permute-start.10) | collective-permute-done | bytes 131104 | tf_op jit(solution)/shard_map/ppermute | solution.py:390
  49.9 0.8 %result.1 = bf16[256,512]{1,0:T(8,128)(2,1)} custom-call(bf16[128,1024]{1,0:T(8,128)(2,1)S(1)} %residual.2.mine_ref.refs_0_, bf16[128,512]{1,0:T(8,128)(2,1)S(1)} %get-tuple-element.48.refs_1_, bf16[128,512]{1,0:T(8,128)(2,1)S(1)} %collective-permute-done.10.refs_2_, bf16[128,1024]{1,0:T(8,128)(2,1)S(1)} %residual.3.mine_ref.refs_3_, ...), custom_call_target="tpu_custom_call" | custom-call | tf_op jit(solution)/shard_map/result/pallas_call | solution.py:633
  (40 shorter events, 2.7 us)
Async XLA Ops:
  2.5 5.4 %copy-start.6 = (bf16[2,2048,512]{2,1,0:T(8,128)(2,1)S(1)}, bf16[2,2048,512]{2,1,0:T(8,128)(2,1)}, u32[]{:S(2)}) copy-start(bf16[2,2048,512]{2,1,0:T(8,128)(2,1)} %wq_ref.5) | copy-start | bytes 12582916
  2.5 5.4 %copy-start.7 = (f32[2,64]{1,0:T(2,128)S(1)}, f32[2,64]{1,0:T(2,128)}, u32[]{:S(2)}) copy-start(f32[2,64]{1,0:T(2,128)} %qg_ref.5) | copy-start | bytes 1540
  2.5 8.8 %collective-permute-start = (bf16[128,256]{1,0:T(8,128)(2,1)S(1)}, bf16[128,256]{1,0:T(8,128)(2,1)S(1)}, u32[]{:S(2)}, u32[]{:S(2)}) collective-permute-start(bf16[128,256]{1,0:T(8,128)(2,1)S(1)} %get-tuple-element.32.refs_1_), channel_id=1, source_target_pairs={{0,4},{4,8},{8,12},{12,16},{16,20},{20,24},{24,28},{28,0},{1,5},{5... | collective-permute-start | bytes 196616 | tf_op jit(solution)/shard_map/ppermute | solution.py:396
  5.6 7.0 %collective-permute-start.5 = (bf16[128,256]{1,0:T(8,128)(2,1)S(1)}, bf16[128,256]{1,0:T(8,128)(2,1)S(1)}, u32[]{:S(2)}, u32[]{:S(2)}) collective-permute-start(bf16[128,256]{1,0:T(8,128)(2,1)S(1)} %get-tuple-element.34.refs_0_), channel_id=1, source_target_pairs={{0,4},{4,8},{8,12},{12,16},{16,20},{20,24},{24,28},{28,0},{1,5},{5... | collective-permute-start | bytes 196616 | tf_op jit(solution)/shard_map/ppermute | solution.py:396
  7.9 3.4 %copy-start = (bf16[2,512,2048]{2,1,0:T(8,128)(2,1)S(1)}, bf16[2,512,2048]{2,1,0:T(8,128)(2,1)}, u32[]{:S(2)}) copy-start(bf16[2,512,2048]{2,1,0:T(8,128)(2,1)} %wout_ref.7) | copy-start | bytes 12582916
  11.8 1.7 %collective-permute-start.1 = (bf16[128,1024]{1,0:T(8,128)(2,1)S(1)}, bf16[128,1024]{1,0:T(8,128)(2,1)S(1)}, u32[]{:S(2)}, u32[]{:S(2)}) collective-permute-start(bf16[128,1024]{1,0:T(8,128)(2,1)S(1)} %get-tuple-element.38), channel_id=1, source_target_pairs={{0,1},{1,0},{2,3},{3,2},{4,5},{5,4},{6,7},{7,6},{8,9},{9,8},{10,11... | collective-permute-start | bytes 786440 | tf_op jit(solution)/shard_map/ppermute | solution.py:390
  13.0 2.6 %collective-permute-start.6 = (bf16[128,1024]{1,0:T(8,128)(2,1)S(1)}, bf16[128,1024]{1,0:T(8,128)(2,1)S(1)}, u32[]{:S(2)}, u32[]{:S(2)}) collective-permute-start(bf16[128,1024]{1,0:T(8,128)(2,1)S(1)} %get-tuple-element.44), channel_id=1, source_target_pairs={{0,1},{1,0},{2,3},{3,2},{4,5},{5,4},{6,7},{7,6},{8,9},{9,8},{10,11... | collective-permute-start | bytes 786440 | tf_op jit(solution)/shard_map/ppermute | solution.py:390
  13.4 9.3 %copy-start.3 = (bf16[256,2048]{1,0:T(8,128)(2,1)S(1)}, bf16[256,2048]{1,0:T(8,128)(2,1)}, u32[]{:S(2)}) copy-start(bf16[256,2048]{1,0:T(8,128)(2,1)} %x_ref.3) | copy-start | bytes 3145732
  13.5 9.2 %collective-permute-start.2 = (bf16[128,1024]{1,0:T(8,128)(2,1)S(1)}, bf16[128,1024]{1,0:T(8,128)(2,1)S(1)}, u32[]{:S(2)}, u32[]{:S(2)}) collective-permute-start(bf16[128,1024]{1,0:T(8,128)(2,1)S(1)} %add.3.refs_0_), channel_id=1, source_target_pairs={{0,2},{1,3},{2,0},{3,1},{4,6},{5,7},{6,4},{7,5},{8,10},{9,11},{10,... | collective-permute-start | bytes 786440 | tf_op jit(solution)/shard_map/ppermute | solution.py:390
  15.7 12.2 %collective-permute-start.7 = (bf16[128,1024]{1,0:T(8,128)(2,1)S(1)}, bf16[128,1024]{1,0:T(8,128)(2,1)S(1)}, u32[]{:S(2)}, u32[]{:S(2)}) collective-permute-start(bf16[128,1024]{1,0:T(8,128)(2,1)S(1)} %add.4.refs_0_), channel_id=1, source_target_pairs={{0,2},{1,3},{2,0},{3,1},{4,6},{5,7},{6,4},{7,5},{8,10},{9,11},{10,... | collective-permute-start | bytes 786440 | tf_op jit(solution)/shard_map/ppermute | solution.py:390
  22.9 6.0 %copy-start.1 = (bf16[2,2048,128]{2,1,0:T(8,128)(2,1)S(1)}, bf16[2,2048,128]{2,1,0:T(8,128)(2,1)}, u32[]{:S(2)}) copy-start(bf16[2,2048,128]{2,1,0:T(8,128)(2,1)} %wk_ref.3) | copy-start | bytes 3145732
  22.9 6.0 %copy-start.2 = (bf16[2,2048,128]{2,1,0:T(8,128)(2,1)S(1)}, bf16[2,2048,128]{2,1,0:T(8,128)(2,1)}, u32[]{:S(2)}) copy-start(bf16[2,2048,128]{2,1,0:T(8,128)(2,1)} %wv_ref.3) | copy-start | bytes 3145732
  22.9 6.0 %copy-start.4 = (f32[2,2048]{1,0:T(2,128)S(1)}, f32[2,2048]{1,0:T(2,128)}, u32[]{:S(2)}) copy-start(f32[2,2048]{1,0:T(2,128)} %gain_ref.3) | copy-start | bytes 49156
  22.9 6.0 %copy-start.5 = (f32[2,64]{1,0:T(2,128)S(1)}, f32[2,64]{1,0:T(2,128)}, u32[]{:S(2)}) copy-start(f32[2,64]{1,0:T(2,128)} %kg_ref.3) | copy-start | bytes 1540
  22.9 6.0 %collective-permute-start.3 = (bf16[128,1024]{1,0:T(8,128)(2,1)S(1)}, bf16[128,1024]{1,0:T(8,128)(2,1)S(1)}, u32[]{:S(2)}, u32[]{:S(2)}) collective-permute-start(bf16[128,1024]{1,0:T(8,128)(2,1)S(1)} %residual.2.mine_ref.refs_0_), channel_id=1, source_target_pairs={{0,1},{1,0},{2,3},{3,2},{4,5},{5,4},{6,7},{7,6},{8,9},{9,8},{10,11... | collective-permute-start | bytes 786440 | tf_op jit(solution)/shard_map/ppermute | solution.py:390
  28.0 3.2 %collective-permute-start.8 = (bf16[128,1024]{1,0:T(8,128)(2,1)S(1)}, bf16[128,1024]{1,0:T(8,128)(2,1)S(1)}, u32[]{:S(2)}, u32[]{:S(2)}) collective-permute-start(bf16[128,1024]{1,0:T(8,128)(2,1)S(1)} %residual.3.mine_ref.refs_3_), channel_id=1, source_target_pairs={{0,1},{1,0},{2,3},{3,2},{4,5},{5,4},{6,7},{7,6},{8,9},{9,8},{10,11... | collective-permute-start | bytes 786440 | tf_op jit(solution)/shard_map/ppermute | solution.py:390
  29.6 7.2 %collective-permute-start.4 = (bf16[128,256]{1,0:T(8,128)(2,1)S(1)}, bf16[128,256]{1,0:T(8,128)(2,1)S(1)}, u32[]{:S(2)}, u32[]{:S(2)}) collective-permute-start(bf16[128,256]{1,0:T(8,128)(2,1)S(1)} %get-tuple-element.40.refs_2_), channel_id=1, source_target_pairs={{0,4},{4,8},{8,12},{12,16},{16,20},{20,24},{24,28},{28,0},{1,5},{5... | collective-permute-start | bytes 196616 | tf_op jit(solution)/shard_map/ppermute | solution.py:396
  32.6 7.0 %collective-permute-start.11 = (bf16[128,256]{1,0:T(8,128)(2,1)S(1)}, bf16[128,256]{1,0:T(8,128)(2,1)S(1)}, u32[]{:S(2)}, u32[]{:S(2)}) collective-permute-start(bf16[128,256]{1,0:T(8,128)(2,1)S(1)} %get-tuple-element.45.refs_1_.refs_0_), channel_id=1, source_target_pairs={{0,4},{4,8},{8,12},{12,16},{16,20},{20,24},{24,28},{28,0},{1,5},{5... | collective-permute-start | bytes 196616 | tf_op jit(solution)/shard_map/ppermute | solution.py:396
  38.2 4.9 %collective-permute-start.9 = (bf16[128,1024]{1,0:T(8,128)(2,1)S(1)}, bf16[128,1024]{1,0:T(8,128)(2,1)S(1)}, u32[]{:S(2)}, u32[]{:S(2)}) collective-permute-start(bf16[128,1024]{1,0:T(8,128)(2,1)S(1)} %get-tuple-element.47), channel_id=1, source_target_pairs={{0,1},{1,0},{2,3},{3,2},{4,5},{5,4},{6,7},{7,6},{8,9},{9,8},{10,11... | collective-permute-start | bytes 786440 | tf_op jit(solution)/shard_map/ppermute | solution.py:390
  40.0 1.4 %collective-permute-start.13 = (bf16[128,512]{1,0:T(8,128)(2,1)S(1)}, bf16[128,512]{1,0:T(8,128)(2,1)S(1)}, u32[]{:S(2)}, u32[]{:S(2)}) collective-permute-start(bf16[128,512]{1,0:T(8,128)(2,1)S(1)} %get-tuple-element.56), channel_id=1, source_target_pairs={{0,1},{1,0},{2,3},{3,2},{4,5},{5,4},{6,7},{7,6},{8,9},{9,8},{10,11... | collective-permute-start | bytes 393224 | tf_op jit(solution)/shard_map/ppermute | solution.py:390
  40.5 3.3 %collective-permute-start.12 = (bf16[128,512]{1,0:T(8,128)(2,1)S(1)}, bf16[128,512]{1,0:T(8,128)(2,1)S(1)}, u32[]{:S(2)}, u32[]{:S(2)}) collective-permute-start(bf16[128,512]{1,0:T(8,128)(2,1)S(1)} %get-tuple-element.55), channel_id=1, source_target_pairs={{0,1},{1,0},{2,3},{3,2},{4,5},{5,4},{6,7},{7,6},{8,9},{9,8},{10,11... | collective-permute-start | bytes 393224 | tf_op jit(solution)/shard_map/ppermute | solution.py:390
  41.5 6.4 %collective-permute-start.14 = (bf16[128,512]{1,0:T(8,128)(2,1)S(1)}, bf16[128,512]{1,0:T(8,128)(2,1)S(1)}, u32[]{:S(2)}, u32[]{:S(2)}) collective-permute-start(bf16[128,512]{1,0:T(8,128)(2,1)S(1)} %add.5), channel_id=1, source_target_pairs={{0,2},{1,3},{2,0},{3,1},{4,6},{5,7},{6,4},{7,5},{8,10},{9,11},{10,... | collective-permute-start | bytes 393224 | tf_op jit(solution)/shard_map/ppermute | solution.py:390
  43.1 6.8 %collective-permute-start.10 = (bf16[128,512]{1,0:T(8,128)(2,1)S(1)}, bf16[128,512]{1,0:T(8,128)(2,1)S(1)}, u32[]{:S(2)}, u32[]{:S(2)}) collective-permute-start(bf16[128,512]{1,0:T(8,128)(2,1)S(1)} %get-tuple-element.49), channel_id=1, source_target_pairs={{0,2},{1,3},{2,0},{3,1},{4,6},{5,7},{6,4},{7,5},{8,10},{9,11},{10,... | collective-permute-start | bytes 393224 | tf_op jit(solution)/shard_map/ppermute | solution.py:390

commit v6 on v5

--- a/solution.py
+++ b/solution.py
@@ -76,38 +76,58 @@
 
 
 def first_norm_kernel(
-    x_hbm, gain_hbm, wk_hbm, wv_hbm, kg_hbm, table_hbm, normed_ref, table_ref, *refs,
+    x_hbm, gain_hbm, wk_hbm, wv_hbm, kg_hbm, table_hbm,
+    normed_ref, kv_ref, gain_ref, weight_ref, kg_ref, table_ref,
+    x_ref, row_sems, sems,
 ):
-    *kv_refs, x_ref, gain_ref, weight_ref, kg_ref, row_sems, sems = refs
     steps = row_sems.shape[0]
+    rest = x_hbm.shape[0] - x_ref.shape[0]
     share = x_ref.shape[0] // steps
     row_copies = []
     for index in range(steps):
         at = pl.ds(index * share, share)
+        source = x_hbm.at[pl.ds(rest + index * share, share), :]
         row_copies.append(
-            pltpu.make_async_copy(x_hbm.at[at, :], x_ref.at[at, :], row_sems.at[index])
+            pltpu.make_async_copy(source, x_ref.at[at, :], row_sems.at[index])
         )
     gain_copy = pltpu.make_async_copy(gain_hbm, gain_ref, sems.at[0])
-    late = [
+    weight_copies = [
         pltpu.make_async_copy(wk_hbm.at[0], weight_ref.at[0], sems.at[1]),
         pltpu.make_async_copy(wv_hbm.at[0], weight_ref.at[1], sems.at[2]),
         pltpu.make_async_copy(kg_hbm, kg_ref, sems.at[3]),
+    ]
+    late = [
         pltpu.make_async_copy(table_hbm, table_ref, sems.at[4]),
     ]
-    for copy in [gain_copy] + row_copies + late:
+    for copy in [gain_copy] + row_copies + weight_copies + late:
         copy.start()
     gain_copy.wait()
     gain = gain_ref[0:1, :]
     for index, copy in enumerate(row_copies):
         copy.wait()
         at = slice(index * share, (index + 1) * share)
-        current = x_ref[at, :].astype(f32)
-        mean = jnp.mean(current * current, axis=-1, keepdims=True)
-        normed_ref[at, :] = (current * lax.rsqrt(mean + norm_eps) * gain).astype(bf16)
+        normed_ref[at, :] = normalized(x_ref[at, :], gain)
+    for copy in weight_copies:
+        copy.wait()
+    weights = jnp.concatenate([weight_ref[0], weight_ref[1]], axis=1)
+    key_value_body(normed_ref[...], weights, kg_ref[0:1, :], [kv_ref])
     for copy in late:
         copy.wait()
+
+
+def normalized(rows, gain):
+    current = rows.astype(f32)
+    mean = jnp.mean(current * current, axis=-1, keepdims=True)
+    return (current * lax.rsqrt(mean + norm_eps) * gain).astype(bf16)
+
+
+def rest_norm_kernel(x_ref, gain_ref, weight_ref, kg_ref, *refs):
+    parts = len(refs) // 2
     weights = jnp.concatenate([weight_ref[0], weight_ref[1]], axis=1)
-    key_value_body(normed_ref[...], weights, kg_ref[0:1, :], kv_refs)
+    for index in range(parts):
+        at = slice(index * CHUNK, (index + 1) * CHUNK)
+        refs[index][...] = normalized(x_ref[at, :], gain_ref[0:1, :])
+        key_value_body(refs[index][...], weights, kg_ref[0:1, :], [refs[parts + index]])
 
 
 def next_norm_kernel(
@@ -133,7 +153,8 @@
     )
 
 
-def query_kernel(layer_index, normed_ref, wq_ref, qg_ref, q_ref):
+def query_kernel(layer_index, normed_ref, wq_ref, qg_ref, *refs):
+    q_ref = refs[-1]
     flat = jnp.dot(normed_ref[...], wq_ref[layer_index], preferred_element_type=f32)
     query_body(flat, qg_ref[layer_index : layer_index + 1, :], q_ref)
 
@@ -154,7 +175,8 @@
         q_ref[head] = jnp.concatenate(spread, axis=1).astype(bf16)
 
 
-def bias_kernel(layer_index, table_ref, tile_ref):
+def bias_kernel(layer_index, table_ref, *refs):
+    tile_ref = refs[-1]
     heads, entries = table_ref.shape[1:]
     source = lax.broadcasted_iota(jnp.int32, (entries, LINE), 0)
     offset = lax.broadcasted_iota(jnp.int32, (entries, LINE), 1)
@@ -411,17 +433,17 @@
     parts = rows // CHUNK
     order = list(reversed(range(parts)))
 
-    def queries(layer_index, normed):
+    def queries(layer_index, normed, *ahead):
         count = normed.shape[0]
         return pl.pallas_call(
             functools.partial(query_kernel, layer_index),
             out_shape=out((heads, count, kv_width)),
-            in_specs=[whole] * 3,
+            in_specs=[whole] * (3 + len(ahead)),
             out_specs=whole,
             compiler_params=params(),
             cost_estimate=cost(2e9, 2 * width * query_width),
             name="queries",
-        )(normed, w_query, query_gain)
+        )(normed, w_query, query_gain, *ahead)
 
     def attention_out(early, count):
         if early:
@@ -496,46 +518,56 @@
             name="add",
         )(one, two)
 
-    normed, table, *kvs_first = pl.pallas_call(
+    last = parts - 1
+    normed, kv, gains, weights, key_gains, table = pl.pallas_call(
         first_norm_kernel,
         out_shape=[
-            out((rows, width)), out(rel_bias.shape, f32),
-            *[out((CHUNK, 2 * kv_width))] * parts,
+            out((CHUNK, width)), out((CHUNK, 2 * kv_width)),
+            out(attn_gain.shape, f32), out((2, width, kv_width)),
+            out(key_gain.shape, f32), out(rel_bias.shape, f32),
         ],
         in_specs=[in_hbm] * 6,
-        out_specs=[whole] * (2 + parts),
+        out_specs=[whole] * 6,
         scratch_shapes=[
-            pltpu.VMEM(stream.shape, bf16),
-            pltpu.VMEM(attn_gain.shape, f32),
-            pltpu.VMEM((2, width, kv_width), bf16),
-            pltpu.VMEM(key_gain.shape, f32),
-            pltpu.SemaphoreType.DMA((4,)),
-            pltpu.SemaphoreType.DMA((5,)),
+            pltpu.VMEM((CHUNK, width), bf16),
+            pltpu.SemaphoreType.DMA((2,)),
+            pltpu.SemaphoreType.DMA((6,)),
         ],
         compiler_params=params(),
         cost_estimate=cost(3e9, 4 * rows * width),
         name="norm_kv_first",
     )(*kept_in_hbm(stream, attn_gain, w_key, w_value, key_gain, rel_bias))
+    found = pl.pallas_call(
+        rest_norm_kernel,
+        out_shape=[out((CHUNK, width))] * last + [out((CHUNK, 2 * kv_width))] * last,
+        in_specs=[whole] * 4,
+        out_specs=[whole] * (2 * last),
+        compiler_params=params(),
+        cost_estimate=cost(1e9, 4 * rows * width),
+        name="norm_kv_rest",
+    )(stream, gains, weights, key_gains)
+    normeds_first = [*found[:last], normed]
+    kvs_first = [*found[last:], kv]
     first_priors = {}
     for part in order[: PIECES - 1]:
         first_priors[part - parts] = passed_along(kvs_first[part], True)
-    query = queries(0, normed)
     tiles = []
     for layer_index in range(LAYERS):
         tiles.append(
             pl.pallas_call(
                 functools.partial(bias_kernel, layer_index),
                 out_shape=out((heads, CHUNK, WINDOW), f32),
-                in_specs=[whole],
+                in_specs=[whole] * (2 - layer_index),
                 out_specs=whole,
                 compiler_params=params(),
                 cost_estimate=cost(2e9, 1e6),
                 name="bias_tiles",
-            )(table)
+            )(table, *[w_query] * (1 - layer_index))
         )
 
     mine, other, kvs, normeds = {}, {}, {}, {}
     for part in order:
+        query = queries(0, normeds_first[part], *[w_out] * (part == last))
         pieces, starts = [], [0] * PIECES
         for index in range(PIECES):
             behind = part - (PIECES - 1) + index
@@ -543,9 +575,9 @@
         sums = []
         for inner, count in split_rows(False):
             if part < PIECES - 1:
-                own = own_part(0, part, query, part * CHUNK, pieces, starts)
+                own = own_part(0, part, query, 0, pieces, starts)
                 send, mixed = joined(
-                    0, part, query, part * CHUNK, pieces, starts, own, half
+                    0, part, query, 0, pieces, starts, own, half
                 )
                 keep = pl.pallas_call(
                     functools.partial(keep_kernel, block, 0),
@@ -558,7 +590,7 @@
                 )(mixed, w_out)
             else:
                 keep, send = attention(
-                    0, part, inner, count, query, part * CHUNK + inner, pieces, starts
+                    0, part, inner, count, query, inner, pieces, starts
                 )
             received = swapped(send, 0)
             for bit in range(1, bits):

time: 50.9 us -> 53.1 us (1.043)
  starting transfers between devices: 12.5 us -> 14.3 us
  waiting for transfers between devices: 23 us -> 21.2 us
  local copies, waits for them, and re-layouts: 0.05 us -> 1.48 us
  Pallas kernels: 14.8 us -> 15.7 us
    ppermute x4, waiting for transfers between devices: 5.17 us -> 3.37 us  [passed_along(): return lax.ppermute(value, 'sp', edges)]
    ppermute x4, starting transfers between devices: 7.03 us -> 8.59 us  [passed_along(): return lax.ppermute(value, 'sp', edges)]
    unnamed x16, local copies, waits for them, and re-layouts: 0.05 us -> 1.48 us
    pallas_call x1 -> x2, Pallas kernels: 2.5 us -> 2.96 us  [the longest x1 2.32 us: layers(): pl.pallas_call(first_norm_kernel, out_shape=[out((CHUNK, width)), out((CH...]
    pallas_call x3 -> x4, Pallas kernels: 2.54 us -> 2.87 us  [queries(): pl.pallas_call(functools.partial(query_kernel, layer_index), out_shape=ou...]
  transfers between devices with their start and end apart: 15 -> 15, of which waited for: 9 -> 8; matrix products, arithmetic and copies ran while one was open for 0% -> 0% of each run, Pallas kernels for 23% -> 24%
where the time goes in v6:
time: 53.1 us; the launch traced here: 53 us
  waiting for transfers between devices  21.2 us (40%)
  Pallas kernels  15.7 us (30%)
  starting transfers between devices  14.3 us (27%)
  local copies, waits for them, and re-layouts  1.48 us (3%)
    ppermute x11, waiting for transfers between devices, swapped(): return lax.ppermute(value, 'tp', [(d, d ^ 1 << bit) for d in range(size)])  17.8 us
    ppermute x4, starting transfers between devices, passed_along(): return lax.ppermute(value, 'sp', edges)  8.59 us
    ppermute x11, starting transfers between devices, swapped(): return lax.ppermute(value, 'tp', [(d, d ^ 1 << bit) for d in range(size)])  5.76 us
    ppermute x4, waiting for transfers between devices, passed_along(): return lax.ppermute(value, 'sp', edges)  3.37 us
    pallas_call x4, Pallas kernels, queries(): pl.pallas_call(functools.partial(query_kernel, layer_index), out_shape=ou...  2.87 us
    pallas_call x1, Pallas kernels, layers(): pl.pallas_call(first_norm_kernel, out_shape=[out((CHUNK, width)), out((CH...  2.32 us
    pallas_call x3, Pallas kernels, own_part(): pl.pallas_call(functools.partial(own_kernel, q_start, starts[prior:]), ou...  1.82 us
    pallas_call x2, Pallas kernels, layers(): pl.pallas_call(functools.partial(bias_kernel, layer_index), out_shape=out...  1.55 us
  transfers between devices with their start and end apart: 15, of which 8 were waited for; matrix products, arithmetic and copies ran while one was open for 0% of the time, Pallas kernels for 24%

profile of v6, /device:TPU:0, one launch (start us, length us, event | category | flops | bytes accessed | tf_op | source)
XLA Modules:
  0.0 53.0 jit_solution(5252431553484455006)
XLA Ops:
  0.0 2.3 %norm_kv_first.1 = (bf16[128,2048]{1,0:T(8,128)(2,1)S(1)}, bf16[128,256]{1,0:T(8,128)(2,1)S(1)}, f32[2,2048]{1,0:T(2,128)S(1)}, bf16[2,2048,128]{2,1,0:T(8,128)(...) custom-call(bf16[256,2048]{1,0:T(8,128)(2,1)} %x_ref.5, f32[2,2048]{1,0:T(2,128)} %gain_ref.3, ...), custom_call_target="tpu_custom_call" | custom-call | flops 3000000000 | bytes 2097152 | tf_op jit(solution)/shard_map/norm_kv_first/pallas_call | solution.py:522
  2.3 3.0 %collective-permute-start = (bf16[128,256]{1,0:T(8,128)(2,1)S(1)}, bf16[128,256]{1,0:T(8,128)(2,1)S(1)}, u32[]{:S(2)}, u32[]{:S(2)}) collective-permute-start(bf16[128,256]{1,0:T(8,128)(2,1)S(1)} %get-tuple-element.36.refs_1_), channel_id=1, source_target_pairs={{0,4},{4,8},{8,12},{12,16},{16,20},{20,24},{24,28},{28,0},{1,5},{5... | collective-permute-start | bytes 196616 | tf_op jit(solution)/shard_map/ppermute | solution.py:418
  5.4 0.6 %norm_kv_rest.1 = (bf16[128,2048]{1,0:T(8,128)(2,1)S(1)}, bf16[128,256]{1,0:T(8,128)(2,1)S(1)}) custom-call(bf16[256,2048]{1,0:T(8,128)(2,1)S(1)} %copy-done.4, f32[2,2048]{1,0:T(2,128)S(1)} %get-tuple-element.38.gain_ref, bf16[2,2048,128]{2,1,0:T(8,128)(2,1)S(1)} %get-tuple-element.39.weight_ref, f32[2,64]{1,0:T(2,128)S(1)} %get-tuple-element.40.kg_ref), custom_call_target="tpu_custom_call" | custom-call | flops 1000000000 | bytes 2097152 | tf_op jit(solution)/shard_map/norm_kv_rest/pallas_call | solution.py:540
  6.0 1.6 %collective-permute-start.5 = (bf16[128,256]{1,0:T(8,128)(2,1)S(1)}, bf16[128,256]{1,0:T(8,128)(2,1)S(1)}, u32[]{:S(2)}, u32[]{:S(2)}) collective-permute-start(bf16[128,256]{1,0:T(8,128)(2,1)S(1)} %get-tuple-element.41.refs_0_), channel_id=1, source_target_pairs={{0,4},{4,8},{8,12},{12,16},{16,20},{20,24},{24,28},{28,0},{1,5},{5... | collective-permute-start | bytes 196616 | tf_op jit(solution)/shard_map/ppermute | solution.py:418
  7.6 0.8 %bias_tiles.2.refs_2_.refs_1_ = f32[8,128,384]{2,1,0:T(8,128)S(1)} custom-call(f32[2,8,257]{2,1,0:T(8,128)S(1)} %get-tuple-element.37.table_ref, bf16[2,2048,512]{2,1,0:T(8,128)(2,1)S(1)} %copy-done.3), custom_call_target="tpu_custom_call" | custom-call | flops 2000000000 | bytes 1000000 | tf_op jit(solution)/shard_map/bias_tiles/pallas_call | solution.py:557
  8.4 0.7 %queries.6.q_ref = bf16[8,128,128]{2,1,0:T(8,128)(2,1)S(1)} custom-call(bf16[128,2048]{1,0:T(8,128)(2,1)S(1)} %get-tuple-element.48.normed_ref, bf16[2,2048,512]{2,1,0:T(8,128)(2,1)S(1)} %copy-done.3, f32[2,64]{1,0:T(2,128)S(1)} %copy-done.7), custom_call_target="tpu_custom_call" | custom-call | flops 2000000000 | bytes 2097152 | tf_op jit(solution)/shard_map/queries/pallas_call | solution.py:438
  9.2 1.4 %copy-done = bf16[2,512,2048]{2,1,0:T(8,128)(2,1)S(1)} copy-done((bf16[2,512,2048]{2,1,0:T(8,128)(2,1)S(1)}, bf16[2,512,2048]{2,1,0:T(8,128)(2,1)}, u32[]{:S(2)}) %copy-start) | copy-done | bytes 4194328
  10.6 0.7 %queries.4.q_ref = bf16[8,128,128]{2,1,0:T(8,128)(2,1)S(1)} custom-call(bf16[128,2048]{1,0:T(8,128)(2,1)S(1)} %get-tuple-element.35.normed_ref, bf16[2,2048,512]{2,1,0:T(8,128)(2,1)S(1)} %copy-done.3, f32[2,64]{1,0:T(2,128)S(1)} %copy-done.7, bf16[2,512,2048]{2,1,0:T(8,128)(2,1)S(1)} %copy-done), custom_call_target="tpu_custom_call" | custom-call | flops 2000000000 | bytes 2097152 | tf_op jit(solution)/shard_map/queries/pallas_call | solution.py:438
  11.3 0.6 %own_part.3 = (f32[8,128,128]{2,1,0:T(8,128)S(1)}, f32[8,128,256]{2,1,0:T(8,128)S(1)}) custom-call(bf16[8,128,128]{2,1,0:T(8,128)(2,1)S(1)} %queries.4.q_ref, bf16[128,256]{1,0:T(8,128)(2,1)S(1)} %get-tuple-element.41.refs_0_, bf16[128,256]{1,0:T(8,128)(2,1)S(1)} %get-tuple-element.36.refs_1_, f32[8,128,384]{2,1,0:T(8,128)S(1)} %bias_tiles.2.refs_2_.refs_1_), custom_call_target="tpu_custom_call" | custom-call | flops 500000000 | bytes 1000000 | tf_op jit(solution)/shard_map/own_part/pallas_call | solution.py:477
  11.9 0.6 %own_part.4 = (f32[8,128,128]{2,1,0:T(8,128)S(1)}, f32[8,128,256]{2,1,0:T(8,128)S(1)}) custom-call(bf16[8,128,128]{2,1,0:T(8,128)(2,1)S(1)} %queries.6.q_ref, bf16[128,256]{1,0:T(8,128)(2,1)S(1)} %get-tuple-element.41.refs_0_, f32[8,128,384]{2,1,0:T(8,128)S(1)} %bias_tiles.2.refs_2_.refs_1_), custom_call_target="tpu_custom_call" | custom-call | flops 500000000 | bytes 1000000 | tf_op jit(solution)/shard_map/own_part/pallas_call | solution.py:477
  13.6 0.5 %collective-permute-start.6 = (bf16[128,1024]{1,0:T(8,128)(2,1)S(1)}, bf16[128,1024]{1,0:T(8,128)(2,1)S(1)}, u32[]{:S(2)}, u32[]{:S(2)}) collective-permute-start(bf16[128,1024]{1,0:T(8,128)(2,1)S(1)} %get-tuple-element.52), channel_id=1, source_target_pairs={{0,1},{1,0},{2,3},{3,2},{4,5},{5,4},{6,7},{7,6},{8,9},{9,8},{10,11... | collective-permute-start | bytes 786440 | tf_op jit(solution)/shard_map/ppermute | solution.py:412
  14.7 1.6 %collective-permute-start.2 = (bf16[128,1024]{1,0:T(8,128)(2,1)S(1)}, bf16[128,1024]{1,0:T(8,128)(2,1)S(1)}, u32[]{:S(2)}, u32[]{:S(2)}) collective-permute-start(bf16[128,1024]{1,0:T(8,128)(2,1)S(1)} %add.3.refs_0_), channel_id=1, source_target_pairs={{0,2},{1,3},{2,0},{3,1},{4,6},{5,7},{6,4},{7,5},{8,10},{9,11},{10,... | collective-permute-start | bytes 786440 | tf_op jit(solution)/shard_map/ppermute | solution.py:412
  16.7 0.6 %collective-permute-start.7 = (bf16[128,1024]{1,0:T(8,128)(2,1)S(1)}, bf16[128,1024]{1,0:T(8,128)(2,1)S(1)}, u32[]{:S(2)}, u32[]{:S(2)}) collective-permute-start(bf16[128,1024]{1,0:T(8,128)(2,1)S(1)} %add.4.refs_0_), channel_id=1, source_target_pairs={{0,2},{1,3},{2,0},{3,1},{4,6},{5,7},{6,4},{7,5},{8,10},{9,11},{10,... | collective-permute-start | bytes 786440 | tf_op jit(solution)/shard_map/ppermute | solution.py:412
  17.3 6.7 %collective-permute-done.2.refs_1_ = bf16[128,1024]{1,0:T(8,128)(2,1)S(1)} collective-permute-done((bf16[128,1024]{1,0:T(8,128)(2,1)S(1)}, bf16[128,1024]{1,0:T(8,128)(2,1)S(1)}, u32[]{:S(2)}, u32[]{:S(2)}) %collective-permute-start.2) | collective-permute-done | bytes 262176 | tf_op jit(solution)/shard_map/ppermute | solution.py:412
  24.2 4.6 %collective-permute-done.7.refs_1_ = bf16[128,1024]{1,0:T(8,128)(2,1)S(1)} collective-permute-done((bf16[128,1024]{1,0:T(8,128)(2,1)S(1)}, bf16[128,1024]{1,0:T(8,128)(2,1)S(1)}, u32[]{:S(2)}, u32[]{:S(2)}) %collective-permute-start.7) | collective-permute-done | bytes 262176 | tf_op jit(solution)/shard_map/ppermute | solution.py:412
  28.9 0.8 %bias_tiles.3.refs_3_.refs_1_.refs_2_ = f32[8,128,384]{2,1,0:T(8,128)S(1)} custom-call(f32[2,8,257]{2,1,0:T(8,128)S(1)} %get-tuple-element.37.table_ref), custom_call_target="tpu_custom_call" | custom-call | flops 2000000000 | bytes 1000000 | tf_op jit(solution)/shard_map/bias_tiles/pallas_call | solution.py:557
  29.8 0.6 %norm_kv_next.2 = (bf16[128,2048]{1,0:T(8,128)(2,1)S(1)}, bf16[128,256]{1,0:T(8,128)(2,1)S(1)}) custom-call(bf16[128,1024]{1,0:T(8,128)(2,1)S(1)} %residual.2.mine_ref.refs_0_, bf16[128,1024]{1,0:T(8,128)(2,1)S(1)} %collective-permute-done.3.other_ref, f32[2,2048]{1,0:T(2,128)S(1)} %copy-done.5, bf16[2,2048,128]{2,1,0:T(8,128)(2,1)S(1)} %copy-done.1, ...), custom_call_target="tpu_custom_call" | custom-call | flops 134217728 | bytes 1048576 | tf_op jit(solution)/shard_map/norm_kv_next/pallas_call | solution.py:612
  30.4 2.4 %collective-permute-start.4 = (bf16[128,256]{1,0:T(8,128)(2,1)S(1)}, bf16[128,256]{1,0:T(8,128)(2,1)S(1)}, u32[]{:S(2)}, u32[]{:S(2)}) collective-permute-start(bf16[128,256]{1,0:T(8,128)(2,1)S(1)} %get-tuple-element.47.refs_2_), channel_id=1, source_target_pairs={{0,4},{4,8},{8,12},{12,16},{16,20},{20,24},{24,28},{28,0},{1,5},{5... | collective-permute-start | bytes 196616 | tf_op jit(solution)/shard_map/ppermute | solution.py:418
  32.8 0.7 %queries.5.q_ref = bf16[8,128,128]{2,1,0:T(8,128)(2,1)S(1)} custom-call(bf16[128,2048]{1,0:T(8,128)(2,1)S(1)} %get-tuple-element.46.normed_ref, bf16[2,2048,512]{2,1,0:T(8,128)(2,1)S(1)} %copy-done.3, f32[2,64]{1,0:T(2,128)S(1)} %copy-done.7), custom_call_target="tpu_custom_call" | custom-call | flops 2000000000 | bytes 2097152 | tf_op jit(solution)/shard_map/queries/pallas_call | solution.py:438
  33.5 0.6 %norm_kv_next.3 = (bf16[128,2048]{1,0:T(8,128)(2,1)S(1)}, bf16[128,256]{1,0:T(8,128)(2,1)S(1)}) custom-call(bf16[128,1024]{1,0:T(8,128)(2,1)S(1)} %residual.3.mine_ref.refs_3_, bf16[128,1024]{1,0:T(8,128)(2,1)S(1)} %collective-permute-done.8.other_ref, f32[2,2048]{1,0:T(2,128)S(1)} %copy-done.5, bf16[2,2048,128]{2,1,0:T(8,128)(2,1)S(1)} %copy-done.1, ...), custom_call_target="tpu_custom_call" | custom-call | flops 134217728 | bytes 1048576 | tf_op jit(solution)/shard_map/norm_kv_next/pallas_call | solution.py:612
  34.2 0.7 %queries.7.q_ref = bf16[8,128,128]{2,1,0:T(8,128)(2,1)S(1)} custom-call(bf16[128,2048]{1,0:T(8,128)(2,1)S(1)} %get-tuple-element.58.normed_ref, bf16[2,2048,512]{2,1,0:T(8,128)(2,1)S(1)} %copy-done.3, f32[2,64]{1,0:T(2,128)S(1)} %copy-done.7), custom_call_target="tpu_custom_call" | custom-call | flops 2000000000 | bytes 2097152 | tf_op jit(solution)/shard_map/queries/pallas_call | solution.py:438
  34.9 1.6 %collective-permute-start.11 = (bf16[128,256]{1,0:T(8,128)(2,1)S(1)}, bf16[128,256]{1,0:T(8,128)(2,1)S(1)}, u32[]{:S(2)}, u32[]{:S(2)}) collective-permute-start(bf16[128,256]{1,0:T(8,128)(2,1)S(1)} %get-tuple-element.53.refs_1_.refs_0_), channel_id=1, source_target_pairs={{0,4},{4,8},{8,12},{12,16},{16,20},{20,24},{24,28},{28,0},{1,5},{5... | collective-permute-start | bytes 196616 | tf_op jit(solution)/shard_map/ppermute | solution.py:418
  36.5 1.2 %collective-permute-done.4.refs_0_.refs_1_ = bf16[128,256]{1,0:T(8,128)(2,1)S(1)} collective-permute-done((bf16[128,256]{1,0:T(8,128)(2,1)S(1)}, bf16[128,256]{1,0:T(8,128)(2,1)S(1)}, u32[]{:S(2)}, u32[]{:S(2)}) %collective-permute-start.4) | collective-permute-done | bytes 65568 | tf_op jit(solution)/shard_map/ppermute | solution.py:418
  37.7 1.4 %attention.1 = (bf16[128,1024]{1,0:T(8,128)(2,1)S(1)}, bf16[128,1024]{1,0:T(8,128)(2,1)S(1)}) custom-call(bf16[8,128,128]{2,1,0:T(8,128)(2,1)S(1)} %queries.5.q_ref, bf16[128,256]{1,0:T(8,128)(2,1)S(1)} %collective-permute-done.4.refs_0_.refs_1_, bf16[128,256]{1,0:T(8,128)(2,1)S(1)} %get-tuple-element.53.refs_1_.refs_0_, ...), custom_call_target="tpu_custom_call" | custom-call | flops 469762048 | bytes 2097152 | tf_op jit(solution)/shard_map/attention/pallas_call | solution.py:461
  39.1 0.6 %own_part.5 = (f32[8,128,128]{2,1,0:T(8,128)S(1)}, f32[8,128,256]{2,1,0:T(8,128)S(1)}) custom-call(bf16[8,128,128]{2,1,0:T(8,128)(2,1)S(1)} %queries.7.q_ref, bf16[128,256]{1,0:T(8,128)(2,1)S(1)} %get-tuple-element.53.refs_1_.refs_0_, f32[8,128,384]{2,1,0:T(8,128)S(1)} %bias_tiles.3.refs_3_.refs_1_.refs_2_), custom_call_target="tpu_custom_call" | custom-call | flops 500000000 | bytes 1000000 | tf_op jit(solution)/shard_map/own_part/pallas_call | solution.py:477
  39.7 2.2 %collective-permute-done.11.refs_0_ = bf16[128,256]{1,0:T(8,128)(2,1)S(1)} collective-permute-done((bf16[128,256]{1,0:T(8,128)(2,1)S(1)}, bf16[128,256]{1,0:T(8,128)(2,1)S(1)}, u32[]{:S(2)}, u32[]{:S(2)}) %collective-permute-start.11) | collective-permute-done | bytes 65568 | tf_op jit(solution)/shard_map/ppermute | solution.py:418
  42.8 0.5 %collective-permute-start.12 = (bf16[128,512]{1,0:T(8,128)(2,1)S(1)}, bf16[128,512]{1,0:T(8,128)(2,1)S(1)}, u32[]{:S(2)}, u32[]{:S(2)}) collective-permute-start(bf16[128,512]{1,0:T(8,128)(2,1)S(1)} %get-tuple-element.63), channel_id=1, source_target_pairs={{0,1},{1,0},{2,3},{3,2},{4,5},{5,4},{6,7},{7,6},{8,9},{9,8},{10,11... | collective-permute-start | bytes 393224 | tf_op jit(solution)/shard_map/ppermute | solution.py:412
  43.8 1.6 %collective-permute-start.14 = (bf16[128,512]{1,0:T(8,128)(2,1)S(1)}, bf16[128,512]{1,0:T(8,128)(2,1)S(1)}, u32[]{:S(2)}, u32[]{:S(2)}) collective-permute-start(bf16[128,512]{1,0:T(8,128)(2,1)S(1)} %add.5), channel_id=1, source_target_pairs={{0,2},{1,3},{2,0},{3,1},{4,6},{5,7},{6,4},{7,5},{8,10},{9,11},{10,... | collective-permute-start | bytes 393224 | tf_op jit(solution)/shard_map/ppermute | solution.py:412
  45.4 0.6 %collective-permute-start.10 = (bf16[128,512]{1,0:T(8,128)(2,1)S(1)}, bf16[128,512]{1,0:T(8,128)(2,1)S(1)}, u32[]{:S(2)}, u32[]{:S(2)}) collective-permute-start(bf16[128,512]{1,0:T(8,128)(2,1)S(1)} %get-tuple-element.57), channel_id=1, source_target_pairs={{0,2},{1,3},{2,0},{3,1},{4,6},{5,7},{6,4},{7,5},{8,10},{9,11},{10,... | collective-permute-start | bytes 393224 | tf_op jit(solution)/shard_map/ppermute | solution.py:412
  46.0 4.2 %collective-permute-done.14.refs_6_ = bf16[128,512]{1,0:T(8,128)(2,1)S(1)} collective-permute-done((bf16[128,512]{1,0:T(8,128)(2,1)S(1)}, bf16[128,512]{1,0:T(8,128)(2,1)S(1)}, u32[]{:S(2)}, u32[]{:S(2)}) %collective-permute-start.14) | collective-permute-done | bytes 131104 | tf_op jit(solution)/shard_map/ppermute | solution.py:412
  50.2 2.0 %collective-permute-done.10.refs_2_ = bf16[128,512]{1,0:T(8,128)(2,1)S(1)} collective-permute-done((bf16[128,512]{1,0:T(8,128)(2,1)S(1)}, bf16[128,512]{1,0:T(8,128)(2,1)S(1)}, u32[]{:S(2)}, u32[]{:S(2)}) %collective-permute-start.10) | collective-permute-done | bytes 131104 | tf_op jit(solution)/shard_map/ppermute | solution.py:412
  52.2 0.8 %result.1 = bf16[256,512]{1,0:T(8,128)(2,1)} custom-call(bf16[128,1024]{1,0:T(8,128)(2,1)S(1)} %residual.2.mine_ref.refs_0_, bf16[128,512]{1,0:T(8,128)(2,1)S(1)} %get-tuple-element.56.refs_1_, bf16[128,512]{1,0:T(8,128)(2,1)S(1)} %collective-permute-done.10.refs_2_, bf16[128,1024]{1,0:T(8,128)(2,1)S(1)} %residual.3.mine_ref.refs_3_, ...), custom_call_target="tpu_custom_call" | custom-call | tf_op jit(solution)/shard_map/result/pallas_call | solution.py:665
  (42 shorter events, 3.8 us)
Async XLA Ops:
  0.0 5.4 %copy-start.4 = (bf16[256,2048]{1,0:T(8,128)(2,1)S(1)}, bf16[256,2048]{1,0:T(8,128)(2,1)}, u32[]{:S(2)}) copy-start(bf16[256,2048]{1,0:T(8,128)(2,1)} %x_ref.5) | copy-start | bytes 3145732
  0.0 7.6 %copy-start.3 = (bf16[2,2048,512]{2,1,0:T(8,128)(2,1)S(1)}, bf16[2,2048,512]{2,1,0:T(8,128)(2,1)}, u32[]{:S(2)}) copy-start(bf16[2,2048,512]{2,1,0:T(8,128)(2,1)} %wq_ref.7) | copy-start | bytes 12582916
  2.3 10.2 %collective-permute-start = (bf16[128,256]{1,0:T(8,128)(2,1)S(1)}, bf16[128,256]{1,0:T(8,128)(2,1)S(1)}, u32[]{:S(2)}, u32[]{:S(2)}) collective-permute-start(bf16[128,256]{1,0:T(8,128)(2,1)S(1)} %get-tuple-element.36.refs_1_), channel_id=1, source_target_pairs={{0,4},{4,8},{8,12},{12,16},{16,20},{20,24},{24,28},{28,0},{1,5},{5... | collective-permute-start | bytes 196616 | tf_op jit(solution)/shard_map/ppermute | solution.py:418
  6.0 2.4 %copy-start.7 = (f32[2,64]{1,0:T(2,128)S(1)}, f32[2,64]{1,0:T(2,128)}, u32[]{:S(2)}) copy-start(f32[2,64]{1,0:T(2,128)} %qg_ref.7) | copy-start | bytes 1540
  6.0 7.1 %collective-permute-start.5 = (bf16[128,256]{1,0:T(8,128)(2,1)S(1)}, bf16[128,256]{1,0:T(8,128)(2,1)S(1)}, u32[]{:S(2)}, u32[]{:S(2)}) collective-permute-start(bf16[128,256]{1,0:T(8,128)(2,1)S(1)} %get-tuple-element.41.refs_0_), channel_id=1, source_target_pairs={{0,4},{4,8},{8,12},{12,16},{16,20},{20,24},{24,28},{28,0},{1,5},{5... | collective-permute-start | bytes 196616 | tf_op jit(solution)/shard_map/ppermute | solution.py:418
  8.4 2.2 %copy-start = (bf16[2,512,2048]{2,1,0:T(8,128)(2,1)S(1)}, bf16[2,512,2048]{2,1,0:T(8,128)(2,1)}, u32[]{:S(2)}) copy-start(bf16[2,512,2048]{2,1,0:T(8,128)(2,1)} %wout_ref.7) | copy-start | bytes 12582916
  13.0 1.6 %collective-permute-start.1 = (bf16[128,1024]{1,0:T(8,128)(2,1)S(1)}, bf16[128,1024]{1,0:T(8,128)(2,1)S(1)}, u32[]{:S(2)}, u32[]{:S(2)}) collective-permute-start(bf16[128,1024]{1,0:T(8,128)(2,1)S(1)} %get-tuple-element.45), channel_id=1, source_target_pairs={{0,1},{1,0},{2,3},{3,2},{4,5},{5,4},{6,7},{7,6},{8,9},{9,8},{10,11... | collective-permute-start | bytes 786440 | tf_op jit(solution)/shard_map/ppermute | solution.py:412
  13.6 3.0 %collective-permute-start.6 = (bf16[128,1024]{1,0:T(8,128)(2,1)S(1)}, bf16[128,1024]{1,0:T(8,128)(2,1)S(1)}, u32[]{:S(2)}, u32[]{:S(2)}) collective-permute-start(bf16[128,1024]{1,0:T(8,128)(2,1)S(1)} %get-tuple-element.52), channel_id=1, source_target_pairs={{0,1},{1,0},{2,3},{3,2},{4,5},{5,4},{6,7},{7,6},{8,9},{9,8},{10,11... | collective-permute-start | bytes 786440 | tf_op jit(solution)/shard_map/ppermute | solution.py:412
  14.7 9.2 %collective-permute-start.2 = (bf16[128,1024]{1,0:T(8,128)(2,1)S(1)}, bf16[128,1024]{1,0:T(8,128)(2,1)S(1)}, u32[]{:S(2)}, u32[]{:S(2)}) collective-permute-start(bf16[128,1024]{1,0:T(8,128)(2,1)S(1)} %add.3.refs_0_), channel_id=1, source_target_pairs={{0,2},{1,3},{2,0},{3,1},{4,6},{5,7},{6,4},{7,5},{8,10},{9,11},{10,... | collective-permute-start | bytes 786440 | tf_op jit(solution)/shard_map/ppermute | solution.py:412
  16.7 12.1 %collective-permute-start.7 = (bf16[128,1024]{1,0:T(8,128)(2,1)S(1)}, bf16[128,1024]{1,0:T(8,128)(2,1)S(1)}, u32[]{:S(2)}, u32[]{:S(2)}) collective-permute-start(bf16[128,1024]{1,0:T(8,128)(2,1)S(1)} %add.4.refs_0_), channel_id=1, source_target_pairs={{0,2},{1,3},{2,0},{3,1},{4,6},{5,7},{6,4},{7,5},{8,10},{9,11},{10,... | collective-permute-start | bytes 786440 | tf_op jit(solution)/shard_map/ppermute | solution.py:412
  24.1 5.7 %copy-start.1 = (bf16[2,2048,128]{2,1,0:T(8,128)(2,1)S(1)}, bf16[2,2048,128]{2,1,0:T(8,128)(2,1)}, u32[]{:S(2)}) copy-start(bf16[2,2048,128]{2,1,0:T(8,128)(2,1)} %wk_ref.3) | copy-start | bytes 3145732
  24.1 5.7 %copy-start.2 = (bf16[2,2048,128]{2,1,0:T(8,128)(2,1)S(1)}, bf16[2,2048,128]{2,1,0:T(8,128)(2,1)}, u32[]{:S(2)}) copy-start(bf16[2,2048,128]{2,1,0:T(8,128)(2,1)} %wv_ref.3) | copy-start | bytes 3145732
  24.1 5.7 %copy-start.5 = (f32[2,2048]{1,0:T(2,128)S(1)}, f32[2,2048]{1,0:T(2,128)}, u32[]{:S(2)}) copy-start(f32[2,2048]{1,0:T(2,128)} %gain_ref.3) | copy-start | bytes 49156
  24.1 5.7 %copy-start.6 = (f32[2,64]{1,0:T(2,128)S(1)}, f32[2,64]{1,0:T(2,128)}, u32[]{:S(2)}) copy-start(f32[2,64]{1,0:T(2,128)} %kg_ref.3) | copy-start | bytes 1540
  24.1 5.6 %collective-permute-start.3 = (bf16[128,1024]{1,0:T(8,128)(2,1)S(1)}, bf16[128,1024]{1,0:T(8,128)(2,1)S(1)}, u32[]{:S(2)}, u32[]{:S(2)}) collective-permute-start(bf16[128,1024]{1,0:T(8,128)(2,1)S(1)} %residual.2.mine_ref.refs_0_), channel_id=1, source_target_pairs={{0,1},{1,0},{2,3},{3,2},{4,5},{5,4},{6,7},{7,6},{8,9},{9,8},{10,11... | collective-permute-start | bytes 786440 | tf_op jit(solution)/shard_map/ppermute | solution.py:412
  28.8 4.7 %collective-permute-start.8 = (bf16[128,1024]{1,0:T(8,128)(2,1)S(1)}, bf16[128,1024]{1,0:T(8,128)(2,1)S(1)}, u32[]{:S(2)}, u32[]{:S(2)}) collective-permute-start(bf16[128,1024]{1,0:T(8,128)(2,1)S(1)} %residual.3.mine_ref.refs_3_), channel_id=1, source_target_pairs={{0,1},{1,0},{2,3},{3,2},{4,5},{5,4},{6,7},{7,6},{8,9},{9,8},{10,11... | collective-permute-start | bytes 786440 | tf_op jit(solution)/shard_map/ppermute | solution.py:412
  30.4 7.2 %collective-permute-start.4 = (bf16[128,256]{1,0:T(8,128)(2,1)S(1)}, bf16[128,256]{1,0:T(8,128)(2,1)S(1)}, u32[]{:S(2)}, u32[]{:S(2)}) collective-permute-start(bf16[128,256]{1,0:T(8,128)(2,1)S(1)} %get-tuple-element.47.refs_2_), channel_id=1, source_target_pairs={{0,4},{4,8},{8,12},{12,16},{16,20},{20,24},{24,28},{28,0},{1,5},{5... | collective-permute-start | bytes 196616 | tf_op jit(solution)/shard_map/ppermute | solution.py:418
  34.9 7.0 %collective-permute-start.11 = (bf16[128,256]{1,0:T(8,128)(2,1)S(1)}, bf16[128,256]{1,0:T(8,128)(2,1)S(1)}, u32[]{:S(2)}, u32[]{:S(2)}) collective-permute-start(bf16[128,256]{1,0:T(8,128)(2,1)S(1)} %get-tuple-element.53.refs_1_.refs_0_), channel_id=1, source_target_pairs={{0,4},{4,8},{8,12},{12,16},{16,20},{20,24},{24,28},{28,0},{1,5},{5... | collective-permute-start | bytes 196616 | tf_op jit(solution)/shard_map/ppermute | solution.py:418
  39.1 6.3 %collective-permute-start.9 = (bf16[128,1024]{1,0:T(8,128)(2,1)S(1)}, bf16[128,1024]{1,0:T(8,128)(2,1)S(1)}, u32[]{:S(2)}, u32[]{:S(2)}) collective-permute-start(bf16[128,1024]{1,0:T(8,128)(2,1)S(1)} %get-tuple-element.55), channel_id=1, source_target_pairs={{0,1},{1,0},{2,3},{3,2},{4,5},{5,4},{6,7},{7,6},{8,9},{9,8},{10,11... | collective-permute-start | bytes 786440 | tf_op jit(solution)/shard_map/ppermute | solution.py:412
  42.3 1.4 %collective-permute-start.13 = (bf16[128,512]{1,0:T(8,128)(2,1)S(1)}, bf16[128,512]{1,0:T(8,128)(2,1)S(1)}, u32[]{:S(2)}, u32[]{:S(2)}) collective-permute-start(bf16[128,512]{1,0:T(8,128)(2,1)S(1)} %get-tuple-element.64), channel_id=1, source_target_pairs={{0,1},{1,0},{2,3},{3,2},{4,5},{5,4},{6,7},{7,6},{8,9},{9,8},{10,11... | collective-permute-start | bytes 393224 | tf_op jit(solution)/shard_map/ppermute | solution.py:412
  42.8 3.3 %collective-permute-start.12 = (bf16[128,512]{1,0:T(8,128)(2,1)S(1)}, bf16[128,512]{1,0:T(8,128)(2,1)S(1)}, u32[]{:S(2)}, u32[]{:S(2)}) collective-permute-start(bf16[128,512]{1,0:T(8,128)(2,1)S(1)} %get-tuple-element.63), channel_id=1, source_target_pairs={{0,1},{1,0},{2,3},{3,2},{4,5},{5,4},{6,7},{7,6},{8,9},{9,8},{10,11... | collective-permute-start | bytes 393224 | tf_op jit(solution)/shard_map/ppermute | solution.py:412
  43.8 6.4 %collective-permute-start.14 = (bf16[128,512]{1,0:T(8,128)(2,1)S(1)}, bf16[128,512]{1,0:T(8,128)(2,1)S(1)}, u32[]{:S(2)}, u32[]{:S(2)}) collective-permute-start(bf16[128,512]{1,0:T(8,128)(2,1)S(1)} %add.5), channel_id=1, source_target_pairs={{0,2},{1,3},{2,0},{3,1},{4,6},{5,7},{6,4},{7,5},{8,10},{9,11},{10,... | collective-permute-start | bytes 393224 | tf_op jit(solution)/shard_map/ppermute | solution.py:412
  45.4 6.8 %collective-permute-start.10 = (bf16[128,512]{1,0:T(8,128)(2,1)S(1)}, bf16[128,512]{1,0:T(8,128)(2,1)S(1)}, u32[]{:S(2)}, u32[]{:S(2)}) collective-permute-start(bf16[128,512]{1,0:T(8,128)(2,1)S(1)} %get-tuple-element.57), channel_id=1, source_target_pairs={{0,2},{1,3},{2,0},{3,1},{4,6},{5,7},{6,4},{7,5},{8,10},{9,11},{10,... | collective-permute-start | bytes 393224 | tf_op jit(solution)/shard_map/ppermute | solution.py:412

commit v7 on v6

--- a/solution.py
+++ b/solution.py
@@ -310,7 +310,7 @@
     summed_ref[...] = summed.reshape(summed_ref.shape)
 
 
-def joined_kernel(block, layer_index, q_start, starts, q_ref, *refs):
+def joined_kernel(block, layer_index, q_start, starts, prior, q_ref, *refs):
     piece_refs = refs[: len(starts)]
     tile_ref, peak_ref, summed_ref, wout_ref, *out_refs, mixed_ref = refs[len(starts) :]
     heads = q_ref.shape[0]
@@ -325,13 +325,7 @@
         into = head * HEAD_DIM
         mixed_ref[:, into : into + HEAD_DIM] = ratio[:, at : at + HEAD_DIM].astype(bf16)
 
-    @pl.when(lax.axis_index("sp") == 0)
-    def _():
-        for head in range(heads):
-            put(head, summed_ref[head])
-
-    @pl.when(lax.axis_index("sp") > 0)
-    def _():
+    def join():
         pieces = [
             ref[start : start + CHUNK, :] for ref, start in zip(piece_refs, starts, strict=True)
         ]
@@ -343,6 +337,10 @@
             preferred_element_type=f32,
         ).reshape(heads, CHUNK, upper)
         scores = scores + tile_ref[:, :, :upper]
+        if prior < len(starts):
+            lane = lax.broadcasted_iota(jnp.int32, (1, 1, upper), 2)
+            outside = (lane < prior * CHUNK) & (lax.axis_index("sp") == 0)
+            scores = scores + jnp.where(outside, masked_score, 0.0)
         before = peak_ref[...]
         peaks = jnp.max(scores, axis=-1, keepdims=True)
         peaks = jnp.maximum(before, jnp.broadcast_to(peaks, before.shape))
@@ -355,6 +353,16 @@
         for head in range(heads):
             wide = jnp.concatenate([scale[head]] * (summed.shape[2] // LANES), axis=1)
             put(head, summed_ref[head] * wide + summed[head])
+
+    if prior < len(starts):
+        join()
+    else:
+        pl.when(lax.axis_index("sp") > 0)(join)
+
+        @pl.when(lax.axis_index("sp") == 0)
+        def _():
+            for head in range(heads):
+                put(head, summed_ref[head])
 
     out_projection(block, layer_index, mixed_ref, wout_ref, *out_refs)
 
@@ -472,8 +480,8 @@
             name="attention",
         )(query, *pieces, tiles[layer_index], w_out)
 
-    def own_part(layer_index, part, query, q_start, pieces, starts):
-        prior = max(0, PIECES - 1 - part)
+    def own_part(layer_index, part, query, q_start, pieces, starts, late=None):
+        prior = max(0, PIECES - 1 - part) if late is None else late
         return pl.pallas_call(
             functools.partial(own_kernel, q_start, starts[prior:]),
             out_shape=[
@@ -486,16 +494,19 @@
             name="own_part",
         )(query, *pieces[prior:], tiles[layer_index])
 
-    def joined(layer_index, part, query, q_start, pieces, starts, own, early=0):
+    def joined(layer_index, part, query, q_start, pieces, starts, own, early=0, late=None):
         prior = max(0, PIECES - 1 - part)
+        late = prior if late is None else late
         return pl.pallas_call(
-            functools.partial(joined_kernel, block, layer_index, q_start, starts[:prior]),
+            functools.partial(
+                joined_kernel, block, layer_index, q_start, starts[:late], prior
+            ),
             **attention_out(early, CHUNK),
-            in_specs=[whole] * (prior + 5),
+            in_specs=[whole] * (late + 5),
             compiler_params=params(),
             cost_estimate=cost(1e9, 2 * width * query_width),
             name="joined",
-        )(query, *pieces[:prior], tiles[layer_index], *own, w_out)
+        )(query, *pieces[:late], tiles[layer_index], *own, w_out)
 
     def project(layer_index, mixed, which):
         return pl.pallas_call(
@@ -557,12 +568,12 @@
             pl.pallas_call(
                 functools.partial(bias_kernel, layer_index),
                 out_shape=out((heads, CHUNK, WINDOW), f32),
-                in_specs=[whole] * (2 - layer_index),
+                in_specs=[whole],
                 out_specs=whole,
                 compiler_params=params(),
                 cost_estimate=cost(2e9, 1e6),
                 name="bias_tiles",
-            )(table, *[w_query] * (1 - layer_index))
+            )(table)
         )
 
     mine, other, kvs, normeds = {}, {}, {}, {}
@@ -632,6 +643,12 @@
         if part == 0:
             own = own_part(1, part, query, 0, pieces, [0] * PIECES)
             keep, send = joined(1, part, query, 0, pieces, [0] * PIECES, own, early)
+        elif part == order[0]:
+            late = PIECES - 1
+            own = own_part(1, part, query, 0, pieces, [0] * PIECES, late)
+            keep, send = joined(
+                1, part, query, 0, pieces, [0] * PIECES, own, early, late
+            )
         else:
             keep, send = attention(
                 1, part, 0, CHUNK, query, 0, pieces, [0] * PIECES, early

time: 53.1 us -> 53.2 us (level)
    pallas_call x1 -> x0, Pallas kernels: 1.38 us -> none  [attention(): pl.pallas_call(functools.partial(attention_kernel, block, layer_index, q_...]
    pallas_call x3 -> x4, Pallas kernels: 1.35 us -> 2.46 us  [joined(): pl.pallas_call(functools.partial(joined_kernel, block, layer_index, q_sta...]
    pallas_call x3 -> x4, Pallas kernels: 1.82 us -> 2.42 us  [own_part(): pl.pallas_call(functools.partial(own_kernel, q_start, starts[prior:]), ou...]
where the time goes in v7:
time: 53.2 us; the launch traced here: 53 us
  waiting for transfers between devices  20.9 us (39%)
  Pallas kernels  16 us (30%)
  starting transfers between devices  14.3 us (27%)
  local copies, waits for them, and re-layouts  1.48 us (3%)
    ppermute x11, waiting for transfers between devices, swapped(): return lax.ppermute(value, 'tp', [(d, d ^ 1 << bit) for d in range(size)])  17.8 us
    ppermute x4, starting transfers between devices, passed_along(): return lax.ppermute(value, 'sp', edges)  8.57 us
    ppermute x11, starting transfers between devices, swapped(): return lax.ppermute(value, 'tp', [(d, d ^ 1 << bit) for d in range(size)])  5.76 us
    ppermute x4, waiting for transfers between devices, passed_along(): return lax.ppermute(value, 'sp', edges)  3.06 us
    pallas_call x4, Pallas kernels, queries(): pl.pallas_call(functools.partial(query_kernel, layer_index), out_shape=ou...  2.93 us
    pallas_call x4, Pallas kernels, joined(): pl.pallas_call(functools.partial(joined_kernel, block, layer_index, q_sta...  2.46 us
    pallas_call x4, Pallas kernels, own_part(): pl.pallas_call(functools.partial(own_kernel, q_start, starts[prior:]), ou...  2.42 us
    pallas_call x1, Pallas kernels, layers(): pl.pallas_call(first_norm_kernel, out_shape=[out((CHUNK, width)), out((CH...  2.26 us
  transfers between devices with their start and end apart: 15, of which 8 were waited for; matrix products, arithmetic and copies ran while one was open for 0% of the time, Pallas kernels for 24%

profile of v7, /device:TPU:0, one launch (start us, length us, event | category | flops | bytes accessed | tf_op | source)
XLA Modules:
  0.0 53.0 jit_solution(769238273890627050)
XLA Ops:
  0.0 2.3 %norm_kv_first.1 = (bf16[128,2048]{1,0:T(8,128)(2,1)S(1)}, bf16[128,256]{1,0:T(8,128)(2,1)S(1)}, f32[2,2048]{1,0:T(2,128)S(1)}, bf16[2,2048,128]{2,1,0:T(8,128)(...) custom-call(bf16[256,2048]{1,0:T(8,128)(2,1)} %x_ref.5, f32[2,2048]{1,0:T(2,128)} %gain_ref.3, ...), custom_call_target="tpu_custom_call" | custom-call | flops 3000000000 | bytes 2097152 | tf_op jit(solution)/shard_map/norm_kv_first/pallas_call | solution.py:533
  2.3 3.0 %collective-permute-start = (bf16[128,256]{1,0:T(8,128)(2,1)S(1)}, bf16[128,256]{1,0:T(8,128)(2,1)S(1)}, u32[]{:S(2)}, u32[]{:S(2)}) collective-permute-start(bf16[128,256]{1,0:T(8,128)(2,1)S(1)} %get-tuple-element.38.refs_1_), channel_id=1, source_target_pairs={{0,4},{4,8},{8,12},{12,16},{16,20},{20,24},{24,28},{28,0},{1,5},{5... | collective-permute-start | bytes 196616 | tf_op jit(solution)/shard_map/ppermute | solution.py:426
  5.3 0.6 %norm_kv_rest.1 = (bf16[128,2048]{1,0:T(8,128)(2,1)S(1)}, bf16[128,256]{1,0:T(8,128)(2,1)S(1)}) custom-call(bf16[256,2048]{1,0:T(8,128)(2,1)S(1)} %copy-done.4, f32[2,2048]{1,0:T(2,128)S(1)} %get-tuple-element.40.gain_ref, bf16[2,2048,128]{2,1,0:T(8,128)(2,1)S(1)} %get-tuple-element.41.weight_ref, f32[2,64]{1,0:T(2,128)S(1)} %get-tuple-element.42.kg_ref), custom_call_target="tpu_custom_call" | custom-call | flops 1000000000 | bytes 2097152 | tf_op jit(solution)/shard_map/norm_kv_rest/pallas_call | solution.py:551
  6.0 1.6 %collective-permute-start.5 = (bf16[128,256]{1,0:T(8,128)(2,1)S(1)}, bf16[128,256]{1,0:T(8,128)(2,1)S(1)}, u32[]{:S(2)}, u32[]{:S(2)}) collective-permute-start(bf16[128,256]{1,0:T(8,128)(2,1)S(1)} %get-tuple-element.43.refs_0_), channel_id=1, source_target_pairs={{0,4},{4,8},{8,12},{12,16},{16,20},{20,24},{24,28},{28,0},{1,5},{5... | collective-permute-start | bytes 196616 | tf_op jit(solution)/shard_map/ppermute | solution.py:426
  7.6 0.8 %bias_tiles.2.refs_2_.refs_1_ = f32[8,128,384]{2,1,0:T(8,128)S(1)} custom-call(f32[2,8,257]{2,1,0:T(8,128)S(1)} %get-tuple-element.39.table_ref), custom_call_target="tpu_custom_call" | custom-call | flops 2000000000 | bytes 1000000 | tf_op jit(solution)/shard_map/bias_tiles/pallas_call | solution.py:568
  8.4 0.7 %queries.6.q_ref = bf16[8,128,128]{2,1,0:T(8,128)(2,1)S(1)} custom-call(bf16[128,2048]{1,0:T(8,128)(2,1)S(1)} %get-tuple-element.50.normed_ref, bf16[2,2048,512]{2,1,0:T(8,128)(2,1)S(1)} %copy-done.3, f32[2,64]{1,0:T(2,128)S(1)} %copy-done.7), custom_call_target="tpu_custom_call" | custom-call | flops 2000000000 | bytes 2097152 | tf_op jit(solution)/shard_map/queries/pallas_call | solution.py:446
  9.1 1.4 %copy-done = bf16[2,512,2048]{2,1,0:T(8,128)(2,1)S(1)} copy-done((bf16[2,512,2048]{2,1,0:T(8,128)(2,1)S(1)}, bf16[2,512,2048]{2,1,0:T(8,128)(2,1)}, u32[]{:S(2)}) %copy-start) | copy-done | bytes 4194328
  10.5 0.7 %queries.4.q_ref = bf16[8,128,128]{2,1,0:T(8,128)(2,1)S(1)} custom-call(bf16[128,2048]{1,0:T(8,128)(2,1)S(1)} %get-tuple-element.37.normed_ref, bf16[2,2048,512]{2,1,0:T(8,128)(2,1)S(1)} %copy-done.3, f32[2,64]{1,0:T(2,128)S(1)} %copy-done.7, bf16[2,512,2048]{2,1,0:T(8,128)(2,1)S(1)} %copy-done), custom_call_target="tpu_custom_call" | custom-call | flops 2000000000 | bytes 2097152 | tf_op jit(solution)/shard_map/queries/pallas_call | solution.py:446
  11.3 0.6 %own_part.4 = (f32[8,128,128]{2,1,0:T(8,128)S(1)}, f32[8,128,256]{2,1,0:T(8,128)S(1)}) custom-call(bf16[8,128,128]{2,1,0:T(8,128)(2,1)S(1)} %queries.4.q_ref, bf16[128,256]{1,0:T(8,128)(2,1)S(1)} %get-tuple-element.43.refs_0_, bf16[128,256]{1,0:T(8,128)(2,1)S(1)} %get-tuple-element.38.refs_1_, f32[8,128,384]{2,1,0:T(8,128)S(1)} %bias_tiles.2.refs_2_.refs_1_), custom_call_target="tpu_custom_call" | custom-call | flops 500000000 | bytes 1000000 | tf_op jit(solution)/shard_map/own_part/pallas_call | solution.py:485
  11.9 0.6 %own_part.5 = (f32[8,128,128]{2,1,0:T(8,128)S(1)}, f32[8,128,256]{2,1,0:T(8,128)S(1)}) custom-call(bf16[8,128,128]{2,1,0:T(8,128)(2,1)S(1)} %queries.6.q_ref, bf16[128,256]{1,0:T(8,128)(2,1)S(1)} %get-tuple-element.43.refs_0_, f32[8,128,384]{2,1,0:T(8,128)S(1)} %bias_tiles.2.refs_2_.refs_1_), custom_call_target="tpu_custom_call" | custom-call | flops 500000000 | bytes 1000000 | tf_op jit(solution)/shard_map/own_part/pallas_call | solution.py:485
  13.6 0.5 %collective-permute-start.6 = (bf16[128,1024]{1,0:T(8,128)(2,1)S(1)}, bf16[128,1024]{1,0:T(8,128)(2,1)S(1)}, u32[]{:S(2)}, u32[]{:S(2)}) collective-permute-start(bf16[128,1024]{1,0:T(8,128)(2,1)S(1)} %get-tuple-element.54), channel_id=1, source_target_pairs={{0,1},{1,0},{2,3},{3,2},{4,5},{5,4},{6,7},{7,6},{8,9},{9,8},{10,11... | collective-permute-start | bytes 786440 | tf_op jit(solution)/shard_map/ppermute | solution.py:420
  14.7 1.6 %collective-permute-start.2 = (bf16[128,1024]{1,0:T(8,128)(2,1)S(1)}, bf16[128,1024]{1,0:T(8,128)(2,1)S(1)}, u32[]{:S(2)}, u32[]{:S(2)}) collective-permute-start(bf16[128,1024]{1,0:T(8,128)(2,1)S(1)} %add.3.refs_0_), channel_id=1, source_target_pairs={{0,2},{1,3},{2,0},{3,1},{4,6},{5,7},{6,4},{7,5},{8,10},{9,11},{10,... | collective-permute-start | bytes 786440 | tf_op jit(solution)/shard_map/ppermute | solution.py:420
  16.6 0.6 %collective-permute-start.7 = (bf16[128,1024]{1,0:T(8,128)(2,1)S(1)}, bf16[128,1024]{1,0:T(8,128)(2,1)S(1)}, u32[]{:S(2)}, u32[]{:S(2)}) collective-permute-start(bf16[128,1024]{1,0:T(8,128)(2,1)S(1)} %add.4.refs_0_), channel_id=1, source_target_pairs={{0,2},{1,3},{2,0},{3,1},{4,6},{5,7},{6,4},{7,5},{8,10},{9,11},{10,... | collective-permute-start | bytes 786440 | tf_op jit(solution)/shard_map/ppermute | solution.py:420
  17.2 6.7 %collective-permute-done.2.refs_1_ = bf16[128,1024]{1,0:T(8,128)(2,1)S(1)} collective-permute-done((bf16[128,1024]{1,0:T(8,128)(2,1)S(1)}, bf16[128,1024]{1,0:T(8,128)(2,1)S(1)}, u32[]{:S(2)}, u32[]{:S(2)}) %collective-permute-start.2) | collective-permute-done | bytes 262176 | tf_op jit(solution)/shard_map/ppermute | solution.py:420
  24.1 4.6 %collective-permute-done.7.refs_1_ = bf16[128,1024]{1,0:T(8,128)(2,1)S(1)} collective-permute-done((bf16[128,1024]{1,0:T(8,128)(2,1)S(1)}, bf16[128,1024]{1,0:T(8,128)(2,1)S(1)}, u32[]{:S(2)}, u32[]{:S(2)}) %collective-permute-start.7) | collective-permute-done | bytes 262176 | tf_op jit(solution)/shard_map/ppermute | solution.py:420
  28.9 0.8 %bias_tiles.3.refs_1_.refs_2_ = f32[8,128,384]{2,1,0:T(8,128)S(1)} custom-call(f32[2,8,257]{2,1,0:T(8,128)S(1)} %get-tuple-element.39.table_ref), custom_call_target="tpu_custom_call" | custom-call | flops 2000000000 | bytes 1000000 | tf_op jit(solution)/shard_map/bias_tiles/pallas_call | solution.py:568
  29.7 0.6 %norm_kv_next.2 = (bf16[128,2048]{1,0:T(8,128)(2,1)S(1)}, bf16[128,256]{1,0:T(8,128)(2,1)S(1)}) custom-call(bf16[128,1024]{1,0:T(8,128)(2,1)S(1)} %residual.2.mine_ref.refs_0_, bf16[128,1024]{1,0:T(8,128)(2,1)S(1)} %collective-permute-done.3.other_ref, f32[2,2048]{1,0:T(2,128)S(1)} %copy-done.5, bf16[2,2048,128]{2,1,0:T(8,128)(2,1)S(1)} %copy-done.1, ...), custom_call_target="tpu_custom_call" | custom-call | flops 134217728 | bytes 1048576 | tf_op jit(solution)/shard_map/norm_kv_next/pallas_call | solution.py:623
  30.4 2.4 %collective-permute-start.4 = (bf16[128,256]{1,0:T(8,128)(2,1)S(1)}, bf16[128,256]{1,0:T(8,128)(2,1)S(1)}, u32[]{:S(2)}, u32[]{:S(2)}) collective-permute-start(bf16[128,256]{1,0:T(8,128)(2,1)S(1)} %get-tuple-element.49.refs_0_), channel_id=1, source_target_pairs={{0,4},{4,8},{8,12},{12,16},{16,20},{20,24},{24,28},{28,0},{1,5},{5... | collective-permute-start | bytes 196616 | tf_op jit(solution)/shard_map/ppermute | solution.py:426
  32.8 0.8 %queries.5.q_ref = bf16[8,128,128]{2,1,0:T(8,128)(2,1)S(1)} custom-call(bf16[128,2048]{1,0:T(8,128)(2,1)S(1)} %get-tuple-element.48.normed_ref, bf16[2,2048,512]{2,1,0:T(8,128)(2,1)S(1)} %copy-done.3, f32[2,64]{1,0:T(2,128)S(1)} %copy-done.7), custom_call_target="tpu_custom_call" | custom-call | flops 2000000000 | bytes 2097152 | tf_op jit(solution)/shard_map/queries/pallas_call | solution.py:446
  33.5 0.6 %norm_kv_next.3 = (bf16[128,2048]{1,0:T(8,128)(2,1)S(1)}, bf16[128,256]{1,0:T(8,128)(2,1)S(1)}) custom-call(bf16[128,1024]{1,0:T(8,128)(2,1)S(1)} %residual.3.mine_ref.refs_3_, bf16[128,1024]{1,0:T(8,128)(2,1)S(1)} %collective-permute-done.8.other_ref, f32[2,2048]{1,0:T(2,128)S(1)} %copy-done.5, bf16[2,2048,128]{2,1,0:T(8,128)(2,1)S(1)} %copy-done.1, ...), custom_call_target="tpu_custom_call" | custom-call | flops 134217728 | bytes 1048576 | tf_op jit(solution)/shard_map/norm_kv_next/pallas_call | solution.py:623
  34.2 0.7 %queries.7.q_ref = bf16[8,128,128]{2,1,0:T(8,128)(2,1)S(1)} custom-call(bf16[128,2048]{1,0:T(8,128)(2,1)S(1)} %get-tuple-element.62.normed_ref, bf16[2,2048,512]{2,1,0:T(8,128)(2,1)S(1)} %copy-done.3, f32[2,64]{1,0:T(2,128)S(1)} %copy-done.7), custom_call_target="tpu_custom_call" | custom-call | flops 2000000000 | bytes 2097152 | tf_op jit(solution)/shard_map/queries/pallas_call | solution.py:446
  34.9 1.6 %collective-permute-start.11 = (bf16[128,256]{1,0:T(8,128)(2,1)S(1)}, bf16[128,256]{1,0:T(8,128)(2,1)S(1)}, u32[]{:S(2)}, u32[]{:S(2)}) collective-permute-start(bf16[128,256]{1,0:T(8,128)(2,1)S(1)} %get-tuple-element.55.refs_1_.refs_0_), channel_id=1, source_target_pairs={{0,4},{4,8},{8,12},{12,16},{16,20},{20,24},{24,28},{28,0},{1,5},{5... | collective-permute-start | bytes 196616 | tf_op jit(solution)/shard_map/ppermute | solution.py:426
  36.5 0.6 %own_part.6 = (f32[8,128,128]{2,1,0:T(8,128)S(1)}, f32[8,128,256]{2,1,0:T(8,128)S(1)}) custom-call(bf16[8,128,128]{2,1,0:T(8,128)(2,1)S(1)} %queries.5.q_ref, bf16[128,256]{1,0:T(8,128)(2,1)S(1)} %get-tuple-element.49.refs_0_, f32[8,128,384]{2,1,0:T(8,128)S(1)} %bias_tiles.3.refs_1_.refs_2_), custom_call_target="tpu_custom_call" | custom-call | flops 500000000 | bytes 1000000 | tf_op jit(solution)/shard_map/own_part/pallas_call | solution.py:485
  37.6 1.1 %joined.6 = (bf16[128,1024]{1,0:T(8,128)(2,1)S(1)}, bf16[128,1024]{1,0:T(8,128)(2,1)S(1)}) custom-call(bf16[8,128,128]{2,1,0:T(8,128)(2,1)S(1)} %queries.5.q_ref, bf16[128,256]{1,0:T(8,128)(2,1)S(1)} %collective-permute-done.4.refs_0_.refs_1_, bf16[128,256]{1,0:T(8,128)(2,1)S(1)} %get-tuple-element.55.refs_1_.refs_0_, ...), custom_call_target="tpu_custom_call" | custom-call | flops 1000000000 | bytes 2097152 | tf_op jit(solution)/shard_map/joined/pallas_call | solution.py:500
  38.8 0.6 %own_part.7 = (f32[8,128,128]{2,1,0:T(8,128)S(1)}, f32[8,128,256]{2,1,0:T(8,128)S(1)}) custom-call(bf16[8,128,128]{2,1,0:T(8,128)(2,1)S(1)} %queries.7.q_ref, bf16[128,256]{1,0:T(8,128)(2,1)S(1)} %get-tuple-element.55.refs_1_.refs_0_, f32[8,128,384]{2,1,0:T(8,128)S(1)} %bias_tiles.3.refs_1_.refs_2_), custom_call_target="tpu_custom_call" | custom-call | flops 500000000 | bytes 1000000 | tf_op jit(solution)/shard_map/own_part/pallas_call | solution.py:485
  39.4 2.5 %collective-permute-done.11.refs_0_ = bf16[128,256]{1,0:T(8,128)(2,1)S(1)} collective-permute-done((bf16[128,256]{1,0:T(8,128)(2,1)S(1)}, bf16[128,256]{1,0:T(8,128)(2,1)S(1)}, u32[]{:S(2)}, u32[]{:S(2)}) %collective-permute-start.11) | collective-permute-done | bytes 65568 | tf_op jit(solution)/shard_map/ppermute | solution.py:426
  42.8 0.5 %collective-permute-start.12 = (bf16[128,512]{1,0:T(8,128)(2,1)S(1)}, bf16[128,512]{1,0:T(8,128)(2,1)S(1)}, u32[]{:S(2)}, u32[]{:S(2)}) collective-permute-start(bf16[128,512]{1,0:T(8,128)(2,1)S(1)} %get-tuple-element.67), channel_id=1, source_target_pairs={{0,1},{1,0},{2,3},{3,2},{4,5},{5,4},{6,7},{7,6},{8,9},{9,8},{10,11... | collective-permute-start | bytes 393224 | tf_op jit(solution)/shard_map/ppermute | solution.py:420
  43.8 1.6 %collective-permute-start.14 = (bf16[128,512]{1,0:T(8,128)(2,1)S(1)}, bf16[128,512]{1,0:T(8,128)(2,1)S(1)}, u32[]{:S(2)}, u32[]{:S(2)}) collective-permute-start(bf16[128,512]{1,0:T(8,128)(2,1)S(1)} %add.5), channel_id=1, source_target_pairs={{0,2},{1,3},{2,0},{3,1},{4,6},{5,7},{6,4},{7,5},{8,10},{9,11},{10,... | collective-permute-start | bytes 393224 | tf_op jit(solution)/shard_map/ppermute | solution.py:420
  45.4 0.6 %collective-permute-start.10 = (bf16[128,512]{1,0:T(8,128)(2,1)S(1)}, bf16[128,512]{1,0:T(8,128)(2,1)S(1)}, u32[]{:S(2)}, u32[]{:S(2)}) collective-permute-start(bf16[128,512]{1,0:T(8,128)(2,1)S(1)} %get-tuple-element.61), channel_id=1, source_target_pairs={{0,2},{1,3},{2,0},{3,1},{4,6},{5,7},{6,4},{7,5},{8,10},{9,11},{10,... | collective-permute-start | bytes 393224 | tf_op jit(solution)/shard_map/ppermute | solution.py:420
  46.0 4.2 %collective-permute-done.14.refs_6_ = bf16[128,512]{1,0:T(8,128)(2,1)S(1)} collective-permute-done((bf16[128,512]{1,0:T(8,128)(2,1)S(1)}, bf16[128,512]{1,0:T(8,128)(2,1)S(1)}, u32[]{:S(2)}, u32[]{:S(2)}) %collective-permute-start.14) | collective-permute-done | bytes 131104 | tf_op jit(solution)/shard_map/ppermute | solution.py:420
  50.2 2.0 %collective-permute-done.10.refs_2_ = bf16[128,512]{1,0:T(8,128)(2,1)S(1)} collective-permute-done((bf16[128,512]{1,0:T(8,128)(2,1)S(1)}, bf16[128,512]{1,0:T(8,128)(2,1)S(1)}, u32[]{:S(2)}, u32[]{:S(2)}) %collective-permute-start.10) | collective-permute-done | bytes 131104 | tf_op jit(solution)/shard_map/ppermute | solution.py:420
  52.2 0.8 %result.1 = bf16[256,512]{1,0:T(8,128)(2,1)} custom-call(bf16[128,1024]{1,0:T(8,128)(2,1)S(1)} %residual.2.mine_ref.refs_0_, bf16[128,512]{1,0:T(8,128)(2,1)S(1)} %get-tuple-element.60.refs_1_, bf16[128,512]{1,0:T(8,128)(2,1)S(1)} %collective-permute-done.10.refs_2_, bf16[128,1024]{1,0:T(8,128)(2,1)S(1)} %residual.3.mine_ref.refs_3_, ...), custom_call_target="tpu_custom_call" | custom-call | tf_op jit(solution)/shard_map/result/pallas_call | solution.py:682
  (43 shorter events, 4.3 us)
Async XLA Ops:
  0.0 5.3 %copy-start.4 = (bf16[256,2048]{1,0:T(8,128)(2,1)S(1)}, bf16[256,2048]{1,0:T(8,128)(2,1)}, u32[]{:S(2)}) copy-start(bf16[256,2048]{1,0:T(8,128)(2,1)} %x_ref.5) | copy-start | bytes 3145732
  2.3 10.2 %collective-permute-start = (bf16[128,256]{1,0:T(8,128)(2,1)S(1)}, bf16[128,256]{1,0:T(8,128)(2,1)S(1)}, u32[]{:S(2)}, u32[]{:S(2)}) collective-permute-start(bf16[128,256]{1,0:T(8,128)(2,1)S(1)} %get-tuple-element.38.refs_1_), channel_id=1, source_target_pairs={{0,4},{4,8},{8,12},{12,16},{16,20},{20,24},{24,28},{28,0},{1,5},{5... | collective-permute-start | bytes 196616 | tf_op jit(solution)/shard_map/ppermute | solution.py:426
  6.0 2.4 %copy-start.3 = (bf16[2,2048,512]{2,1,0:T(8,128)(2,1)S(1)}, bf16[2,2048,512]{2,1,0:T(8,128)(2,1)}, u32[]{:S(2)}) copy-start(bf16[2,2048,512]{2,1,0:T(8,128)(2,1)} %wq_ref.7) | copy-start | bytes 12582916
  6.0 2.4 %copy-start.7 = (f32[2,64]{1,0:T(2,128)S(1)}, f32[2,64]{1,0:T(2,128)}, u32[]{:S(2)}) copy-start(f32[2,64]{1,0:T(2,128)} %qg_ref.7) | copy-start | bytes 1540
  6.0 7.1 %collective-permute-start.5 = (bf16[128,256]{1,0:T(8,128)(2,1)S(1)}, bf16[128,256]{1,0:T(8,128)(2,1)S(1)}, u32[]{:S(2)}, u32[]{:S(2)}) collective-permute-start(bf16[128,256]{1,0:T(8,128)(2,1)S(1)} %get-tuple-element.43.refs_0_), channel_id=1, source_target_pairs={{0,4},{4,8},{8,12},{12,16},{16,20},{20,24},{24,28},{28,0},{1,5},{5... | collective-permute-start | bytes 196616 | tf_op jit(solution)/shard_map/ppermute | solution.py:426
  8.3 2.2 %copy-start = (bf16[2,512,2048]{2,1,0:T(8,128)(2,1)S(1)}, bf16[2,512,2048]{2,1,0:T(8,128)(2,1)}, u32[]{:S(2)}) copy-start(bf16[2,512,2048]{2,1,0:T(8,128)(2,1)} %wout_ref.7) | copy-start | bytes 12582916
  13.0 1.6 %collective-permute-start.1 = (bf16[128,1024]{1,0:T(8,128)(2,1)S(1)}, bf16[128,1024]{1,0:T(8,128)(2,1)S(1)}, u32[]{:S(2)}, u32[]{:S(2)}) collective-permute-start(bf16[128,1024]{1,0:T(8,128)(2,1)S(1)} %get-tuple-element.47), channel_id=1, source_target_pairs={{0,1},{1,0},{2,3},{3,2},{4,5},{5,4},{6,7},{7,6},{8,9},{9,8},{10,11... | collective-permute-start | bytes 786440 | tf_op jit(solution)/shard_map/ppermute | solution.py:420
  13.6 3.0 %collective-permute-start.6 = (bf16[128,1024]{1,0:T(8,128)(2,1)S(1)}, bf16[128,1024]{1,0:T(8,128)(2,1)S(1)}, u32[]{:S(2)}, u32[]{:S(2)}) collective-permute-start(bf16[128,1024]{1,0:T(8,128)(2,1)S(1)} %get-tuple-element.54), channel_id=1, source_target_pairs={{0,1},{1,0},{2,3},{3,2},{4,5},{5,4},{6,7},{7,6},{8,9},{9,8},{10,11... | collective-permute-start | bytes 786440 | tf_op jit(solution)/shard_map/ppermute | solution.py:420
  14.7 9.2 %collective-permute-start.2 = (bf16[128,1024]{1,0:T(8,128)(2,1)S(1)}, bf16[128,1024]{1,0:T(8,128)(2,1)S(1)}, u32[]{:S(2)}, u32[]{:S(2)}) collective-permute-start(bf16[128,1024]{1,0:T(8,128)(2,1)S(1)} %add.3.refs_0_), channel_id=1, source_target_pairs={{0,2},{1,3},{2,0},{3,1},{4,6},{5,7},{6,4},{7,5},{8,10},{9,11},{10,... | collective-permute-start | bytes 786440 | tf_op jit(solution)/shard_map/ppermute | solution.py:420
  16.6 12.1 %collective-permute-start.7 = (bf16[128,1024]{1,0:T(8,128)(2,1)S(1)}, bf16[128,1024]{1,0:T(8,128)(2,1)S(1)}, u32[]{:S(2)}, u32[]{:S(2)}) collective-permute-start(bf16[128,1024]{1,0:T(8,128)(2,1)S(1)} %add.4.refs_0_), channel_id=1, source_target_pairs={{0,2},{1,3},{2,0},{3,1},{4,6},{5,7},{6,4},{7,5},{8,10},{9,11},{10,... | collective-permute-start | bytes 786440 | tf_op jit(solution)/shard_map/ppermute | solution.py:420
  24.0 5.7 %copy-start.1 = (bf16[2,2048,128]{2,1,0:T(8,128)(2,1)S(1)}, bf16[2,2048,128]{2,1,0:T(8,128)(2,1)}, u32[]{:S(2)}) copy-start(bf16[2,2048,128]{2,1,0:T(8,128)(2,1)} %wk_ref.3) | copy-start | bytes 3145732
  24.0 5.7 %copy-start.2 = (bf16[2,2048,128]{2,1,0:T(8,128)(2,1)S(1)}, bf16[2,2048,128]{2,1,0:T(8,128)(2,1)}, u32[]{:S(2)}) copy-start(bf16[2,2048,128]{2,1,0:T(8,128)(2,1)} %wv_ref.3) | copy-start | bytes 3145732
  24.0 5.7 %copy-start.5 = (f32[2,2048]{1,0:T(2,128)S(1)}, f32[2,2048]{1,0:T(2,128)}, u32[]{:S(2)}) copy-start(f32[2,2048]{1,0:T(2,128)} %gain_ref.3) | copy-start | bytes 49156
  24.0 5.7 %copy-start.6 = (f32[2,64]{1,0:T(2,128)S(1)}, f32[2,64]{1,0:T(2,128)}, u32[]{:S(2)}) copy-start(f32[2,64]{1,0:T(2,128)} %kg_ref.3) | copy-start | bytes 1540
  24.1 5.6 %collective-permute-start.3 = (bf16[128,1024]{1,0:T(8,128)(2,1)S(1)}, bf16[128,1024]{1,0:T(8,128)(2,1)S(1)}, u32[]{:S(2)}, u32[]{:S(2)}) collective-permute-start(bf16[128,1024]{1,0:T(8,128)(2,1)S(1)} %residual.2.mine_ref.refs_0_), channel_id=1, source_target_pairs={{0,1},{1,0},{2,3},{3,2},{4,5},{5,4},{6,7},{7,6},{8,9},{9,8},{10,11... | collective-permute-start | bytes 786440 | tf_op jit(solution)/shard_map/ppermute | solution.py:420
  28.8 4.7 %collective-permute-start.8 = (bf16[128,1024]{1,0:T(8,128)(2,1)S(1)}, bf16[128,1024]{1,0:T(8,128)(2,1)S(1)}, u32[]{:S(2)}, u32[]{:S(2)}) collective-permute-start(bf16[128,1024]{1,0:T(8,128)(2,1)S(1)} %residual.3.mine_ref.refs_3_), channel_id=1, source_target_pairs={{0,1},{1,0},{2,3},{3,2},{4,5},{5,4},{6,7},{7,6},{8,9},{9,8},{10,11... | collective-permute-start | bytes 786440 | tf_op jit(solution)/shard_map/ppermute | solution.py:420
  30.4 7.2 %collective-permute-start.4 = (bf16[128,256]{1,0:T(8,128)(2,1)S(1)}, bf16[128,256]{1,0:T(8,128)(2,1)S(1)}, u32[]{:S(2)}, u32[]{:S(2)}) collective-permute-start(bf16[128,256]{1,0:T(8,128)(2,1)S(1)} %get-tuple-element.49.refs_0_), channel_id=1, source_target_pairs={{0,4},{4,8},{8,12},{12,16},{16,20},{20,24},{24,28},{28,0},{1,5},{5... | collective-permute-start | bytes 196616 | tf_op jit(solution)/shard_map/ppermute | solution.py:426
  34.9 7.0 %collective-permute-start.11 = (bf16[128,256]{1,0:T(8,128)(2,1)S(1)}, bf16[128,256]{1,0:T(8,128)(2,1)S(1)}, u32[]{:S(2)}, u32[]{:S(2)}) collective-permute-start(bf16[128,256]{1,0:T(8,128)(2,1)S(1)} %get-tuple-element.55.refs_1_.refs_0_), channel_id=1, source_target_pairs={{0,4},{4,8},{8,12},{12,16},{16,20},{20,24},{24,28},{28,0},{1,5},{5... | collective-permute-start | bytes 196616 | tf_op jit(solution)/shard_map/ppermute | solution.py:426
  38.7 6.6 %collective-permute-start.9 = (bf16[128,1024]{1,0:T(8,128)(2,1)S(1)}, bf16[128,1024]{1,0:T(8,128)(2,1)S(1)}, u32[]{:S(2)}, u32[]{:S(2)}) collective-permute-start(bf16[128,1024]{1,0:T(8,128)(2,1)S(1)} %get-tuple-element.59), channel_id=1, source_target_pairs={{0,1},{1,0},{2,3},{3,2},{4,5},{5,4},{6,7},{7,6},{8,9},{9,8},{10,11... | collective-permute-start | bytes 786440 | tf_op jit(solution)/shard_map/ppermute | solution.py:420
  42.3 1.4 %collective-permute-start.13 = (bf16[128,512]{1,0:T(8,128)(2,1)S(1)}, bf16[128,512]{1,0:T(8,128)(2,1)S(1)}, u32[]{:S(2)}, u32[]{:S(2)}) collective-permute-start(bf16[128,512]{1,0:T(8,128)(2,1)S(1)} %get-tuple-element.68), channel_id=1, source_target_pairs={{0,1},{1,0},{2,3},{3,2},{4,5},{5,4},{6,7},{7,6},{8,9},{9,8},{10,11... | collective-permute-start | bytes 393224 | tf_op jit(solution)/shard_map/ppermute | solution.py:420
  42.8 3.3 %collective-permute-start.12 = (bf16[128,512]{1,0:T(8,128)(2,1)S(1)}, bf16[128,512]{1,0:T(8,128)(2,1)S(1)}, u32[]{:S(2)}, u32[]{:S(2)}) collective-permute-start(bf16[128,512]{1,0:T(8,128)(2,1)S(1)} %get-tuple-element.67), channel_id=1, source_target_pairs={{0,1},{1,0},{2,3},{3,2},{4,5},{5,4},{6,7},{7,6},{8,9},{9,8},{10,11... | collective-permute-start | bytes 393224 | tf_op jit(solution)/shard_map/ppermute | solution.py:420
  43.8 6.4 %collective-permute-start.14 = (bf16[128,512]{1,0:T(8,128)(2,1)S(1)}, bf16[128,512]{1,0:T(8,128)(2,1)S(1)}, u32[]{:S(2)}, u32[]{:S(2)}) collective-permute-start(bf16[128,512]{1,0:T(8,128)(2,1)S(1)} %add.5), channel_id=1, source_target_pairs={{0,2},{1,3},{2,0},{3,1},{4,6},{5,7},{6,4},{7,5},{8,10},{9,11},{10,... | collective-permute-start | bytes 393224 | tf_op jit(solution)/shard_map/ppermute | solution.py:420
  45.4 6.8 %collective-permute-start.10 = (bf16[128,512]{1,0:T(8,128)(2,1)S(1)}, bf16[128,512]{1,0:T(8,128)(2,1)S(1)}, u32[]{:S(2)}, u32[]{:S(2)}) collective-permute-start(bf16[128,512]{1,0:T(8,128)(2,1)S(1)} %get-tuple-element.61), channel_id=1, source_target_pairs={{0,2},{1,3},{2,0},{3,1},{4,6},{5,7},{6,4},{7,5},{8,10},{9,11},{10,... | collective-permute-start | bytes 393224 | tf_op jit(solution)/shard_map/ppermute | solution.py:420
